TPU v7x, 256 devices: a whole 4x4x8 slice. The times are simulated.
256 devices in a mesh: kv: 64 (over z, y, core), tp: 4 (over x).
Axes of the slice: x: 4, y: 4, z: 8, core: 2. Of those that a mesh axis runs over, the one named last changes fastest.
Arguments:
- queries: bfloat16 [24576, 2048], P('kv', 'tp'), may hold values from -3 to 3
- key_heads: bfloat16 [24576, 512], P('kv', 'tp'), may hold values from -3 to 3
- values: bfloat16 [24576, 512], P('kv', 'tp'), may hold values from -6 to 6
- log_sums: float32 [32, 24576], P('tp', 'kv'), may hold values from 4 to 6
- out_grad: bfloat16 [24576, 2048], P('kv', 'tp'), may hold values from -12 to 12
- inputs: bfloat16 [24576, 4096], P('kv', 'tp'), may hold values from -0.059814453 to 0.059814453
- chosen: int32 [8, 384, 16], P('tp'), may hold values from -1 to 383, as said below
Outputs:
- query_grad: float32 [24576, 2048], P('kv', 'tp')
- key_grad: float32 [24576, 512], P('kv', 'tp')
- value_grad: float32 [24576, 512], P('kv', 'tp')
- weight_grad: float32 [4096, 512], P('kv', 'tp')
Inputs may be any that keep to these rules, and one draw needn't show every extreme that they name: `chosen`: for each key-value head and query block the used entries come first, are distinct, and none is above the query block's own number; -1 fills the rest. Up to 16 entries are used, all of them in some query blocks. For one key-value head, the query blocks held by one index of kv list at most one block of each other index of kv, and every index of kv but the first lists a block of the first.
All inputs are finite; a program needn't handle non-finite values.
Results may differ from a plain program's by a relative error of at most 0.014.
Values may be sent and summed in bfloat16 or wider, within the bound.
A program may use at most 128 MiB of HBM per device.

v0:
```python
import jax
import jax.numpy as jnp
from jax import lax
from jax.sharding import PartitionSpec as P

HD = 64
BLOCK = 64


def split_up(array, dim, count):
    lengths = array.shape
    pieces = array.reshape(*lengths[:dim], count, lengths[dim] // count, *lengths[dim + 1 :])
    return jnp.moveaxis(pieces, dim, 0)


def sum_at_owner(array, axis, dim):
    pieces = split_up(array, dim, lax.axis_size(axis))
    arrived = lax.all_to_all(pieces, axis, split_axis=0, concat_axis=0, tiled=True)
    return arrived.astype(jnp.float32).sum(axis=0)


def local(queries, key_heads, values, log_sums, out_grad, inputs, chosen):
    device_count = lax.axis_size("kv")
    my_index = lax.axis_index("kv")
    local_rows = queries.shape[0]
    blocks_here = local_rows // BLOCK
    groups_here = key_heads.shape[1] // HD
    heads_here = log_sums.shape[0]
    per_group = heads_here // groups_here
    list_size = chosen.shape[2]
    scaling = HD ** (-0.5)
    kv_pairs = jnp.concatenate(
        [
            key_heads.reshape(local_rows, groups_here, HD),
            values.reshape(local_rows, groups_here, HD),
        ],
        axis=2,
    )
    own_blocks = kv_pairs.reshape(blocks_here, BLOCK, groups_here, 2 * HD)
    my_lists = lax.dynamic_slice_in_dim(chosen, my_index * blocks_here, blocks_here, 1)
    offsets = jnp.arange(blocks_here, dtype=jnp.int32)
    other_devs = (jnp.arange(device_count) != my_index)[None, :, None]
    asked_for = chosen.reshape(groups_here, device_count, blocks_here * list_size)[..., None]
    asked_for = jnp.any(asked_for == my_index * blocks_here + offsets, axis=2) & other_devs
    outgoing = jnp.einsum(
        "grb,bkgc->rkgc",
        asked_for.astype(jnp.bfloat16),
        own_blocks,
        preferred_element_type=jnp.float32,
    ).astype(jnp.bfloat16)
    remote = lax.all_to_all(outgoing, "kv", split_axis=0, concat_axis=0, tiled=True)
    key_table = jnp.concatenate([remote, own_blocks], axis=0)
    owner_dev = my_lists // blocks_here
    is_valid = my_lists >= 0
    source = jnp.where(
        owner_dev == my_index, device_count + my_lists % blocks_here, jnp.maximum(owner_dev, 0)
    )
    group_col = jnp.arange(groups_here, dtype=jnp.int32)[:, None]
    key_offsets = jnp.arange(BLOCK, dtype=jnp.int32)

    def one_block(totals, position):
        slot_index = lax.dynamic_index_in_dim(source, position, 1, keepdims=False)
        block_list = lax.dynamic_index_in_dim(my_lists, position, 1, keepdims=False)
        list_valid = lax.dynamic_index_in_dim(is_valid, position, 1, keepdims=False)
        fetched = key_table[slot_index, :, group_col, :].reshape(
            groups_here, list_size * BLOCK, 2 * HD
        )
        key_part = fetched[..., :HD]
        value_part = fetched[..., HD:]
        first_row = position * BLOCK
        query_part = lax.dynamic_slice_in_dim(queries, first_row, BLOCK, 0).reshape(
            BLOCK, groups_here, per_group, HD
        )
        grad_part = lax.dynamic_slice_in_dim(out_grad, first_row, BLOCK, 0).reshape(
            BLOCK, groups_here, per_group, HD
        )
        sums_part = lax.dynamic_slice_in_dim(log_sums, first_row, BLOCK, 1).reshape(
            groups_here, per_group, BLOCK
        )
        scores = (
            jnp.einsum("igrd,gkd->grik", query_part, key_part, preferred_element_type=jnp.float32)
            * scaling
        )
        key_pos = (jnp.maximum(block_list, 0)[:, :, None] * BLOCK + key_offsets).reshape(
            groups_here, -1
        )
        key_valid = jnp.repeat(list_valid, BLOCK, axis=1)
        query_pos = (my_index * blocks_here + position) * BLOCK + key_offsets
        visible = key_valid[:, None, None, :] & (
            key_pos[:, None, None, :] <= query_pos[None, None, :, None]
        )
        prob_rows = jnp.where(visible, jnp.exp(scores - sums_part[..., None]), 0.0)
        prob_grad = jnp.einsum(
            "igrd,gkd->grik", grad_part, value_part, preferred_element_type=jnp.float32
        )
        row_delta = jnp.sum(prob_rows * prob_grad, axis=-1, keepdims=True)
        score_grad = prob_rows * (prob_grad - row_delta)
        prob_half = prob_rows.astype(jnp.bfloat16)
        score_half = score_grad.astype(jnp.bfloat16)
        query_part_grad = (
            jnp.einsum("grik,gkd->igrd", score_half, key_part, preferred_element_type=jnp.float32)
            * scaling
        )
        key_contrib = (
            jnp.einsum("grik,igrd->gkd", score_half, query_part, preferred_element_type=jnp.float32)
            * scaling
        )
        value_contrib = jnp.einsum(
            "grik,igrd->gkd", prob_half, grad_part, preferred_element_type=jnp.float32
        )
        contribs = jnp.concatenate([key_contrib, value_contrib], axis=2).reshape(
            groups_here, list_size, BLOCK, 2 * HD
        )
        totals = totals.at[slot_index, :, group_col, :].add(contribs)
        return (totals, query_part_grad.reshape(BLOCK, heads_here * HD))

    start_totals = jnp.zeros((device_count + blocks_here, BLOCK, groups_here, 2 * HD), jnp.float32)
    totals, query_blocks = lax.scan(
        one_block, start_totals, jnp.arange(blocks_here, dtype=jnp.int32)
    )
    query_grad = query_blocks.reshape(local_rows, heads_here * HD)
    returned = lax.all_to_all(
        totals[:device_count].astype(jnp.bfloat16), "kv", split_axis=0, concat_axis=0, tiled=True
    ).astype(jnp.float32)
    summed = totals[device_count:] + jnp.einsum(
        "grb,rkgc->bkgc", asked_for.astype(jnp.float32), returned, precision=lax.Precision.HIGHEST
    )
    summed = summed.reshape(local_rows, groups_here, 2 * HD)
    key_grad = summed[..., :HD].reshape(local_rows, groups_here * HD)
    value_grad = summed[..., HD:].reshape(local_rows, groups_here * HD)
    whole_inputs = lax.all_gather(inputs, "tp", axis=1, tiled=True)
    key_half = key_grad.astype(jnp.bfloat16)
    weight_grad = sum_at_owner(
        lax.dot_general(
            whole_inputs, key_half, (((0,), (0,)), ((), ())), preferred_element_type=jnp.float32
        ).astype(jnp.bfloat16),
        "kv",
        0,
    )
    return (query_grad, key_grad, value_grad, weight_grad)


def solution(mesh):
    placed = (
        P("kv", "tp"),
        P("kv", "tp"),
        P("kv", "tp"),
        P("tp", "kv"),
        P("kv", "tp"),
        P("kv", "tp"),
        P("tp", None, None),
    )
    return jax.shard_map(
        local,
        mesh=mesh,
        in_specs=placed,
        out_specs=(P("kv", "tp"), P("kv", "tp"), P("kv", "tp"), P("kv", "tp")),
        check_vma=False,
    )
```

profile of v0, /device:TPU:6, one launch (start us, length us, event | category | flops | bytes accessed | tf_op | source)
XLA Modules:
  0.0 308.4 jit_solution(11476069297831048445)
XLA Ops:
  7.2 1.0 copy.71
  8.3 1.0 concatenate.22
  9.5 1.0 concatenate.23
  12.0 2.7 copy.72
  14.6 12.1 %all-to-all-start = ((bf16[64,64,2,128]{3,1,2,0:T(8,128)(2,1)}), bf16[64,64,2,128]{3,1,2,0:T(8,128)(2,1)S(1)}, u32[]{:S(2)}, u32[]{:S(2)}) async-start(bf16[64,64,2,128]{3,1,2,0:T(8,128)(2,1)} %copy.72), calls=%async_computation | async-start | bytes 4194304 | tf_op jit(solution)/shard_map/all_to_all | solution.py:51
  28.5 49.6 %all-to-all-done = bf16[64,64,2,128]{3,1,2,0:T(8,128)(2,1)S(1)} async-done(((bf16[64,64,2,128]{3,1,2,0:T(8,128)(2,1)}), bf16[64,64,2,128]{3,1,2,0:T(8,128)(2,1)S(1)}, u32[]{:S(2)}, u32[]{:S(2)}) %all-to-all-start) | async-done | bytes 2097184 | tf_op jit(solution)/shard_map/all_to_all | solution.py:51
  78.1 1.6 pad_maximum_fusion.1
  79.7 2.7 broadcast_in_dim.53
  82.4 117.4 %while.16 = (s32[]{:T(128)}, f32[70,64,2,128]{3,1,2,0:T(8,128)}, f32[6,64,512]{2,1,0:T(8,128)}, s32[6]{0:T(128)S(1)}, s32[2,6,16]{2,0,1:T(2,128)S(1)}, /*index=5...) while((s32[]{:T(128)}, f32[70,64,2,128]{3,1,2,0:T(8,128)}, ...), condition=%wide.region_4.5_spmd.clone.clone, body=%wide.region_1.4_spmd.clone.clone.sunk | while | flops 341215168 | bytes 32724180 | solution.py:118
  83.6 0.9 constant_dynamic-slice_fusion.8
  86.8 2.3 gather_fusion
  94.3 6.5 %scatter_fusion = f32[70,64,2,128]{3,1,2,0:T(8,128)} fusion(f32[70,64,2,128]{3,1,2,0:T(8,128)} %get-tuple-element.400, s32[32]{0:T(128)S(1)} %reshape.219, f32[32,64,128]{2,1,0:T(8,128)S(1)} %bitcast.142), kind=kCustom, calls=%fused_computation.1.clone.clone.1 | custom fusion | flops 262144 | bytes 3145984 | tf_op jit(solution)/shard_map/while/body/eval_jaxpr/scatter-add | solution.py:114
  103.5 0.9 constant_dynamic-slice_fusion.8
  106.6 2.3 gather_fusion
  114.2 6.4 %scatter_fusion = f32[70,64,2,128]{3,1,2,0:T(8,128)} fusion(f32[70,64,2,128]{3,1,2,0:T(8,128)} %get-tuple-element.400, s32[32]{0:T(128)S(1)} %reshape.219, f32[32,64,128]{2,1,0:T(8,128)S(1)} %bitcast.142), kind=kCustom, calls=%fused_computation.1.clone.clone.1 | custom fusion | flops 262144 | bytes 3145984 | tf_op jit(solution)/shard_map/while/body/eval_jaxpr/scatter-add | solution.py:114
  126.4 2.3 gather_fusion
  134.0 6.3 %scatter_fusion = f32[70,64,2,128]{3,1,2,0:T(8,128)} fusion(f32[70,64,2,128]{3,1,2,0:T(8,128)} %get-tuple-element.400, s32[32]{0:T(128)S(1)} %reshape.219, f32[32,64,128]{2,1,0:T(8,128)S(1)} %bitcast.142), kind=kCustom, calls=%fused_computation.1.clone.clone.1 | custom fusion | flops 262144 | bytes 3145984 | tf_op jit(solution)/shard_map/while/body/eval_jaxpr/scatter-add | solution.py:114
  146.0 2.3 gather_fusion
  153.6 6.2 %scatter_fusion = f32[70,64,2,128]{3,1,2,0:T(8,128)} fusion(f32[70,64,2,128]{3,1,2,0:T(8,128)} %get-tuple-element.400, s32[32]{0:T(128)S(1)} %reshape.219, f32[32,64,128]{2,1,0:T(8,128)S(1)} %bitcast.142), kind=kCustom, calls=%fused_computation.1.clone.clone.1 | custom fusion | flops 262144 | bytes 3145984 | tf_op jit(solution)/shard_map/while/body/eval_jaxpr/scatter-add | solution.py:114
  165.6 2.3 gather_fusion
  173.1 6.0 %scatter_fusion = f32[70,64,2,128]{3,1,2,0:T(8,128)} fusion(f32[70,64,2,128]{3,1,2,0:T(8,128)} %get-tuple-element.400, s32[32]{0:T(128)S(1)} %reshape.219, f32[32,64,128]{2,1,0:T(8,128)S(1)} %bitcast.142), kind=kCustom, calls=%fused_computation.1.clone.clone.1 | custom fusion | flops 262144 | bytes 3145984 | tf_op jit(solution)/shard_map/while/body/eval_jaxpr/scatter-add | solution.py:114
  185.0 2.3 gather_fusion
  192.5 5.9 %scatter_fusion = f32[70,64,2,128]{3,1,2,0:T(8,128)} fusion(f32[70,64,2,128]{3,1,2,0:T(8,128)} %get-tuple-element.400, s32[32]{0:T(128)S(1)} %reshape.219, f32[32,64,128]{2,1,0:T(8,128)S(1)} %bitcast.142), kind=kCustom, calls=%fused_computation.1.clone.clone.1 | custom fusion | flops 262144 | bytes 3145984 | tf_op jit(solution)/shard_map/while/body/eval_jaxpr/scatter-add | solution.py:114
  199.8 4.1 %slice.48 = bf16[64,64,2,128]{3,1,2,0:T(8,128)(2,1)} slice(f32[70,64,2,128]{3,1,2,0:T(8,128)} %get-tuple-element.169), slice={[0:64], [0:64], [0:2], [0:128]} | slice | bytes 4194304 | tf_op jit(solution)/shard_map/slice | solution.py:123
  203.9 4.9 %all-to-all-start.1 = ((bf16[64,64,2,128]{3,1,2,0:T(8,128)(2,1)}), bf16[64,64,2,128]{3,1,2,0:T(8,128)(2,1)S(1)}, u32[]{:S(2)}, u32[]{:S(2)}) async-start(bf16[64,64,2,128]{3,1,2,0:T(8,128)(2,1)} %slice.48), calls=%async_computation.1 | async-start | bytes 4194304 | tf_op jit(solution)/shard_map/all_to_all | solution.py:122
  208.8 7.1 %copy.75 = f32[70,64,2,128]{3,0,1,2:T(8,128)} copy(f32[70,64,2,128]{3,1,2,0:T(8,128)} %get-tuple-element.169) | data formatting | bytes 9175040 | tf_op jit(solution)/shard_map/while | solution.py:118
  215.9 44.1 %all-to-all-done.1 = bf16[64,64,2,128]{3,1,2,0:T(8,128)(2,1)S(1)} async-done(((bf16[64,64,2,128]{3,1,2,0:T(8,128)(2,1)}), bf16[64,64,2,128]{3,1,2,0:T(8,128)(2,1)S(1)}, u32[]{:S(2)}, u32[]{:S(2)}) %all-to-all-start.1) | async-done | bytes 2097184 | tf_op jit(solution)/shard_map/all_to_all | solution.py:122
  259.9 2.3 fusion.24
  262.6 2.6 fusion.18
  265.3 1.3 copy.80
  266.6 5.3 %all-to-all-start.2 = ((bf16[64,64,128]{2,1,0:T(8,128)(2,1)}), bf16[64,64,128]{2,1,0:T(8,128)(2,1)S(1)}, u32[]{:S(2)}, u32[]{:S(2)}) async-start(bf16[64,64,128]{2,1,0:T(8,128)(2,1)} %bitcast.10), calls=%async_computation.2 | async-start | bytes 2097152 | tf_op jit(solution)/shard_map/all_to_all | solution.py:18
  273.7 27.1 %all-to-all-done.2 = bf16[64,64,128]{2,1,0:T(8,128)(2,1)S(1)} async-done(((bf16[64,64,128]{2,1,0:T(8,128)(2,1)}), bf16[64,64,128]{2,1,0:T(8,128)(2,1)S(1)}, u32[]{:S(2)}, u32[]{:S(2)}) %all-to-all-start.2) | async-done | bytes 1048608 | tf_op jit(solution)/shard_map/all_to_all | solution.py:18
  (233 shorter events, 50.4 us)
Async XLA Ops:
  14.6 63.4 %all-to-all-start = ((bf16[64,64,2,128]{3,1,2,0:T(8,128)(2,1)}), bf16[64,64,2,128]{3,1,2,0:T(8,128)(2,1)S(1)}, u32[]{:S(2)}, u32[]{:S(2)}) async-start(bf16[64,64,2,128]{3,1,2,0:T(8,128)(2,1)} %copy.72), calls=%async_computation | async-start | bytes 4194304 | tf_op jit(solution)/shard_map/all_to_all | solution.py:51
  26.8 235.9 %all-gather.2.cloned.1.call-start = ((), (), s32[]{:S(2)}) async-start(), calls=%async_computation.3 | async-start | bytes 3932160 | tf_op jit(solution)/shard_map/all_gather | solution.py:131
  89.1 3.6 %copy-start = (bf16[32,64,128]{2,1,0:T(8,128)(2,1)}, bf16[32,64,128]{2,1,0:T(8,128)(2,1)S(1)}, u32[]{:S(2)}) copy-start(bf16[32,64,128]{2,1,0:T(8,128)(2,1)S(1)} %gather_fusion) | copy-start | bytes 1572868 | tf_op jit(solution)/shard_map/while
  94.2 6.6 %copy-start.1 = (bf16[32,64,128]{2,1,0:T(8,128)(2,1)S(1)}, bf16[32,64,128]{2,1,0:T(8,128)(2,1)}, u32[]{:S(2)}) copy-start(bf16[32,64,128]{2,1,0:T(8,128)(2,1)} %copy-done) | copy-start | bytes 1572868 | tf_op jit(solution)/shard_map/while
  109.0 3.6 %copy-start = (bf16[32,64,128]{2,1,0:T(8,128)(2,1)}, bf16[32,64,128]{2,1,0:T(8,128)(2,1)S(1)}, u32[]{:S(2)}) copy-start(bf16[32,64,128]{2,1,0:T(8,128)(2,1)S(1)} %gather_fusion) | copy-start | bytes 1572868 | tf_op jit(solution)/shard_map/while
  114.1 6.5 %copy-start.1 = (bf16[32,64,128]{2,1,0:T(8,128)(2,1)S(1)}, bf16[32,64,128]{2,1,0:T(8,128)(2,1)}, u32[]{:S(2)}) copy-start(bf16[32,64,128]{2,1,0:T(8,128)(2,1)} %copy-done) | copy-start | bytes 1572868 | tf_op jit(solution)/shard_map/while
  128.7 3.6 %copy-start = (bf16[32,64,128]{2,1,0:T(8,128)(2,1)}, bf16[32,64,128]{2,1,0:T(8,128)(2,1)S(1)}, u32[]{:S(2)}) copy-start(bf16[32,64,128]{2,1,0:T(8,128)(2,1)S(1)} %gather_fusion) | copy-start | bytes 1572868 | tf_op jit(solution)/shard_map/while
  133.9 6.4 %copy-start.1 = (bf16[32,64,128]{2,1,0:T(8,128)(2,1)S(1)}, bf16[32,64,128]{2,1,0:T(8,128)(2,1)}, u32[]{:S(2)}) copy-start(bf16[32,64,128]{2,1,0:T(8,128)(2,1)} %copy-done) | copy-start | bytes 1572868 | tf_op jit(solution)/shard_map/while
  148.4 3.6 %copy-start = (bf16[32,64,128]{2,1,0:T(8,128)(2,1)}, bf16[32,64,128]{2,1,0:T(8,128)(2,1)S(1)}, u32[]{:S(2)}) copy-start(bf16[32,64,128]{2,1,0:T(8,128)(2,1)S(1)} %gather_fusion) | copy-start | bytes 1572868 | tf_op jit(solution)/shard_map/while
  153.5 6.3 %copy-start.1 = (bf16[32,64,128]{2,1,0:T(8,128)(2,1)S(1)}, bf16[32,64,128]{2,1,0:T(8,128)(2,1)}, u32[]{:S(2)}) copy-start(bf16[32,64,128]{2,1,0:T(8,128)(2,1)} %copy-done) | copy-start | bytes 1572868 | tf_op jit(solution)/shard_map/while
  167.9 3.6 %copy-start = (bf16[32,64,128]{2,1,0:T(8,128)(2,1)}, bf16[32,64,128]{2,1,0:T(8,128)(2,1)S(1)}, u32[]{:S(2)}) copy-start(bf16[32,64,128]{2,1,0:T(8,128)(2,1)S(1)} %gather_fusion) | copy-start | bytes 1572868 | tf_op jit(solution)/shard_map/while
  173.0 6.1 %copy-start.1 = (bf16[32,64,128]{2,1,0:T(8,128)(2,1)S(1)}, bf16[32,64,128]{2,1,0:T(8,128)(2,1)}, u32[]{:S(2)}) copy-start(bf16[32,64,128]{2,1,0:T(8,128)(2,1)} %copy-done) | copy-start | bytes 1572868 | tf_op jit(solution)/shard_map/while
  187.3 3.6 %copy-start = (bf16[32,64,128]{2,1,0:T(8,128)(2,1)}, bf16[32,64,128]{2,1,0:T(8,128)(2,1)S(1)}, u32[]{:S(2)}) copy-start(bf16[32,64,128]{2,1,0:T(8,128)(2,1)S(1)} %gather_fusion) | copy-start | bytes 1572868 | tf_op jit(solution)/shard_map/while
  192.4 6.0 %copy-start.1 = (bf16[32,64,128]{2,1,0:T(8,128)(2,1)S(1)}, bf16[32,64,128]{2,1,0:T(8,128)(2,1)}, u32[]{:S(2)}) copy-start(bf16[32,64,128]{2,1,0:T(8,128)(2,1)} %copy-done) | copy-start | bytes 1572868 | tf_op jit(solution)/shard_map/while
  203.9 56.0 %all-to-all-start.1 = ((bf16[64,64,2,128]{3,1,2,0:T(8,128)(2,1)}), bf16[64,64,2,128]{3,1,2,0:T(8,128)(2,1)S(1)}, u32[]{:S(2)}, u32[]{:S(2)}) async-start(bf16[64,64,2,128]{3,1,2,0:T(8,128)(2,1)} %slice.48), calls=%async_computation.1 | async-start | bytes 4194304 | tf_op jit(solution)/shard_map/all_to_all | solution.py:122
  266.6 34.2 %all-to-all-start.2 = ((bf16[64,64,128]{2,1,0:T(8,128)(2,1)}), bf16[64,64,128]{2,1,0:T(8,128)(2,1)S(1)}, u32[]{:S(2)}, u32[]{:S(2)}) async-start(bf16[64,64,128]{2,1,0:T(8,128)(2,1)} %bitcast.10), calls=%async_computation.2 | async-start | bytes 2097152 | tf_op jit(solution)/shard_map/all_to_all | solution.py:18
Sparse Core Ops, SparseCore 0:
  29.4 41.2 all-gather.1
where the time goes:
time: 312 us; the launch traced here: 308 us
  waiting for transfers between devices  121 us (39%)
  local copies, waits for them, and re-layouts  63.2 us (20%)
  other arithmetic  45 us (14%)
  starting transfers between devices  22.4 us (7%)
  matrix products  21.8 us (7%)
  loops' own time  20.4 us (7%)
  between operations  14.2 us (5%)
    all_to_all x1, waiting for transfers between devices, local(): lax.all_to_all(outgoing, 'kv', split_axis=0, concat_axis=0, tiled=True)  49.6 us
    all_to_all x1, waiting for transfers between devices, local(): lax.all_to_all(totals[:device_count].astype(jnp.bfloat16), 'kv', split_ax...  44.1 us
    scatter-add x6, other arithmetic, one_block(): totals = totals.at[slot_index, :, group_col, :].add(contribs)  37.4 us
    all_to_all x1, waiting for transfers between devices, sum_at_owner(): lax.all_to_all(pieces, axis, split_axis=0, concat_axis=0, tiled=True)  27.1 us
    another operation x1, loops' own time, local(): lax.scan(one_block, start_totals, jnp.arange(blocks_here, dtype=jnp.int32))  20.4 us
    gather x6, local copies, waits for them, and re-layouts, one_block(): key_table[slot_index, :, group_col, :]  13.9 us
    all_to_all x1, starting transfers between devices, local(): lax.all_to_all(outgoing, 'kv', split_axis=0, concat_axis=0, tiled=True)  12.1 us
    while x1, local copies, waits for them, and re-layouts, local(): lax.scan(one_block, start_totals, jnp.arange(blocks_here, dtype=jnp.int32))  7.08 us
  transfers between devices with their start and end apart: 4, of which 3 were waited for; matrix products, arithmetic and copies ran while one was open for 38% of the time, Pallas kernels for 0%

commit v1 on v0

v1 whole, which is shorter than its diff:
```python
import functools

import jax
import jax.numpy as jnp
from jax import lax
from jax.experimental import pallas as pl
from jax.experimental.pallas import tpu as pltpu
from jax.sharding import PartitionSpec as P

HD = 64
BLOCK = 64
NEG = -1e30


def attention_kernel(
    slots, kinds, table, keys, vals, queries, out_grad, lse,
    query_grad, remote_tot, own_tot,
    tab, tot, bias, k_cat, v_cat, s_scr, dp_scr, p16, ds16, dk, dv,
    *, n_dev, n_blocks, n_list, per_group, groups,
):
    cols = per_group * BLOCK
    n_keys = n_list * BLOCK
    lane = lax.broadcasted_iota(jnp.int32, (BLOCK, 128), 1)
    tab[:n_dev] = table[...]
    for b in range(n_blocks):
        tab[n_dev + b, 0] = keys[b * BLOCK : (b + 1) * BLOCK, :]
        tab[n_dev + b, 1] = vals[b * BLOCK : (b + 1) * BLOCK, :]
    key_at = lax.broadcasted_iota(jnp.int32, (BLOCK, cols), 0)
    tok_at = lax.broadcasted_iota(jnp.int32, (BLOCK, cols), 1) % BLOCK
    bias[0] = jnp.zeros((BLOCK, cols), jnp.float32)
    bias[1] = jnp.where(key_at <= tok_at, 0.0, NEG)
    bias[2] = jnp.full((BLOCK, cols), NEG, jnp.float32)

    def clear(j, c):
        tot[j] = jnp.zeros((2, BLOCK, 128), jnp.float32)
        return c

    lax.fori_loop(0, n_dev + n_blocks, clear, 0)

    def masked_rows(ref, row, g, factor):
        mine = (lane >= HD) if g else (lane < HD)
        parts = []
        for r in range(per_group):
            col = (g * per_group + r) * HD
            tile = ref[pl.ds(row, BLOCK), col // 128 * 128 : col // 128 * 128 + 128]
            tile = tile.astype(jnp.float32) * factor
            if (r % 2) != g:
                tile = pltpu.roll(tile, HD, 1)
            parts.append(jnp.where(mine, tile, 0.0).astype(jnp.bfloat16))
        return jnp.concatenate(parts, axis=0)

    def one_position(p, c):
        row = pl.multiple_of(p * BLOCK, BLOCK)
        for g in range(groups):
            unit = p * groups + g
            q_rows = masked_rows(queries, row, g, HD ** -0.5)
            g_rows = masked_rows(out_grad, row, g, 1.0)
            for n in range(n_list):
                slot = slots[unit * n_list + n]
                k_cat[n * BLOCK : (n + 1) * BLOCK, :] = tab[slot, 0]
                v_cat[n * BLOCK : (n + 1) * BLOCK, :] = tab[slot, 1]
            nt = (((1,), (1,)), ((), ()))
            s_scr[...] = lax.dot_general(k_cat[...], q_rows, nt, preferred_element_type=jnp.float32)
            dp_scr[...] = lax.dot_general(v_cat[...], g_rows, nt, preferred_element_type=jnp.float32)
            lse_row = lse[pl.ds(unit, 1), :]

            def probs(n, acc):
                at = pl.ds(pl.multiple_of(n * BLOCK, BLOCK), BLOCK)
                pr = jnp.exp((s_scr[at, :] - lse_row) + bias[kinds[unit * n_list + n]])
                s_scr[at, :] = pr
                p16[at, :] = pr.astype(jnp.bfloat16)
                return acc + (pr * dp_scr[at, :]).reshape(BLOCK // 8, 8, cols).sum(axis=0)

            acc = lax.fori_loop(0, n_list, probs, jnp.zeros((8, cols), jnp.float32), unroll=4)
            delta = acc.sum(axis=0, keepdims=True)

            def grads(n, carry):
                at = pl.ds(pl.multiple_of(n * BLOCK, BLOCK), BLOCK)
                ds16[at, :] = (s_scr[at, :] * (dp_scr[at, :] - delta)).astype(jnp.bfloat16)
                return carry

            lax.fori_loop(0, n_list, grads, 0, unroll=4)
            nn = (((1,), (0,)), ((), ()))
            dk[...] = lax.dot_general(ds16[...], q_rows, nn, preferred_element_type=jnp.float32)
            dv[...] = lax.dot_general(p16[...], g_rows, nn, preferred_element_type=jnp.float32)
            dq_t = lax.dot_general(
                k_cat[...], ds16[...], (((0,), (0,)), ((), ())), preferred_element_type=jnp.float32
            )
            dq = dq_t.T * (HD ** -0.5)

            def spread(n, carry):
                at = pl.ds(pl.multiple_of(n * BLOCK, BLOCK), BLOCK)
                slot = slots[unit * n_list + n]
                tot[slot, 0] += dk[at, :]
                tot[slot, 1] += dv[at, :]
                return carry

            lax.fori_loop(0, n_list, spread, 0, unroll=2)
            for pair in range(per_group // 2):
                even = dq[(2 * pair) * BLOCK : (2 * pair + 1) * BLOCK]
                odd = dq[(2 * pair + 1) * BLOCK : (2 * pair + 2) * BLOCK]
                if g:
                    even = pltpu.roll(even, HD, 1)
                else:
                    odd = pltpu.roll(odd, HD, 1)
                col = g * per_group * HD + pair * 128
                query_grad[pl.ds(row, BLOCK), col : col + 128] = jnp.where(lane < HD, even, odd)
        return c

    lax.fori_loop(0, n_blocks, one_position, 0)

    def put(j, c):
        remote_tot[j] = tot[j].astype(jnp.bfloat16)
        return c

    lax.fori_loop(0, n_dev, put, 0)
    own_tot[...] = tot[n_dev:]


def attention(slots, kinds, table, keys, vals, queries, out_grad, lse, *, n_list):
    n_dev = table.shape[0]
    rows = keys.shape[0]
    n_blocks = rows // BLOCK
    groups = keys.shape[1] // HD
    per_group = queries.shape[1] // HD // groups
    cols = per_group * BLOCK
    n_keys = n_list * BLOCK
    vm = pl.BlockSpec(memory_space=pltpu.VMEM)
    sm = pl.BlockSpec(memory_space=pltpu.SMEM)
    f32, bf16 = jnp.float32, jnp.bfloat16
    return pl.pallas_call(
        functools.partial(
            attention_kernel, n_dev=n_dev, n_blocks=n_blocks, n_list=n_list,
            per_group=per_group, groups=groups,
        ),
        out_shape=(
            jax.ShapeDtypeStruct(queries.shape, f32),
            jax.ShapeDtypeStruct((n_dev, 2, BLOCK, 128), bf16),
            jax.ShapeDtypeStruct((n_blocks, 2, BLOCK, 128), f32),
        ),
        in_specs=[sm, sm] + [vm] * 6,
        out_specs=(vm, vm, vm),
        scratch_shapes=[
            pltpu.VMEM((n_dev + n_blocks, 2, BLOCK, 128), bf16),
            pltpu.VMEM((n_dev + n_blocks, 2, BLOCK, 128), f32),
            pltpu.VMEM((3, BLOCK, cols), f32),
            pltpu.VMEM((n_keys, 128), bf16),
            pltpu.VMEM((n_keys, 128), bf16),
            pltpu.VMEM((n_keys, cols), f32),
            pltpu.VMEM((n_keys, cols), f32),
            pltpu.VMEM((n_keys, cols), bf16),
            pltpu.VMEM((n_keys, cols), bf16),
            pltpu.VMEM((n_keys, 128), f32),
            pltpu.VMEM((n_keys, 128), f32),
        ],
        compiler_params=pltpu.CompilerParams(vmem_limit_bytes=48 * 1024 * 1024),
        cost_estimate=pl.CostEstimate(
            flops=10 * n_blocks * groups * n_keys * cols * 128,
            bytes_accessed=8 * 1024 * 1024,
            transcendentals=n_blocks * groups * n_keys * cols,
        ),
        name="attention",
    )(slots, kinds, table, keys, vals, queries, out_grad, lse)


def sum_at_owner(array, axis):
    count = lax.axis_size(axis)
    pieces = array.reshape(count, array.shape[0] // count, array.shape[1])
    arrived = lax.all_to_all(pieces, axis, split_axis=0, concat_axis=0, tiled=True)
    return arrived.astype(jnp.float32).sum(axis=0)


def local(queries, key_heads, values, log_sums, out_grad, inputs, chosen):
    n_dev = lax.axis_size("kv")
    me = lax.axis_index("kv")
    rows = queries.shape[0]
    n_blocks = rows // BLOCK
    groups = key_heads.shape[1] // HD
    per_group = log_sums.shape[0] // groups
    n_list = chosen.shape[2]

    my_lists = lax.dynamic_slice_in_dim(chosen, me * n_blocks, n_blocks, 1)
    owner = my_lists // n_blocks
    slot = jnp.where(owner == me, n_dev + my_lists % n_blocks, jnp.maximum(owner, 0))
    kind = jnp.where(
        my_lists < 0,
        2,
        (my_lists == me * n_blocks + jnp.arange(n_blocks)[None, :, None]).astype(jnp.int32),
    )
    slots = slot.transpose(1, 0, 2).reshape(-1)
    kinds = kind.transpose(1, 0, 2).reshape(-1)
    lse = log_sums.reshape(groups, per_group, n_blocks, BLOCK).transpose(2, 0, 1, 3)
    lse = lse.reshape(n_blocks * groups, per_group * BLOCK)

    entries = chosen.reshape(groups, n_dev, n_blocks * n_list)
    rel = entries - me * n_blocks
    mine = (rel >= 0) & (rel < n_blocks)
    sel = jnp.max(jnp.where(mine, rel, -1), axis=2)
    sel = jnp.where(jnp.arange(n_dev)[None] == me, -1, sel)
    sel_lane = jnp.repeat(sel.T, HD, axis=1)[:, None, None, :]
    own = jnp.stack([key_heads.reshape(n_blocks, BLOCK, -1), values.reshape(n_blocks, BLOCK, -1)], axis=1)
    outgoing = jnp.zeros((n_dev,) + own.shape[1:], jnp.bfloat16)
    for b in range(n_blocks):
        outgoing = jnp.where(sel_lane == b, own[b][None], outgoing)
    table = lax.all_to_all(outgoing, "kv", split_axis=0, concat_axis=0, tiled=True)

    query_grad, remote_tot, own_tot = attention(
        slots, kinds, table, key_heads, values, queries, out_grad, lse, n_list=n_list
    )
    returned = lax.all_to_all(remote_tot, "kv", split_axis=0, concat_axis=0, tiled=True)
    returned = returned.astype(jnp.float32)
    total = [
        own_tot[b] + jnp.sum(jnp.where(sel_lane == b, returned, 0.0), axis=0) for b in range(n_blocks)
    ]
    total = jnp.stack(total, axis=0)
    key_grad = total[:, 0].reshape(rows, -1)
    value_grad = total[:, 1].reshape(rows, -1)
    whole_inputs = lax.all_gather(inputs, "tp", axis=1, tiled=True)
    weight_grad = sum_at_owner(
        lax.dot_general(
            whole_inputs, key_grad.astype(jnp.bfloat16), (((0,), (0,)), ((), ())),
            preferred_element_type=jnp.float32,
        ).astype(jnp.bfloat16),
        "kv",
    )
    return (query_grad, key_grad, value_grad, weight_grad)


def solution(mesh):
    placed = (
        P("kv", "tp"),
        P("kv", "tp"),
        P("kv", "tp"),
        P("tp", "kv"),
        P("kv", "tp"),
        P("kv", "tp"),
        P("tp", None, None),
    )
    return jax.shard_map(
        local,
        mesh=mesh,
        in_specs=placed,
        out_specs=(P("kv", "tp"), P("kv", "tp"), P("kv", "tp"), P("kv", "tp")),
        check_vma=False,
    )
```

time: 312 us -> 208 us (0.67)
  local copies, waits for them, and re-layouts: 63.2 us -> 4.04 us
  other arithmetic: 45 us -> 8.96 us
  blocking collectives: 0 us -> 34 us
  Pallas kernels: 0 us -> 24.2 us
  loops' own time: 20.4 us -> 0 us
  waiting for transfers between devices: 121 us -> 101 us
  matrix products: 21.8 us -> 2.7 us
  starting transfers between devices: 22.4 us -> 17.6 us
    scatter-add x6 -> x0, other arithmetic: 37.4 us -> none  [one_block(): totals = totals.at[slot_index, :, group_col, :].add(contribs)]
    all_to_all x0 -> x1, blocking collectives: none -> 34 us  [sum_at_owner(): lax.all_to_all(pieces, axis, split_axis=0, concat_axis=0, tiled=True)]
    pallas_call x0 -> x1, Pallas kernels: none -> 24.2 us  [attention(): pl.pallas_call(functools.partial(attention_kernel, n_dev=n_dev, n_blocks=...]
    all_to_all x2 -> x1, waiting for transfers between devices: 71.2 us -> 50.6 us  [local(): lax.all_to_all(remote_tot, 'kv', split_axis=0, concat_axis=0, tiled=True)]
    another operation x1 -> x0, loops' own time: 20.4 us -> none  [local(): lax.scan(one_block, start_totals, jnp.arange(blocks_here, dtype=jnp.int32))]
    dot_general x33 -> x1, matrix products: 21.8 us -> 2.7 us  [local(): lax.dot_general(whole_inputs, key_grad.astype(jnp.bfloat16), (((0,), (0,)...]
    dynamic_slice x19 -> x0, local copies, waits for them, and re-layouts: 14.2 us -> none  [the longest x6 5.32 us: one_block(): lax.dynamic_slice_in_dim(out_grad, first_row, BLOCK, 0)]
    gather x6 -> x0, local copies, waits for them, and re-layouts: 13.9 us -> none  [one_block(): key_table[slot_index, :, group_col, :]]
  transfers between devices with their start and end apart: 4 -> 3, of which waited for: 3 -> 2; matrix products, arithmetic and copies ran while one was open for 38% -> 3% of each run, Pallas kernels for 0% -> 0%
where the time goes in v1:
time: 208 us; the launch traced here: 207 us
  waiting for transfers between devices  101 us (49%)
  blocking collectives  34 us (16%)
  Pallas kernels  24.2 us (12%)
  starting transfers between devices  17.6 us (8%)
  between operations  14.3 us (7%)
  other arithmetic  8.96 us (4%)
  local copies, waits for them, and re-layouts  4.04 us (2%)
  matrix products  2.7 us (1%)
    all_to_all x1, waiting for transfers between devices, local(): lax.all_to_all(remote_tot, 'kv', split_axis=0, concat_axis=0, tiled=True)  50.6 us
    all_to_all x1, waiting for transfers between devices, local(): lax.all_to_all(outgoing, 'kv', split_axis=0, concat_axis=0, tiled=True)  49.9 us
    all_to_all x1, blocking collectives, sum_at_owner(): lax.all_to_all(pieces, axis, split_axis=0, concat_axis=0, tiled=True)  34 us
    pallas_call x1, Pallas kernels, attention(): pl.pallas_call(functools.partial(attention_kernel, n_dev=n_dev, n_blocks=...  24.2 us
    all_to_all x1, starting transfers between devices, local(): lax.all_to_all(outgoing, 'kv', split_axis=0, concat_axis=0, tiled=True)  12.2 us
    all_to_all x1, starting transfers between devices, local(): lax.all_to_all(remote_tot, 'kv', split_axis=0, concat_axis=0, tiled=True)  5.33 us
  transfers between devices with their start and end apart: 3, of which 2 were waited for; matrix products, arithmetic and copies ran while one was open for 3% of the time, Pallas kernels for 0%

profile of v1, /device:TPU:6, one launch (start us, length us, event | category | flops | bytes accessed | tf_op | source)
XLA Modules:
  0.0 207.0 jit_solution(7826241755852121766)
XLA Ops:
  7.2 0.8 select_reduce_fusion
  8.0 0.1 reduce_max.14
  8.2 0.1 reduce_max.18
  8.3 0.1 copy.19
  8.4 0.1 copy.20
  8.6 0.1 copy.21
  8.7 0.1 copy.22
  8.8 0.1 copy.23
  8.9 0.1 copy.16
  9.0 0.9 fusion.17
  9.9 2.0 select_select_fusion
  11.9 12.2 %all-to-all-start = ((bf16[64,2,64,128]{3,2,1,0:T(8,128)(2,1)}), bf16[64,2,64,128]{3,2,1,0:T(8,128)(2,1)S(1)}, u32[]{:S(2)}, u32[]{:S(2)}) async-start(bf16[64,2,64,128]{3,2,1,0:T(8,128)(2,1)} %select_select_fusion), calls=%async_computation | async-start | bytes 4194304 | tf_op jit(solution)/shard_map/all_to_all | solution.py:205
  24.2 0.9 select_bitcast_fusion
  25.1 0.1 copy.14
  25.2 0.1 reshape.95.slots
  25.2 0.1 copy.15
  25.3 0.1 reshape.96.kinds
  25.4 0.1 reshape.97
  25.5 0.1 reshape.98.lse
  25.6 49.9 %all-to-all-done.table = bf16[64,2,64,128]{3,2,1,0:T(8,128)(2,1)S(1)} async-done(((bf16[64,2,64,128]{3,2,1,0:T(8,128)(2,1)}), bf16[64,2,64,128]{3,2,1,0:T(8,128)(2,1)S(1)}, u32[]{:S(2)}, u32[]{:S(2)}) %all-to-all-start) | async-done | bytes 2097184 | tf_op jit(solution)/shard_map/all_to_all | solution.py:205
  75.5 24.2 %attention.1 = (f32[384,512]{1,0:T(8,128)}, bf16[64,2,64,128]{3,2,1,0:T(8,128)(2,1)S(1)}, f32[6,2,64,128]{3,2,1,0:T(8,128)S(1)}) custom-call(s32[192]{0:T(256)S(1)} %reshape.95.slots, s32[192]{0:T(256)S(1)} %reshape.96.kinds, bf16[64,2,64,128]{3,2,1,0:T(8,128)(2,1)S(1)} %all-to-all-done.table, bf16[384,128]{1,0:T(8,128)(2,1)S(1)} %copy-done.1, ...), custom_call_target="tpu_custom_call" | custom-call | flops 4026531840 | bytes 8388608 | tf_op jit(solution)/shard_map/attention/pallas_call | solution.py:131
  99.7 1.4 copy-done
  101.1 5.3 %all-to-all-start.1 = ((bf16[64,2,64,128]{3,2,1,0:T(8,128)(2,1)}), bf16[64,2,64,128]{3,2,1,0:T(8,128)(2,1)S(1)}, u32[]{:S(2)}, u32[]{:S(2)}) async-start(bf16[64,2,64,128]{3,2,1,0:T(8,128)(2,1)} %copy-done), calls=%async_computation.1 | async-start | bytes 4194304 | tf_op jit(solution)/shard_map/all_to_all | solution.py:210
  106.4 0.0 all-gather.2.cloned.1.call-start
  106.5 0.7 all-gather.2.cloned.1.call-update
  107.2 50.6 %all-to-all-done.1 = bf16[64,2,64,128]{3,2,1,0:T(8,128)(2,1)S(1)} async-done(((bf16[64,2,64,128]{3,2,1,0:T(8,128)(2,1)}), bf16[64,2,64,128]{3,2,1,0:T(8,128)(2,1)S(1)}, u32[]{:S(2)}, u32[]{:S(2)}) %all-to-all-start.1) | async-done | bytes 2097184 | tf_op jit(solution)/shard_map/all_to_all | solution.py:210
  157.8 3.4 %fusion.6 = (f32[2,64,128]{2,1,0:T(8,128)S(1)}, f32[2,64,128]{2,1,0:T(8,128)S(1)}, f32[2,64,128]{2,1,0:T(8,128)S(1)}, f32[2,64,128]{2,1,0:T(8,128)S(1)}, f32[2,6...) fusion(bf16[64,2,64,128]{3,2,1,0:T(8,128)(2,1)S(1)} %all-to-all-done.1, pred[64,128]{1,0:T(8,128)(4,1)S(1)} %copy.16, ...), kind=kLoop, calls=%fused_computation.13 | loop fusion | flops 13533184 | bytes 2539520 | tf_op jit(solution)/shard_map/reduce_sum | solution.py:213
  161.3 0.7 fusion.29
  162.0 2.7 %fusion = bf16[4096,128]{0,1:T(8,128)(2,1)S(1)} fusion(bf16[384,4096]{1,0:T(8,128)(2,1)} %all-gather.2.cloned.1.call-done, f32[384,128]{1,0:T(8,128)S(1)} %bitcast.74), kind=kOutput, calls=%fused_computation.7 | convolution fusion | flops 403226624 | bytes 4390912 | tf_op jit(solution)/shard_map/dot_general | solution.py:220
  164.7 0.7 copy.25
  165.4 34.0 %all_to_all.15 = bf16[64,64,128]{2,1,0:T(8,128)(2,1)S(1)} all-to-all(bf16[64,64,128]{2,1,0:T(8,128)(2,1)S(1)} %bitcast.73), channel_id=1, replica_groups=mesh['kv'=64,'tp'=4] {'kv'}, dimensions={0} | all-to-all | bytes 2097152 | tf_op jit(solution)/shard_map/all_to_all | solution.py:169
  199.4 0.8 convert_reduce_fusion
  (31 shorter events, 0.2 us)
Async XLA Ops:
  11.9 13.5 %copy-start.6 = (f32[8,384]{1,0:T(8,128)S(1)}, f32[8,384]{1,0:T(8,128)}, u32[]{:S(2)}) copy-start(f32[8,384]{1,0:T(8,128)} %param.10) | copy-start | bytes 36868
  11.9 63.6 %copy-start.1 = (bf16[384,128]{1,0:T(8,128)(2,1)S(1)}, bf16[384,128]{1,0:T(8,128)(2,1)}, u32[]{:S(2)}) copy-start(bf16[384,128]{1,0:T(8,128)(2,1)} %keys.1) | copy-start | bytes 294916
  11.9 63.6 %copy-start.2 = (bf16[384,128]{1,0:T(8,128)(2,1)S(1)}, bf16[384,128]{1,0:T(8,128)(2,1)}, u32[]{:S(2)}) copy-start(bf16[384,128]{1,0:T(8,128)(2,1)} %vals.1) | copy-start | bytes 294916
  11.9 63.6 %copy-start.3 = (bf16[384,512]{1,0:T(8,128)(2,1)S(1)}, bf16[384,512]{1,0:T(8,128)(2,1)}, u32[]{:S(2)}) copy-start(bf16[384,512]{1,0:T(8,128)(2,1)} %queries.1) | copy-start | bytes 1179652
  11.9 63.6 %copy-start.4 = (bf16[384,512]{1,0:T(8,128)(2,1)S(1)}, bf16[384,512]{1,0:T(8,128)(2,1)}, u32[]{:S(2)}) copy-start(bf16[384,512]{1,0:T(8,128)(2,1)} %out_grad.1) | copy-start | bytes 1179652
  11.9 63.6 %all-to-all-start = ((bf16[64,2,64,128]{3,2,1,0:T(8,128)(2,1)}), bf16[64,2,64,128]{3,2,1,0:T(8,128)(2,1)S(1)}, u32[]{:S(2)}, u32[]{:S(2)}) async-start(bf16[64,2,64,128]{3,2,1,0:T(8,128)(2,1)} %select_select_fusion), calls=%async_computation | async-start | bytes 4194304 | tf_op jit(solution)/shard_map/all_to_all | solution.py:205
  99.7 1.4 copy-start
  101.1 56.7 %all-to-all-start.1 = ((bf16[64,2,64,128]{3,2,1,0:T(8,128)(2,1)}), bf16[64,2,64,128]{3,2,1,0:T(8,128)(2,1)S(1)}, u32[]{:S(2)}, u32[]{:S(2)}) async-start(bf16[64,2,64,128]{3,2,1,0:T(8,128)(2,1)} %copy-done), calls=%async_computation.1 | async-start | bytes 4194304 | tf_op jit(solution)/shard_map/all_to_all | solution.py:210
  106.4 55.5 %all-gather.2.cloned.1.call-start = ((), (), s32[]{:S(2)}) async-start(), calls=%async_computation.3 | async-start | bytes 3932160 | tf_op jit(solution)/shard_map/all_gather | solution.py:218
  162.0 2.7 %copy-start.5 = (f32[6,1,64,128]{3,2,1,0:T(8,128)}, f32[6,1,64,128]{3,2,1,0:T(8,128)S(1)}, u32[]{:S(2)}) copy-start(f32[6,1,64,128]{3,2,1,0:T(8,128)S(1)} %get-tuple-element.19) | copy-start | bytes 589828
Sparse Core Ops, SparseCore 0:
  109.0 41.2 all-gather.1

commit v2 on v1

--- a/solution.py
+++ b/solution.py
@@ -10,6 +10,256 @@
 HD = 64
 BLOCK = 64
 NEG = -1e30
+
+
+N_Y = 4
+N_C = 2
+PLANE = N_Y * N_C
+MESH = pl.DeviceIdType.MESH
+
+
+def place():
+    me = lax.axis_index("kv")
+    return me // PLANE, me % PLANE
+
+
+def greet(partners):
+    barrier = pltpu.get_barrier_semaphore()
+    for who in partners:
+        pl.semaphore_signal(barrier, inc=1, device_id=who, device_id_type=MESH)
+    pl.semaphore_wait(barrier, len(partners))
+
+
+def gather_kernel(
+    sel, keys, vals, inputs, table, others,
+    u1, u2, u3, u4, w1, w2, w3, picked,
+    z_send, z_recv, y_send, y_recv, x_send, x_recv,
+    *, n_z, n_x,
+):
+    z, q = place()
+    x = lax.axis_index("tp")
+    half = inputs.shape[0] // 2
+    up_z = {"kv": (z + 1) % n_z * PLANE + q}
+    dn_z = {"kv": (z + n_z - 1) % n_z * PLANE + q}
+    right = {"tp": (x + 1) % n_x}
+    left = {"tp": (x + n_x - 1) % n_x}
+    plane = [{"kv": z * PLANE + (q + r) % PLANE} for r in range(1, PLANE)]
+    greet([up_z, dn_z, right, left] + plane)
+
+    ups = [None, u1, u2, u3, u4]
+    downs = [None, w1, w2, w3]
+    own = (keys, vals)
+
+    def source(held, step, part):
+        return own[part] if step == 0 else held[step].at[part]
+
+    def z_copy(way, step, part):
+        held, who = (ups, up_z) if way == 0 else (downs, dn_z)
+        return pltpu.make_async_remote_copy(
+            src_ref=source(held, step - 1, part),
+            dst_ref=held[step].at[part],
+            send_sem=z_send.at[way, step, part],
+            recv_sem=z_recv.at[way, step, part],
+            device_id=who,
+            device_id_type=MESH,
+        )
+
+    def sends_up(step):
+        return (z < n_z - 1) & (z - step + 1 >= 0)
+
+    def gets_up(step):
+        return z - step >= 0
+
+    def sends_down(step):
+        return (z + step - 1) % n_z < 3
+
+    def gets_down(step):
+        return (z + step) % n_z < 3
+
+    def x_copy(to_right, rel, part):
+        rows = pl.ds(part * half, half)
+        slot = rel - 1 if to_right else n_x - 1 - rel
+        src = inputs.at[rows] if rel == 1 else others.at[0 if to_right else n_x - 2, rows]
+        return pltpu.make_async_remote_copy(
+            src_ref=src,
+            dst_ref=others.at[slot, rows],
+            send_sem=x_send.at[0 if to_right else 1, rel, part],
+            recv_sem=x_recv.at[0 if to_right else 1, rel, part],
+            device_id=right if to_right else left,
+            device_id_type=MESH,
+        )
+
+    @pl.when(sends_up(1))
+    def _():
+        z_copy(0, 1, 0).start()
+        z_copy(0, 1, 1).start()
+
+    @pl.when(sends_down(1))
+    def _():
+        z_copy(1, 1, 0).start()
+        z_copy(1, 1, 1).start()
+
+    for part in range(2):
+        x_copy(True, 1, part).start()
+        x_copy(False, 1, 1 - part).start()
+
+    lane = lax.broadcasted_iota(jnp.int32, (BLOCK, 128), 1)
+
+    def y_copy(order, z_from, r):
+        to = (q + r) % PLANE
+        return pltpu.make_async_remote_copy(
+            src_ref=picked.at[order, r],
+            dst_ref=table.at[z_from * PLANE + q],
+            send_sem=y_send.at[order, r],
+            recv_sem=y_recv.at[order, q],
+            device_id={"kv": z * PLANE + to},
+            device_id_type=MESH,
+        )
+
+    def pick(order, z_from, held):
+        def chosen_rows(to, part):
+            at = (z_from * PLANE + to) * 2
+            ref = own[part] if held is None else held
+            halves = []
+            for g in range(2):
+                b = sel[at + g]
+                halves.append(ref[b] if held is None else ref[part, b])
+            return jnp.where(lane < HD, halves[0], halves[1])
+
+        def one(r, c):
+            for part in range(2):
+                picked[order, r, part] = chosen_rows((q + r) % PLANE, part)
+
+            @pl.when(r > 1)
+            def _():
+                y_copy(order, z_from, r - 1).start()
+
+            return c
+
+        lax.fori_loop(1, PLANE, one, 0)
+        for part in range(2):
+            table[z_from * PLANE + q, part] = chosen_rows(q, part)
+        y_copy(order, z_from, PLANE - 1).start()
+
+    pick(0, z, None)
+    for step in range(1, 5):
+        for part in range(2):
+            @pl.when(gets_up(step))
+            def _():
+                z_copy(0, step, part).wait_recv()
+
+            if step < 4:
+                @pl.when(sends_up(step + 1))
+                def _():
+                    z_copy(0, step + 1, part).start()
+
+                @pl.when(gets_down(step))
+                def _():
+                    z_copy(1, step, part).wait_recv()
+
+                if step < 3:
+                    @pl.when(sends_down(step + 1))
+                    def _():
+                        z_copy(1, step + 1, part).start()
+
+        @pl.when(gets_up(step))
+        def _():
+            pick(step, z - step, ups[step])
+
+        if step < 4:
+            @pl.when(gets_down(step) & (z + step >= n_z))
+            def _():
+                pick(4 + step, z + step - n_z, downs[step])
+
+        if step == 2:
+            x_copy(True, 1, 0).wait_recv()
+            x_copy(True, 2, 0).start()
+            x_copy(False, 1, 1).wait_recv()
+            x_copy(False, 2, 1).start()
+
+    def each_order(act):
+        act(0, z)
+        for step in range(1, 5):
+            @pl.when(gets_up(step))
+            def _():
+                act(step, z - step)
+
+            if step < 4:
+                @pl.when(gets_down(step) & (z + step >= n_z))
+                def _():
+                    act(4 + step, z + step - n_z)
+
+    def drain(order, z_from):
+        def one(r, c):
+            frm = (q + r) % PLANE
+            got = pltpu.make_async_remote_copy(
+                src_ref=picked.at[order, r],
+                dst_ref=table.at[z_from * PLANE + frm],
+                send_sem=y_send.at[order, r],
+                recv_sem=y_recv.at[order, frm],
+                device_id={"kv": z * PLANE + frm},
+                device_id_type=MESH,
+            )
+            got.wait_recv()
+            got.wait_send()
+            return c
+
+        lax.fori_loop(1, PLANE, one, 0)
+
+    each_order(drain)
+    for step in range(1, 5):
+        for part in range(2):
+            @pl.when(sends_up(step))
+            def _():
+                z_copy(0, step, part).wait_send()
+
+            if step < 4:
+                @pl.when(sends_down(step))
+                def _():
+                    z_copy(1, step, part).wait_send()
+    x_copy(True, 1, 1).wait_recv()
+    x_copy(False, 1, 0).wait_recv()
+    x_copy(True, 2, 0).wait_recv()
+    x_copy(False, 2, 1).wait_recv()
+    for part in range(2):
+        x_copy(True, 1, part).wait_send()
+        x_copy(False, 1, part).wait_send()
+    x_copy(True, 2, 0).wait_send()
+    x_copy(False, 2, 1).wait_send()
+
+
+def gather(sel, keys, vals, inputs):
+    n_dev = lax.axis_size("kv")
+    n_x = lax.axis_size("tp")
+    n_z = n_dev // PLANE
+    bf16 = jnp.bfloat16
+    vm = pl.BlockSpec(memory_space=pltpu.VMEM)
+    hbm = pl.BlockSpec(memory_space=pl.ANY)
+    dma = pltpu.SemaphoreType.DMA
+    held = pltpu.VMEM((2,) + keys.shape, bf16)
+    return pl.pallas_call(
+        functools.partial(gather_kernel, n_z=n_z, n_x=n_x),
+        out_shape=(
+            jax.ShapeDtypeStruct((n_dev, 2, BLOCK, 128), bf16),
+            jax.ShapeDtypeStruct((n_x - 1,) + inputs.shape, bf16),
+        ),
+        in_specs=[pl.BlockSpec(memory_space=pltpu.SMEM), vm, vm, hbm],
+        out_specs=(vm, hbm),
+        scratch_shapes=[held] * 7
+        + [
+            pltpu.VMEM((8, PLANE, 2, BLOCK, 128), bf16),
+            dma((2, 5, 2)),
+            dma((2, 5, 2)),
+            dma((8, PLANE)),
+            dma((8, PLANE)),
+            dma((2, 3, 2)),
+            dma((2, 3, 2)),
+        ],
+        compiler_params=pltpu.CompilerParams(
+            collective_id=0, has_side_effects=True, vmem_limit_bytes=32 * 1024 * 1024
+        ),
+        name="gather",
+    )(sel, keys, vals, inputs)
 
 
 def attention_kernel(
@@ -198,11 +448,16 @@
     sel = jnp.max(jnp.where(mine, rel, -1), axis=2)
     sel = jnp.where(jnp.arange(n_dev)[None] == me, -1, sel)
     sel_lane = jnp.repeat(sel.T, HD, axis=1)[:, None, None, :]
-    own = jnp.stack([key_heads.reshape(n_blocks, BLOCK, -1), values.reshape(n_blocks, BLOCK, -1)], axis=1)
-    outgoing = jnp.zeros((n_dev,) + own.shape[1:], jnp.bfloat16)
-    for b in range(n_blocks):
-        outgoing = jnp.where(sel_lane == b, own[b][None], outgoing)
-    table = lax.all_to_all(outgoing, "kv", split_axis=0, concat_axis=0, tiled=True)
+    z, q = place()
+    plane_lists = lax.dynamic_slice_in_dim(chosen, z * PLANE * n_blocks, PLANE * n_blocks, 1)
+    own_col = (jnp.arange(n_dev // PLANE) * PLANE + q) * n_blocks
+    offs = plane_lists[..., None] - own_col
+    offs = jnp.where((offs >= 0) & (offs < n_blocks), offs, 0)
+    picks = jnp.max(offs.reshape(groups, PLANE, n_blocks * n_list, -1), axis=2)
+    picks = picks.transpose(2, 1, 0).reshape(-1)
+    key_blocks = key_heads.reshape(n_blocks, BLOCK, -1)
+    value_blocks = values.reshape(n_blocks, BLOCK, -1)
+    table, others = gather(picks, key_blocks, value_blocks, inputs)
 
     query_grad, remote_tot, own_tot = attention(
         slots, kinds, table, key_heads, values, queries, out_grad, lse, n_list=n_list
@@ -215,14 +470,16 @@
     total = jnp.stack(total, axis=0)
     key_grad = total[:, 0].reshape(rows, -1)
     value_grad = total[:, 1].reshape(rows, -1)
-    whole_inputs = lax.all_gather(inputs, "tp", axis=1, tiled=True)
-    weight_grad = sum_at_owner(
-        lax.dot_general(
-            whole_inputs, key_grad.astype(jnp.bfloat16), (((0,), (0,)), ((), ())),
-            preferred_element_type=jnp.float32,
-        ).astype(jnp.bfloat16),
-        "kv",
-    )
+    x, n_x = lax.axis_index("tp"), lax.axis_size("tp")
+    key_half = key_grad.astype(jnp.bfloat16)
+    parts = jnp.zeros((n_x, inputs.shape[1], key_half.shape[1]), jnp.bfloat16)
+    for rel in range(n_x):
+        piece = inputs if rel == 0 else others[rel - 1]
+        part = lax.dot_general(
+            piece, key_half, (((0,), (0,)), ((), ())), preferred_element_type=jnp.float32
+        ).astype(jnp.bfloat16)
+        parts = lax.dynamic_update_index_in_dim(parts, part, (x + n_x - rel) % n_x, 0)
+    weight_grad = sum_at_owner(parts.reshape(-1, key_half.shape[1]), "kv")
     return (query_grad, key_grad, value_grad, weight_grad)
 
 

time: 208 us -> 177 us (0.85)
  waiting for transfers between devices: 101 us -> 47.7 us
  Pallas kernels: 24.2 us -> 59.4 us
  between operations: 14.3 us -> 0.95 us
  local copies, waits for them, and re-layouts: 4.04 us -> 14.1 us
  starting transfers between devices: 17.6 us -> 9.13 us
    all_to_all x1 -> x0, waiting for transfers between devices: 49.9 us -> none  [local(): lax.all_to_all(outgoing, 'kv', split_axis=0, concat_axis=0, tiled=True)]
    pallas_call x0 -> x1, Pallas kernels: none -> 34.6 us  [gather(): pl.pallas_call(functools.partial(gather_kernel, n_z=n_z, n_x=n_x), out_sh...]
    all_to_all x1 -> x0, starting transfers between devices: 12.2 us -> none  [local(): lax.all_to_all(outgoing, 'kv', split_axis=0, concat_axis=0, tiled=True)]
    unnamed x14 -> x20, local copies, waits for them, and re-layouts: 1.39 us -> 7.35 us
    all_to_all x1, starting transfers between devices: 5.33 us -> 9.13 us  [local(): lax.all_to_all(remote_tot, 'kv', split_axis=0, concat_axis=0, tiled=True)]
    all_to_all x1, waiting for transfers between devices: 50.6 us -> 47.7 us  [local(): lax.all_to_all(remote_tot, 'kv', split_axis=0, concat_axis=0, tiled=True)]
    eq x6, local copies, waits for them, and re-layouts: 0.57 us -> 2.96 us  [local(): sel_lane == b]
  transfers between devices with their start and end apart: 3 -> 1, of which waited for: 2 -> 1; matrix products, arithmetic and copies ran while one was open for 3% -> 2% of each run, Pallas kernels for 0% -> 0%
where the time goes in v2:
time: 177 us; the launch traced here: 174 us
  Pallas kernels  59.4 us (34%)
  waiting for transfers between devices  47.7 us (27%)
  blocking collectives  34 us (19%)
  local copies, waits for them, and re-layouts  14.1 us (8%)
  starting transfers between devices  9.13 us (5%)
  other arithmetic  6.96 us (4%)
    all_to_all x1, waiting for transfers between devices, local(): lax.all_to_all(remote_tot, 'kv', split_axis=0, concat_axis=0, tiled=True)  47.7 us
    pallas_call x1, Pallas kernels, gather(): pl.pallas_call(functools.partial(gather_kernel, n_z=n_z, n_x=n_x), out_sh...  34.6 us
    all_to_all x1, blocking collectives, sum_at_owner(): lax.all_to_all(pieces, axis, split_axis=0, concat_axis=0, tiled=True)  34 us
    pallas_call x1, Pallas kernels, attention(): pl.pallas_call(functools.partial(attention_kernel, n_dev=n_dev, n_blocks=...  24.8 us
    all_to_all x1, starting transfers between devices, local(): lax.all_to_all(remote_tot, 'kv', split_axis=0, concat_axis=0, tiled=True)  9.13 us
    unnamed x20, local copies, waits for them, and re-layouts  7.35 us
    reduce_sum x1, other arithmetic, local(): jnp.sum(jnp.where(sel_lane == b, returned, 0.0), axis=0)  4.66 us
  transfers between devices with their start and end apart: 1, of which 1 were waited for; matrix products, arithmetic and copies ran while one was open for 2% of the time, Pallas kernels for 0%

profile of v2, /device:TPU:6, one launch (start us, length us, event | category | flops | bytes accessed | tf_op | source)
XLA Modules:
  0.0 174.0 jit_solution(15111467585376461143)
XLA Ops:
  0.7 0.8 constant_dynamic-slice_fusion
  1.7 0.4 fusion.20
  2.2 0.1 reshape.116.sel
  2.4 0.9 select_bitcast_fusion
  3.6 0.8 reshape.119
  4.5 1.1 copy-done
  5.6 0.9 copy-done.2
  6.5 0.9 copy-done.4
  7.4 34.6 %gather.1 = (bf16[64,2,64,128]{3,2,1,0:T(8,128)(2,1)S(1)}, bf16[3,384,1024]{2,1,0:T(8,128)(2,1)S(1)}) custom-call(s32[128]{0:T(128)S(1)} %reshape.116.sel, bf16[6,64,128]{2,1,0:T(8,128)(2,1)S(1)} %bitcast.83, bf16[6,64,128]{2,1,0:T(8,128)(2,1)S(1)} %bitcast.84, bf16[384,1024]{1,0:T(8,128)(2,1)S(1)} %copy-done), custom_call_target="tpu_custom_call" | custom-call | tf_op jit(solution)/shard_map/gather/pallas_call | solution.py:240
  42.0 0.9 copy-done.3
  42.9 0.9 copy-done.5
  43.8 1.0 copy-done.6
  44.8 1.0 copy-done.7
  45.8 24.8 %attention.1 = (f32[384,512]{1,0:T(8,128)}, bf16[64,2,64,128]{3,2,1,0:T(8,128)(2,1)}, f32[6,2,64,128]{3,2,1,0:T(8,128)S(1)}) custom-call(s32[192]{0:T(256)S(1)} %reshape.114.slots, s32[192]{0:T(256)S(1)} %reshape.115.kinds, bf16[64,2,64,128]{3,2,1,0:T(8,128)(2,1)S(1)} %get-tuple-element.9.table, bf16[384,128]{1,0:T(8,128)(2,1)S(1)} %copy-done.3, ...), custom_call_target="tpu_custom_call" | custom-call | flops 4026531840 | bytes 8388608 | tf_op jit(solution)/shard_map/attention/pallas_call | solution.py:381
  70.6 9.1 %all-to-all-start = ((bf16[64,2,64,128]{3,2,1,0:T(8,128)(2,1)}), bf16[64,2,64,128]{3,2,1,0:T(8,128)(2,1)}, u32[]{:S(2)}, u32[]{:S(2)}) async-start(bf16[64,2,64,128]{3,2,1,0:T(8,128)(2,1)} %get-tuple-element.12), calls=%async_computation | async-start | bytes 4194304 | tf_op jit(solution)/shard_map/all_to_all | solution.py:465
  79.9 0.1 reduce_max.27
  80.4 0.7 copy.34
  81.1 0.7 copy.35
  81.8 0.7 copy.36
  82.5 0.7 copy.31
  83.2 47.7 %all-to-all-done = bf16[64,2,64,128]{3,2,1,0:T(8,128)(2,1)} async-done(((bf16[64,2,64,128]{3,2,1,0:T(8,128)(2,1)}), bf16[64,2,64,128]{3,2,1,0:T(8,128)(2,1)}, u32[]{:S(2)}, u32[]{:S(2)}) %all-to-all-start) | async-done | bytes 2097184 | tf_op jit(solution)/shard_map/all_to_all | solution.py:465
  131.0 4.7 %fusion.5 = (f32[2,64,128]{2,1,0:T(8,128)S(1)}, f32[2,64,128]{2,1,0:T(8,128)S(1)}, f32[2,64,128]{2,1,0:T(8,128)S(1)}, f32[2,64,128]{2,1,0:T(8,128)S(1)}, f32[2,6...) fusion(bf16[64,2,64,128]{3,2,1,0:T(8,128)(2,1)} %all-to-all-done, pred[64,128]{1,0:T(8,128)(4,1)} %copy.36, ...), kind=kLoop, calls=%fused_computation.11 | loop fusion | flops 13533184 | bytes 2539520 | tf_op jit(solution)/shard_map/reduce_sum | solution.py:468
  135.7 0.7 fusion.32
  136.5 0.7 copy-done.8
  137.1 0.3 fusion.6
  137.4 0.2 copy.37
  137.6 0.1 broadcast_in_dim.114
  137.8 0.5 fusion.8
  138.3 0.5 fusion.10
  138.8 0.5 fusion.12
  139.2 34.0 %all_to_all.10 = bf16[64,64,128]{2,1,0:T(8,128)(2,1)S(1)} all-to-all(bf16[64,64,128]{2,1,0:T(8,128)(2,1)S(1)} %bitcast.85), channel_id=1, replica_groups=mesh['kv'=64,'tp'=4] {'kv'}, dimensions={0} | all-to-all | bytes 2097152 | tf_op jit(solution)/shard_map/all_to_all | solution.py:419
  173.2 0.8 convert_reduce_fusion
  (44 shorter events, 1.3 us)
Async XLA Ops:
  4.5 1.1 copy-start
  5.6 0.9 copy-start.2
  6.5 0.9 copy-start.4
  42.0 0.9 copy-start.3
  42.9 0.9 copy-start.5
  43.8 1.0 copy-start.6
  44.8 1.0 copy-start.7
  70.6 9.2 %copy-start.9 = (s32[2,384,16]{1,2,0:T(8,128)S(1)}, s32[2,384,16]{1,2,0:T(8,128)}, u32[]{:S(2)}) copy-start(s32[2,384,16]{1,2,0:T(8,128)} %param.13) | copy-start | bytes 147460
  70.6 60.3 %all-to-all-start = ((bf16[64,2,64,128]{3,2,1,0:T(8,128)(2,1)}), bf16[64,2,64,128]{3,2,1,0:T(8,128)(2,1)}, u32[]{:S(2)}, u32[]{:S(2)}) async-start(bf16[64,2,64,128]{3,2,1,0:T(8,128)(2,1)} %get-tuple-element.12), calls=%async_computation | async-start | bytes 4194304 | tf_op jit(solution)/shard_map/all_to_all | solution.py:465
  83.2 53.9 %copy-start.1 = (bf16[384,1024]{1,0:T(8,128)(2,1)S(1)}, bf16[384,1024]{1,0:T(8,128)(2,1)}, u32[]{:S(2)}) copy-start(bf16[384,1024]{1,0:T(8,128)(2,1)} %inputs.1) | copy-start | bytes 2359300
  136.4 0.7 copy-start.8

commit v3 on v0

v3 whole, which is shorter than its diff:
```python
import functools

import jax
import jax.numpy as jnp
from jax import lax
from jax.experimental import pallas as pl
from jax.experimental.pallas import tpu as pltpu
from jax.sharding import PartitionSpec as P

HD = 64
BLOCK = 64
NEG = -1e30
N_Y = 4
N_C = 2
PLANE = N_Y * N_C
MESH = pl.DeviceIdType.MESH
RETURN_ORDER = (4, 5, 3, 6, 2, 7, 1, 0)
F32, BF16 = jnp.float32, jnp.bfloat16


def place():
    me = lax.axis_index("kv")
    return me // PLANE, me % PLANE


def scratch_list(rows, n_dev, n_x, n_list, feats, heads):
    n_b = rows // BLOCK
    tile = (BLOCK, 128)
    cols = heads // 2 * BLOCK
    dma = pltpu.SemaphoreType.DMA
    out = [
        ("kraw", pltpu.VMEM((n_b,) + tile, BF16)),
        ("vraw", pltpu.VMEM((n_b,) + tile, BF16)),
        ("qraw", pltpu.VMEM((rows, heads * HD), BF16)),
        ("graw", pltpu.VMEM((rows, heads * HD), BF16)),
        ("lraw", pltpu.VMEM((heads, rows), F32)),
        ("xraw", pltpu.VMEM((n_x, rows, feats), BF16)),
        ("lse", pltpu.VMEM((n_b * 2, 1, cols), F32)),
        ("bias", pltpu.VMEM((3,) + (BLOCK, cols), F32)),
        ("picked", pltpu.VMEM((2, 8, PLANE) + tile, BF16)),
        ("qd", pltpu.VMEM((2 * cols, 128), BF16)),
        ("cat", pltpu.VMEM((n_list,) + tile, BF16)),
        ("sdp", pltpu.VMEM((n_list, BLOCK, 2 * cols), F32)),
        ("pd", pltpu.VMEM((n_list, BLOCK, 2 * cols), BF16)),
        ("terms", pltpu.VMEM((n_b, n_list + 1) + tile, F32)),
        ("ret", pltpu.VMEM((2, n_dev) + tile, BF16)),
        ("own_tot", pltpu.VMEM((2, n_b) + tile, F32)),
        ("back", pltpu.VMEM((2, 8, PLANE) + tile, BF16)),
        ("acc", pltpu.VMEM((2, n_b) + tile, F32)),
        ("zs", pltpu.VMEM((2, 8, n_b) + tile, BF16)),
        ("zr_dn", pltpu.VMEM((2, 4, n_b) + tile, BF16)),
        ("zr_up", pltpu.VMEM((2, 3, n_b) + tile, BF16)),
        ("kg", pltpu.VMEM((rows, 128), BF16)),
        ("wpart", pltpu.VMEM((8, N_C, N_Y) + tile, BF16)),
        ("crecv", pltpu.VMEM((8, N_Y) + tile, BF16)),
        ("wy", pltpu.VMEM((N_Y, 8) + tile, BF16)),
        ("wy_own", pltpu.VMEM((8,) + tile, F32)),
        ("wyr", pltpu.VMEM((N_Y, 8) + tile, BF16)),
        ("wz", pltpu.VMEM((8,) + tile, BF16)),
        ("wz_own", pltpu.VMEM((8,) + tile, F32)),
        ("wzr", pltpu.VMEM((8,) + tile, BF16)),
        ("in_sem", dma((6,))),
        ("z_send", dma((2, 2, 5))),
        ("z_recv", dma((2, 2, 5))),
        ("y_send", dma((2, 8, PLANE))),
        ("y_recv", dma((2, 8, PLANE))),
        ("x_send", dma((2, 3, 2))),
        ("x_recv", dma((2, 3, 2))),
        ("b_send", dma((2, 8, PLANE))),
        ("b_recv", dma((2, 8, PLANE))),
        ("r_send", dma((2, 8))),
        ("r_recv_dn", dma((2, 4))),
        ("r_recv_up", dma((2, 3))),
        ("c_send", dma((8,))),
        ("c_recv", dma((8,))),
        ("wy_send", dma((N_Y,))),
        ("wy_recv", dma((N_Y,))),
        ("wz_send", dma((8,))),
        ("wz_recv", dma((8,))),
    ]
    for g in range(2):
        out.append((f"own{g}", pltpu.VMEM((n_b,) + tile, BF16)))
        out.append((f"tab{g}", pltpu.VMEM((n_dev + n_b,) + tile, BF16)))
        for step in range(1, 5):
            out.append((f"held{g}0{step}", pltpu.VMEM((n_b,) + tile, BF16)))
        for step in range(1, 4):
            out.append((f"held{g}1{step}", pltpu.VMEM((n_b,) + tile, BF16)))
    return out


def fused_kernel(names, n_z, n_x, n_list, *refs):
    idx, keys, vals, queries, out_grad, log_sums, inputs = refs[:7]
    query_grad, key_grad, value_grad, weight_grad = refs[7:11]
    m = dict(zip(names, refs[11:]))
    n_b = m["kraw"].shape[0]
    n_dev = n_z * PLANE
    heads = m["lraw"].shape[0]
    per_group = heads // 2
    cols = per_group * BLOCK
    at_picks = 0
    at_slots = at_picks + n_z * PLANE * 2
    at_kinds = at_slots + n_b * 2 * n_list
    at_inv = at_kinds + n_b * 2 * n_list
    z, q = place()
    y, c = q // N_C, q % N_C
    x = lax.axis_index("tp")

    barrier = pltpu.get_barrier_semaphore()
    partners = [{"kv": (z + r) % n_z * PLANE + q} for r in range(1, n_z)]
    partners += [{"kv": z * PLANE + (q + r) % PLANE} for r in range(1, PLANE)]
    right, left = {"tp": (x + 1) % n_x}, {"tp": (x + n_x - 1) % n_x}
    partners += [right, left]
    for who in partners:
        pl.semaphore_signal(barrier, inc=1, device_id=who, device_id_type=MESH)

    loads = [
        pltpu.make_async_copy(src, dst, m["in_sem"].at[i])
        for i, (src, dst) in enumerate(
            [
                (keys, m["kraw"]),
                (vals, m["vraw"]),
                (queries, m["qraw"]),
                (out_grad, m["graw"]),
                (log_sums, m["lraw"]),
                (inputs, m["xraw"].at[0]),
            ]
        )
    ]
    for copy in loads:
        copy.start()
    up_z = {"kv": (z + 1) % n_z * PLANE + q}
    dn_z = {"kv": (z + n_z - 1) % n_z * PLANE + q}
    lane = lax.broadcasted_iota(jnp.int32, (BLOCK, 128), 1)
    low = lane < HD
    loads[0].wait()
    loads[1].wait()
    for b in range(n_b):
        k = m["kraw"][b].astype(F32)
        v = m["vraw"][b].astype(F32)
        kv0 = jnp.where(low, k, pltpu.roll(v, HD, 1)).astype(BF16)
        kv1 = jnp.where(low, pltpu.roll(k, HD, 1), v).astype(BF16)
        m["own0"][b] = kv0
        m["own1"][b] = kv1
        m["tab0"][n_dev + b] = kv0
        m["tab1"][n_dev + b] = kv1
    pl.semaphore_wait(barrier, len(partners))

    def held(g, way, step):
        return m[f"own{g}"] if step == 0 else m[f"held{g}{way}{step}"]

    def z_copy(g, way, step):
        return pltpu.make_async_remote_copy(
            src_ref=held(g, way, step - 1),
            dst_ref=held(g, way, step),
            send_sem=m["z_send"].at[g, way, step],
            recv_sem=m["z_recv"].at[g, way, step],
            device_id=dn_z if way else up_z,
            device_id_type=MESH,
        )

    def sends(way, step):
        if way:
            return (z + step - 1) % n_z < 3
        return (z < n_z - 1) & (z - step + 1 >= 0)

    def gets(way, step):
        if way:
            return (z + step) % n_z < 3
        return z - step >= 0

    def steps(way):
        return 3 if way else 4

    def x_copy(to_right, rel, part):
        half = inputs.shape[0] // 2
        rows = pl.ds(part * half, half)
        slot = rel if to_right else n_x - rel
        if rel == 1:
            src = inputs.at[rows]
        else:
            src = m["xraw"].at[1 if to_right else n_x - 1, rows]
        side = 0 if to_right else 1
        return pltpu.make_async_remote_copy(
            src_ref=src,
            dst_ref=m["xraw"].at[slot, rows],
            send_sem=m["x_send"].at[side, rel, part],
            recv_sem=m["x_recv"].at[side, rel, part],
            device_id=right if to_right else left,
            device_id_type=MESH,
        )

    def y_copy(g, order, z_from, r, receiving=False):
        other = (q + r) % PLANE
        at = other if receiving else q
        return pltpu.make_async_remote_copy(
            src_ref=m["picked"].at[g, order, r],
            dst_ref=m[f"tab{g}"].at[z_from * PLANE + at],
            send_sem=m["y_send"].at[g, order, r],
            recv_sem=m["y_recv"].at[g, order, at],
            device_id={"kv": z * PLANE + other},
            device_id_type=MESH,
        )

    def pick(g, order, z_from, ref):
        def one(r, carry):
            to = (q + r) % PLANE
            m["picked"][g, order, r] = ref[idx[at_picks + (z_from * PLANE + to) * 2 + g]]

            @pl.when(r > 1)
            def _():
                y_copy(g, order, z_from, r - 1).start()

            return carry

        lax.fori_loop(1, PLANE, one, 0)
        m[f"tab{g}"][z_from * PLANE + q] = ref[idx[at_picks + (z_from * PLANE + q) * 2 + g]]
        y_copy(g, order, z_from, PLANE - 1).start()

    def each_piece(g, step, act):
        @pl.when(gets(0, step))
        def _():
            act(g, step, z - step, held(g, 0, step))

        if step < 4:
            @pl.when(gets(1, step) & (z + step >= n_z))
            def _():
                act(g, 4 + step, z + step - n_z, held(g, 1, step))

    for g in range(2):
        for way in range(2):
            @pl.when(sends(way, 1))
            def _():
                z_copy(g, way, 1).start()

    for part in range(2):
        x_copy(True, 1, part).start()
        x_copy(False, 1, 1 - part).start()
    pick(0, 0, z, m["own0"])
    pick(1, 0, z, m["own1"])

    def relay(g, step):
        for way in range(2):
            if step <= steps(way):
                @pl.when(gets(way, step))
                def _():
                    z_copy(g, way, step).wait_recv()

            if step + 1 <= steps(way):
                @pl.when(sends(way, step + 1))
                def _():
                    z_copy(g, way, step + 1).start()

    key_at = lax.broadcasted_iota(jnp.int32, (BLOCK, cols), 0)
    tok_at = lax.broadcasted_iota(jnp.int32, (BLOCK, cols), 1) % BLOCK
    m["bias"][0] = jnp.zeros((BLOCK, cols), F32)
    m["bias"][1] = jnp.where(key_at <= tok_at, 0.0, NEG)
    m["bias"][2] = jnp.full((BLOCK, cols), NEG, F32)
    for p in range(n_b):
        m["terms"][p, n_list] = jnp.zeros((BLOCK, 128), F32)
    loads[4].wait()
    for p in range(n_b):
        for g in range(2):
            row = [
                m["lraw"][g * per_group + r : g * per_group + r + 1, p * BLOCK : (p + 1) * BLOCK]
                for r in range(per_group)
            ]
            m["lse"][p * 2 + g] = jnp.concatenate(row, axis=1)

    for step in range(1, 5):
        relay(0, step)
        each_piece(0, step, pick)
        relay(1, step)
        if step > 1:
            each_piece(1, step - 1, pick)
        if step == 2:
            x_copy(True, 1, 0).wait_recv()
            x_copy(True, 2, 0).start()
            x_copy(False, 1, 1).wait_recv()
            x_copy(False, 2, 1).start()
    each_piece(1, 4, pick)

    def landed(g, order, z_from, ref):
        def one(r, carry):
            y_copy(g, order, z_from, r, receiving=True).wait_recv()
            return carry

        lax.fori_loop(1, PLANE, one, 0)

    def masked_rows(ref, row, g, factor, side):
        parts = []
        for r in range(per_group):
            col = (g * per_group + r) * HD
            part = ref[pl.ds(row, BLOCK), col // 128 * 128 : col // 128 * 128 + 128]
            part = part.astype(F32) * factor
            if r % 2 != side:
                part = pltpu.roll(part, HD, 1)
            parts.append(jnp.where(low != (side == 1), part, 0.0).astype(BF16))
        return parts

    def attention(g):
        tab = m[f"tab{g}"]
        sdp, pd, qd, cat = m["sdp"], m["pd"], m["qd"], m["cat"]

        def one_position(p, carry):
            row = pl.multiple_of(p * BLOCK, BLOCK)
            unit = (p * 2 + g) * n_list
            for r, part in enumerate(masked_rows(m["qraw"], row, g, HD ** -0.5, 0)):
                qd[r * BLOCK : (r + 1) * BLOCK, :] = part
            for r, part in enumerate(masked_rows(m["graw"], row, g, 1.0, 1)):
                qd[cols + r * BLOCK : cols + (r + 1) * BLOCK, :] = part
            for n in range(n_list):
                cat[n] = tab[idx[at_slots + unit + n]]
            keys_all = cat[...].reshape(n_list * BLOCK, 128)
            nt = (((1,), (1,)), ((), ()))
            sdp[...] = lax.dot_general(
                keys_all, qd[...], nt, preferred_element_type=F32
            ).reshape(n_list, BLOCK, 2 * cols)
            lse_row = m["lse"][p * 2 + g]

            def probs(n, acc):
                kind = m["bias"][idx[at_kinds + unit + n]]
                pr = jnp.exp((sdp[n, :, :cols] - lse_row) + kind)
                sdp[n, :, :cols] = pr
                pd[n, :, cols:] = pr.astype(BF16)
                pr = pr * sdp[n, :, cols:]
                return acc + pr.reshape(BLOCK // 8, 8, cols).sum(axis=0)

            acc = lax.fori_loop(0, n_list, probs, jnp.zeros((8, cols), F32), unroll=4)
            delta = acc.sum(axis=0, keepdims=True)

            def grads(n, carry):
                ds = sdp[n, :, :cols] * (sdp[n, :, cols:] - delta)
                pd[n, :, :cols] = ds.astype(BF16)
                return carry

            lax.fori_loop(0, n_list, grads, 0, unroll=4)
            nn = (((1,), (0,)), ((), ()))
            both = pd[...].reshape(n_list * BLOCK, 2 * cols)
            m["terms"][p, :n_list] = lax.dot_general(
                both, qd[...], nn, preferred_element_type=F32
            ).reshape(n_list, BLOCK, 128)
            dq_t = lax.dot_general(
                keys_all, both[:, :cols], (((0,), (0,)), ((), ())), preferred_element_type=F32
            )
            dq = dq_t.T * (HD ** -0.5)
            for pair in range(per_group // 2):
                even = dq[(2 * pair) * BLOCK : (2 * pair + 1) * BLOCK]
                odd = dq[(2 * pair + 1) * BLOCK : (2 * pair + 2) * BLOCK]
                col = g * per_group * HD + pair * 128
                query_grad[pl.ds(row, BLOCK), col : col + 128] = jnp.where(
                    low, even, pltpu.roll(odd, HD, 1)
                )
            return carry

        lax.fori_loop(0, n_b, one_position, 0)

    def summed_terms(g, j):
        at = at_inv + (g * (n_dev + n_b) + j) * n_b
        total = m["terms"][0, idx[at]]
        for p in range(1, n_b):
            total = total + m["terms"][p, idx[at + p]]
        return total

    def b_copy(g, d, r, receiving=False):
        other = (q + r) % PLANE
        at = other if receiving else q
        return pltpu.make_async_remote_copy(
            src_ref=m["ret"].at[g, (z - d) * PLANE + other],
            dst_ref=m["back"].at[g, d, at],
            send_sem=m["b_send"].at[g, d, r],
            recv_sem=m["b_recv"].at[g, d, at],
            device_id={"kv": z * PLANE + other},
            device_id_type=MESH,
        )

    def give_back(g):
        for d in RETURN_ORDER:
            @pl.when(z - d >= 0)
            def _():
                def one(r, carry):
                    j = (z - d) * PLANE + (q + r) % PLANE
                    m["ret"][g, j] = summed_terms(g, j).astype(BF16)

                    @pl.when(r > 1)
                    def _():
                        b_copy(g, d, r - 1).start()

                    return carry

                lax.fori_loop(1, PLANE, one, 0)
                j = (z - d) * PLANE + q
                m["ret"][g, j] = summed_terms(g, j).astype(BF16)
                b_copy(g, d, PLANE - 1).start()

        def own(b, carry):
            m["own_tot"][g, b] = summed_terms(g, n_dev + b)
            return carry

        lax.fori_loop(0, n_b, own, 0)

    def accumulate(g, d):
        def arrived(r, carry):
            b_copy(g, d, r, receiving=True).wait_recv()
            return carry

        lax.fori_loop(1, PLANE, arrived, 0)

        def rows_of(part, carry):
            rows = pl.ds(pl.multiple_of(part * 32, 32), 32)
            accs = [jnp.zeros((32, 128), F32) for _ in range(n_b)]
            for r in range(PLANE):
                frm = (q + r) % PLANE
                if r == 0:
                    val = m["ret"][g, (z - d) * PLANE + q, rows, :]
                else:
                    val = m["back"][g, d, frm, rows, :]
                val = val.astype(F32)
                block = idx[at_picks + ((z - d) * PLANE + frm) * 2 + g]
                for b in range(n_b):
                    accs[b] = accs[b] + jnp.where(block == b, val, 0.0)
            for b in range(n_b):
                m["acc"][g, b, rows, :] = accs[b]
            return carry

        lax.fori_loop(0, 2, rows_of, 0)

    def add_to_acc(g, ref):
        for b in range(n_b):
            m["acc"][g, b] += ref[b].astype(F32)

    def dn_copy(g, d):
        return pltpu.make_async_remote_copy(
            src_ref=m["zs"].at[g, d],
            dst_ref=m["zr_dn"].at[g, d - 1],
            send_sem=m["r_send"].at[g, d],
            recv_sem=m["r_recv_dn"].at[g, d - 1],
            device_id=dn_z,
            device_id_type=MESH,
        )

    def up_copy(g, e, passing=False):
        return pltpu.make_async_remote_copy(
            src_ref=m["zr_up"].at[g, e] if passing else m["zs"].at[g, n_z - e],
            dst_ref=m["zr_up"].at[g, e - 1],
            send_sem=m["r_send"].at[g, n_z - e],
            recv_sem=m["r_recv_up"].at[g, e - 1],
            device_id=up_z,
            device_id_type=MESH,
        )

    def dn_arrival(g, d):
        dn_copy(g, d + 1).wait_recv()
        add_to_acc(g, m["zr_dn"].at[g, d])

    def up_arrival(g, e):
        up_copy(g, e + 1).wait_recv()
        add_to_acc(g, m["zr_up"].at[g, e])

    def store_out(g, d):
        for b in range(n_b):
            m["zs"][g, d, b] = m["acc"][g, b].astype(BF16)

    def collect(g):
        for d in RETURN_ORDER:
            e = n_z - d
            if d > 4:
                @pl.when(z - d >= 0)
                def _():
                    accumulate(g, d)
                    if e < 3:
                        up_arrival(g, e)
                    store_out(g, d)
                    up_copy(g, e).start()

                if e < 3:
                    @pl.when(z < 3 - e)
                    def _():
                        up_copy(g, e + 1).wait_recv()
                        up_copy(g, e, passing=True).start()
            else:
                @pl.when(z - d >= 0)
                def _():
                    accumulate(g, d)
                    if d < 4:
                        @pl.when(z < n_z - 1)
                        def _():
                            dn_arrival(g, d)
                    if d > 0:
                        store_out(g, d)
                        dn_copy(g, d).start()
        @pl.when(z < 3)
        def _():
            up_arrival(g, 0)

    def wait_fetch(g):
        landed(g, 0, z, None)
        for step in range(1, 5):
            each_piece(g, step, landed)

    loads[2].wait()
    loads[3].wait()
    wait_fetch(0)
    attention(0)
    give_back(0)
    wait_fetch(1)
    attention(1)
    give_back(1)
    collect(0)
    collect(1)

    for b in range(n_b):
        rows = slice(b * BLOCK, (b + 1) * BLOCK)
        t0 = m["acc"][0, b] + m["own_tot"][0, b]
        t1 = m["acc"][1, b] + m["own_tot"][1, b]
        kg = jnp.where(low, t0, pltpu.roll(t1, HD, 1))
        key_grad[rows, :] = kg
        value_grad[rows, :] = jnp.where(low, pltpu.roll(t0, HD, 1), t1)
        m["kg"][rows, :] = kg.astype(BF16)

    def c_copy(i):
        return pltpu.make_async_remote_copy(
            src_ref=m["wpart"].at[i, 1 - c],
            dst_ref=m["crecv"].at[i],
            send_sem=m["c_send"].at[i],
            recv_sem=m["c_recv"].at[i],
            device_id={"kv": z * PLANE + y * N_C + (1 - c)},
            device_id_type=MESH,
        )

    x_copy(True, 1, 1).wait_recv()
    x_copy(False, 1, 0).wait_recv()
    x_copy(True, 2, 0).wait_recv()
    x_copy(False, 2, 1).wait_recv()
    loads[5].wait()
    kg_t = m["kg"][...].T
    feats = inputs.shape[1]
    half = feats // 2
    for i in range(2 * n_x):
        rel, h = i // 2, i % 2
        w_t = lax.dot_general(
            kg_t, m["xraw"][rel, :, h * half : (h + 1) * half], (((1,), (0,)), ((), ())),
            preferred_element_type=F32,
        )
        w = w_t.T.astype(BF16)
        for yy in range(N_Y):
            for cc in range(N_C):
                first = (yy * N_C + cc) * BLOCK
                m["wpart"][i, cc, yy] = w[first : first + BLOCK]
        if i:
            c_copy(i - 1).start()
    c_copy(2 * n_x - 1).start()

    def wy_copy(r):
        to = (y + r) % N_Y
        return pltpu.make_async_remote_copy(
            src_ref=m["wy"].at[r],
            dst_ref=m["wyr"].at[r],
            send_sem=m["wy_send"].at[r],
            recv_sem=m["wy_recv"].at[r],
            device_id={"kv": z * PLANE + to * N_C + c},
            device_id_type=MESH,
        )

    for i in range(2 * n_x):
        c_copy(i).wait_recv()
        for r in range(N_Y):
            yy = (y + r) % N_Y
            both = m["wpart"][i, c, yy].astype(F32) + m["crecv"][i, yy].astype(F32)
            if r:
                m["wy"][r, i] = both.astype(BF16)
            else:
                m["wy_own"][i] = both
    for r in (2, 1, 3):
        wy_copy(r).start()

    def z_of(i):
        return 2 * ((x + n_x - i // 2) % n_x) + i % 2

    def wz_copy(i):
        return pltpu.make_async_remote_copy(
            src_ref=m["wz"].at[i],
            dst_ref=m["wzr"].at[z],
            send_sem=m["wz_send"].at[i],
            recv_sem=m["wz_recv"].at[z],
            device_id={"kv": z_of(i) * PLANE + q},
            device_id_type=MESH,
        )

    for r in (1, 3, 2):
        wy_copy(r).wait_recv()
    for i in range(2 * n_x):
        total = m["wy_own"][i]
        for r in range(1, N_Y):
            total = total + m["wyr"][r, i].astype(F32)
        m["wz_own"][i] = total
        m["wz"][i] = total.astype(BF16)
    for i in range(2 * n_x):
        @pl.when(z_of(i) != z)
        def _():
            wz_copy(i).start()
    mine = 2 * ((x + n_x - z // 2) % n_x) + z % 2
    total = m["wz_own"][mine]
    for r in range(1, n_z):
        frm = (z + r) % n_z
        pltpu.make_async_remote_copy(
            src_ref=m["wz"].at[0],
            dst_ref=m["wzr"].at[frm],
            send_sem=m["wz_send"].at[0],
            recv_sem=m["wz_recv"].at[frm],
            device_id={"kv": frm * PLANE + q},
            device_id_type=MESH,
        ).wait_recv()
        total = total + m["wzr"][frm].astype(F32)
    weight_grad[...] = total

    def sent(g, order, z_from, ref):
        def one(r, carry):
            y_copy(g, order, z_from, r).wait_send()
            return carry

        lax.fori_loop(1, PLANE, one, 0)

    for g in range(2):
        for way in range(2):
            for step in range(1, steps(way) + 1):
                @pl.when(sends(way, step))
                def _():
                    z_copy(g, way, step).wait_send()

        sent(g, 0, z, None)
        for step in range(1, 5):
            each_piece(g, step, sent)
        for d in range(8):
            @pl.when(z - d >= 0)
            def _():
                def one(r, carry):
                    b_copy(g, d, r).wait_send()
                    return carry

                lax.fori_loop(1, PLANE, one, 0)

            if 0 < d < 5:
                @pl.when(z - d >= 0)
                def _():
                    dn_copy(g, d).wait_send()
            elif d:
                e = n_z - d
                @pl.when((z - d >= 0) | (z < 3 - e))
                def _():
                    up_copy(g, e).wait_send()

    for part in range(2):
        x_copy(True, 1, part).wait_send()
        x_copy(False, 1, part).wait_send()
    x_copy(True, 2, 0).wait_send()
    x_copy(False, 2, 1).wait_send()
    for i in range(2 * n_x):
        c_copy(i).wait_send()
        @pl.when(z_of(i) != z)
        def _():
            wz_copy(i).wait_send()
    for r in range(1, N_Y):
        wy_copy(r).wait_send()


def index_table(chosen, n_b, n_dev):
    groups, _, n_list = chosen.shape
    me = lax.axis_index("kv")
    z, q = place()
    plane = lax.dynamic_slice_in_dim(chosen, z * PLANE * n_b, PLANE * n_b, 1)
    column = (jnp.arange(n_dev // PLANE) * PLANE + q) * n_b
    offs = plane[..., None] - column
    offs = jnp.where((offs >= 0) & (offs < n_b), offs, 0)
    picks = jnp.max(offs.reshape(groups, PLANE, n_b * n_list, -1), axis=2)
    picks = picks.transpose(2, 1, 0).reshape(-1)
    lists = lax.dynamic_slice_in_dim(chosen, me * n_b, n_b, 1)
    owner = lists // n_b
    slot = jnp.where(owner == me, n_dev + lists % n_b, jnp.maximum(owner, 0))
    at_diag = lists == me * n_b + jnp.arange(n_b)[None, :, None]
    kind = jnp.where(lists < 0, 2, at_diag.astype(jnp.int32))
    listed = (slot[..., None] == jnp.arange(n_dev + n_b)) & (lists >= 0)[..., None]
    inverse = jnp.min(
        jnp.where(listed, jnp.arange(n_list)[:, None], n_list), axis=2
    )
    slots = slot.transpose(1, 0, 2).reshape(-1)
    kinds = kind.transpose(1, 0, 2).reshape(-1)
    inverse = inverse.transpose(0, 2, 1).reshape(-1)
    return jnp.concatenate([picks, slots, kinds, inverse]).astype(jnp.int32)


def local(queries, key_heads, values, log_sums, out_grad, inputs, chosen):
    n_dev = lax.axis_size("kv")
    n_x = lax.axis_size("tp")
    rows, feats = inputs.shape
    n_b = rows // BLOCK
    heads = log_sums.shape[0]
    n_list = chosen.shape[2]
    idx = index_table(chosen, n_b, n_dev)
    scratch = scratch_list(rows, n_dev, n_x, n_list, feats, heads)
    hbm = pl.BlockSpec(memory_space=pl.ANY)
    vm = pl.BlockSpec(memory_space=pltpu.VMEM)
    return pl.pallas_call(
        functools.partial(
            fused_kernel, [name for name, _ in scratch], n_dev // PLANE, n_x, n_list
        ),
        out_shape=(
            jax.ShapeDtypeStruct(queries.shape, F32),
            jax.ShapeDtypeStruct(key_heads.shape, F32),
            jax.ShapeDtypeStruct(values.shape, F32),
            jax.ShapeDtypeStruct((feats * n_x // n_dev, 128), F32),
        ),
        in_specs=[pl.BlockSpec(memory_space=pltpu.SMEM)] + [hbm] * 6,
        out_specs=(vm, vm, vm, vm),
        scratch_shapes=[kind for _, kind in scratch],
        compiler_params=pltpu.CompilerParams(
            collective_id=0, has_side_effects=True, vmem_limit_bytes=60 * 1024 * 1024
        ),
        name="fused",
    )(
        idx,
        key_heads.reshape(n_b, BLOCK, -1),
        values.reshape(n_b, BLOCK, -1),
        queries,
        out_grad,
        log_sums,
        inputs,
    )


def solution(mesh):
    placed = (
        P("kv", "tp"),
        P("kv", "tp"),
        P("kv", "tp"),
        P("tp", "kv"),
        P("kv", "tp"),
        P("kv", "tp"),
        P("tp", None, None),
    )
    return jax.shard_map(
        local,
        mesh=mesh,
        in_specs=placed,
        out_specs=(P("kv", "tp"), P("kv", "tp"), P("kv", "tp"), P("kv", "tp")),
        check_vma=False,
    )
```

time: 312 us -> 122 us (0.39)
  waiting for transfers between devices: 121 us -> 0 us
  Pallas kernels: 0 us -> 112 us
  local copies, waits for them, and re-layouts: 63.2 us -> 7.01 us
  other arithmetic: 45 us -> 0.66 us
  starting transfers between devices: 22.4 us -> 0 us
  matrix products: 21.8 us -> 0 us
  loops' own time: 20.4 us -> 0 us
  between operations: 14.2 us -> 0.73 us
    all_to_all x3 -> x0, waiting for transfers between devices: 121 us -> none  [the longest x1 49.6 us: local(): lax.all_to_all(outgoing, 'kv', split_axis=0, concat_axis=0, tiled=True)]
    pallas_call x0 -> x1, Pallas kernels: none -> 112 us  [local(): pl.pallas_call(functools.partial(fused_kernel, [name for name, _ in scrat...]
    scatter-add x6 -> x0, other arithmetic: 37.4 us -> none  [one_block(): totals = totals.at[slot_index, :, group_col, :].add(contribs)]
    all_to_all x3 -> x0, starting transfers between devices: 22.3 us -> none  [the longest x1 12.1 us: local(): lax.all_to_all(outgoing, 'kv', split_axis=0, concat_axis=0, tiled=True)]
    dot_general x33 -> x0, matrix products: 21.8 us -> none  [the longest x6 5.24 us: one_block(): jnp.einsum('igrd,gkd->grik', query_part, key_part, preferred_element_type...]
    another operation x1 -> x0, loops' own time: 20.4 us -> none  [local(): lax.scan(one_block, start_totals, jnp.arange(blocks_here, dtype=jnp.int32))]
    dynamic_slice x19 -> x3, local copies, waits for them, and re-layouts: 14.2 us -> 0.24 us  [the longest x2 0.16 us: index_table(): plane = lax.dynamic_slice_in_dim(chosen, z * PLANE * n_b, PLANE * n_b, 1)]
    gather x6 -> x0, local copies, waits for them, and re-layouts: 13.9 us -> none  [one_block(): key_table[slot_index, :, group_col, :]]
  transfers between devices with their start and end apart: 4 -> 0, of which waited for: 3 -> 0; matrix products, arithmetic and copies ran while one was open for 38% -> 0% of each run, Pallas kernels for 0% -> 0%
where the time goes in v3:
time: 122 us; the launch traced here: 121 us
  Pallas kernels  112 us (92%)
  local copies, waits for them, and re-layouts  7.01 us (6%)
    pallas_call x1, Pallas kernels, local(): pl.pallas_call(functools.partial(fused_kernel, [name for name, _ in scrat...  112 us
    unnamed x13, local copies, waits for them, and re-layouts  5.31 us

profile of v3, /device:TPU:6, one launch (start us, length us, event | category | flops | bytes accessed | tf_op | source)
XLA Modules:
  0.0 120.9 jit_solution(5225416172313623326)
XLA Ops:
  0.6 0.0 copy-start
  0.7 0.7 copy-done
  1.4 0.1 constant_dynamic-slice_fusion
  1.5 0.1 copy.31
  1.6 0.1 select_bitcast_fusion
  1.7 0.1 reshape.45
  1.8 0.1 reshape.44
  1.9 0.1 select_reduce_fusion
  2.0 0.1 constant_dynamic-slice_fusion.1
  2.1 0.1 copy.25
  2.2 0.1 sub.27
  2.3 0.4 fusion.1
  2.7 0.1 copy.26
  2.8 0.1 reshape.43
  3.0 0.1 copy.30
  3.1 0.1 reshape.46
  3.2 0.7 concatenate.3.refs_0_
  3.9 112.5 %fused.1 = (f32[384,512]{1,0:T(8,128)}, f32[384,128]{1,0:T(8,128)}, f32[384,128]{1,0:T(8,128)}, f32[64,128]{1,0:T(8,128)}) custom-call(s32[1352]{0:T(1024)} %concatenate.3.refs_0_, bf16[6,64,128]{2,1,0:T(8,128)(2,1)} %bitcast.7, bf16[6,64,128]{2,1,0:T(8,128)(2,1)} %bitcast.8, bf16[384,512]{1,0:T(8,128)(2,1)} %refs_3_.1, bf16[384,512]{1,0:T(8,128)(2,1)} %refs_4_.1, ...), custom_call_target="tpu_custom_call" | custom-call | tf_op jit(solution)/shard_map/fused/pallas_call | solution.py:702
  116.4 0.0 copy-start.2
  116.4 2.1 %copy.36 = f32[384,512]{1,0:T(8,128)} copy(f32[384,512]{1,0:T(8,128)} %get-tuple-element.10) | data formatting | bytes 1572864
  118.5 0.0 copy-done.2
  118.5 0.0 copy-start.1
  118.5 0.7 copy.37
  119.2 0.3 copy-done.1
  119.5 0.0 copy-start.3
  119.5 0.7 copy.38
  120.2 0.1 copy-done.3
  120.3 0.6 copy.39
  (5 shorter events, 0.0 us)
Async XLA Ops:
  0.6 0.8 copy-start
  116.4 2.1 %copy-start.2 = (f32[384,128]{1,0:T(8,128)S(1)}, f32[384,128]{1,0:T(8,128)}, u32[]{:S(2)}) copy-start(f32[384,128]{1,0:T(8,128)} %get-tuple-element.11) | copy-start | bytes 589828
  118.5 1.0 copy-start.1
  119.5 0.8 copy-start.3

commit v4 on v3

v4 whole, which is shorter than its diff:
```python
import functools

import jax
import jax.numpy as jnp
from jax import lax
from jax.experimental import pallas as pl
from jax.experimental.pallas import tpu as pltpu
from jax.sharding import PartitionSpec as P

HD = 64
BLOCK = 64
NEG = -1e30
LOG2E = 1.4426950408889634
CHUNK = 4
N_Y = 4
N_C = 2
PLANE = N_Y * N_C
MESH = pl.DeviceIdType.MESH
RETURN_ORDER = (4, 5, 3, 6, 2, 7, 1, 0)
F32, BF16 = jnp.float32, jnp.bfloat16


def place():
    me = lax.axis_index("kv")
    return me // PLANE, me % PLANE


def scratch_list(rows, n_dev, n_x, n_list, feats, heads):
    n_b = rows // BLOCK
    tile = (BLOCK, 128)
    cols = heads // 2 * BLOCK
    dma = pltpu.SemaphoreType.DMA
    out = [
        ("kraw", pltpu.VMEM((n_b,) + tile, BF16)),
        ("vraw", pltpu.VMEM((n_b,) + tile, BF16)),
        ("qraw", pltpu.VMEM((rows, heads * HD), BF16)),
        ("graw", pltpu.VMEM((rows, heads * HD), BF16)),
        ("lraw", pltpu.VMEM((heads, rows), F32)),
        ("xraw", pltpu.VMEM((n_x, rows, feats), BF16)),
        ("lse", pltpu.VMEM((n_b * 2, 1, cols), F32)),
        ("bias", pltpu.VMEM((3,) + (BLOCK, cols), F32)),
        ("shift", pltpu.VMEM((3,) + (BLOCK, cols), F32)),
        ("qg", pltpu.VMEM((rows, heads * HD), F32)),
        ("kgo", pltpu.VMEM((rows, 128), F32)),
        ("vgo", pltpu.VMEM((rows, 128), F32)),
        ("wgo", pltpu.VMEM(tile, F32)),
        ("picked", pltpu.VMEM((2, 8, PLANE) + tile, BF16)),
        ("qd", pltpu.VMEM((2 * cols, 128), BF16)),
        ("cat", pltpu.VMEM((n_list,) + tile, BF16)),
        ("sdp", pltpu.VMEM((n_list, BLOCK, 2 * cols), F32)),
        ("pd", pltpu.VMEM((n_list, BLOCK, 2 * cols), BF16)),
        ("terms", pltpu.VMEM((n_b, n_list + 1) + tile, F32)),
        ("ret", pltpu.VMEM((2, n_dev) + tile, BF16)),
        ("own_tot", pltpu.VMEM((2, n_b) + tile, F32)),
        ("back", pltpu.VMEM((2, 8, PLANE) + tile, BF16)),
        ("acc", pltpu.VMEM((2, n_b) + tile, F32)),
        ("zs", pltpu.VMEM((2, 8, 2, n_b, BLOCK // 2, 128), BF16)),
        ("zr_dn", pltpu.VMEM((2, 4, 2, n_b, BLOCK // 2, 128), BF16)),
        ("zr_up", pltpu.VMEM((2, 3, 2, n_b, BLOCK // 2, 128), BF16)),
        ("kg", pltpu.VMEM((rows, 128), BF16)),
        ("wpart", pltpu.VMEM((8, N_C, N_Y) + tile, BF16)),
        ("crecv", pltpu.VMEM((8, N_Y) + tile, BF16)),
        ("wy", pltpu.VMEM((2, N_Y, 4) + tile, BF16)),
        ("wy_own", pltpu.VMEM((8,) + tile, F32)),
        ("wyr", pltpu.VMEM((2, N_Y, 4) + tile, BF16)),
        ("wz", pltpu.VMEM((8,) + tile, BF16)),
        ("wz_own", pltpu.VMEM((8,) + tile, F32)),
        ("wzr", pltpu.VMEM((8,) + tile, BF16)),
        ("in_sem", dma((6,))),
        ("out_sem", dma((4,))),
        ("z_send", dma((2, 2, 5, 2))),
        ("z_recv", dma((2, 2, 5, 2))),
        ("y_send", dma((2, 8))),
        ("y_recv", dma((2, 8))),
        ("x_send", dma((2, 3, 2))),
        ("x_recv", dma((2, 3, 2))),
        ("b_send", dma((2, 8))),
        ("b_recv", dma((2, 8))),
        ("r_send", dma((2, 8, 2))),
        ("r_recv_dn", dma((2, 4, 2))),
        ("r_recv_up", dma((2, 3, 2))),
        ("c_send", dma((8,))),
        ("c_recv", dma((8,))),
        ("wy_send", dma((2, N_Y))),
        ("wy_recv", dma((2, N_Y))),
        ("wz_send", dma((8,))),
        ("wz_recv", dma((8,))),
    ]
    for g in range(2):
        out.append((f"own{g}", pltpu.VMEM((n_b,) + tile, BF16)))
        out.append((f"tab{g}", pltpu.VMEM((n_dev + n_b,) + tile, BF16)))
        for step in range(1, 5):
            out.append((f"held{g}0{step}", pltpu.VMEM((n_b,) + tile, BF16)))
        for step in range(1, 4):
            out.append((f"held{g}1{step}", pltpu.VMEM((n_b,) + tile, BF16)))
    return out


def fused_kernel(names, n_z, n_x, n_list, *refs):
    idx, keys, vals, queries, out_grad, log_sums, inputs = refs[:7]
    query_grad, key_grad, value_grad, weight_grad = refs[7:11]
    m = dict(zip(names, refs[11:]))
    n_b = m["kraw"].shape[0]
    n_dev = n_z * PLANE
    heads = m["lraw"].shape[0]
    per_group = heads // 2
    cols = per_group * BLOCK
    at_picks = 0
    at_slots = at_picks + n_z * PLANE * 2
    at_kinds = at_slots + n_b * 2 * n_list
    at_inv = at_kinds + n_b * 2 * n_list
    z, q = place()
    y, c = q // N_C, q % N_C
    x = lax.axis_index("tp")

    barrier = pltpu.get_barrier_semaphore()
    partners = [{"kv": (z + r) % n_z * PLANE + q} for r in range(1, n_z)]
    partners += [{"kv": z * PLANE + (q + r) % PLANE} for r in range(1, PLANE)]
    right, left = {"tp": (x + 1) % n_x}, {"tp": (x + n_x - 1) % n_x}
    partners += [right, left]
    for who in partners:
        pl.semaphore_signal(barrier, inc=1, device_id=who, device_id_type=MESH)

    loads = [
        pltpu.make_async_copy(src, dst, m["in_sem"].at[i])
        for i, (src, dst) in enumerate(
            [
                (keys, m["kraw"]),
                (vals, m["vraw"]),
                (queries, m["qraw"]),
                (out_grad, m["graw"]),
                (log_sums, m["lraw"]),
                (inputs, m["xraw"].at[0]),
            ]
        )
    ]
    for copy in loads:
        copy.start()
    up_z = {"kv": (z + 1) % n_z * PLANE + q}
    dn_z = {"kv": (z + n_z - 1) % n_z * PLANE + q}
    lane = lax.broadcasted_iota(jnp.int32, (BLOCK, 128), 1)
    low = lane < HD
    loads[0].wait()
    loads[1].wait()
    for b in range(n_b):
        k = m["kraw"][b].astype(F32)
        v = m["vraw"][b].astype(F32)
        kv0 = jnp.where(low, k, pltpu.roll(v, HD, 1)).astype(BF16)
        kv1 = jnp.where(low, pltpu.roll(k, HD, 1), v).astype(BF16)
        m["own0"][b] = kv0
        m["own1"][b] = kv1
        m["tab0"][n_dev + b] = kv0
        m["tab1"][n_dev + b] = kv1
    pl.semaphore_wait(barrier, len(partners))

    def held(g, way, step):
        return m[f"own{g}"] if step == 0 else m[f"held{g}{way}{step}"]

    def z_copy(g, way, step, part):
        blocks = pl.ds(part * (n_b // 2), n_b // 2)
        return pltpu.make_async_remote_copy(
            src_ref=held(g, way, step - 1).at[blocks],
            dst_ref=held(g, way, step).at[blocks],
            send_sem=m["z_send"].at[g, way, step, part],
            recv_sem=m["z_recv"].at[g, way, step, part],
            device_id=dn_z if way else up_z,
            device_id_type=MESH,
        )

    def sends(way, step):
        if way:
            return (z + step - 1) % n_z < 3
        return (z < n_z - 1) & (z - step + 1 >= 0)

    def gets(way, step):
        if way:
            return (z + step) % n_z < 3
        return z - step >= 0

    def steps(way):
        return 3 if way else 4

    def x_copy(to_right, rel, part):
        half = inputs.shape[0] // 2
        rows = pl.ds(part * half, half)
        slot = rel if to_right else n_x - rel
        if rel == 1:
            src = inputs.at[rows]
        else:
            src = m["xraw"].at[1 if to_right else n_x - 1, rows]
        side = 0 if to_right else 1
        return pltpu.make_async_remote_copy(
            src_ref=src,
            dst_ref=m["xraw"].at[slot, rows],
            send_sem=m["x_send"].at[side, rel, part],
            recv_sem=m["x_recv"].at[side, rel, part],
            device_id=right if to_right else left,
            device_id_type=MESH,
        )

    def y_copy(g, order, z_from, r):
        to = (q + r) % PLANE
        return pltpu.make_async_remote_copy(
            src_ref=m["picked"].at[g, order, r],
            dst_ref=m[f"tab{g}"].at[z_from * PLANE + q],
            send_sem=m["y_send"].at[g, order],
            recv_sem=m["y_recv"].at[g, order],
            device_id={"kv": z * PLANE + to},
            device_id_type=MESH,
        )

    others = pl.ds(1, PLANE - 1)

    def wait_group(ref, sem):
        pltpu.make_async_copy(ref, ref, sem).wait()

    def pick(g, order, z_from, ref):
        def one(r, carry):
            to = (q + r) % PLANE
            m["picked"][g, order, r] = ref[idx[at_picks + (z_from * PLANE + to) * 2 + g]]

            @pl.when(r > 1)
            def _():
                y_copy(g, order, z_from, r - 1).start()

            return carry

        lax.fori_loop(1, PLANE, one, 0)
        m[f"tab{g}"][z_from * PLANE + q] = ref[idx[at_picks + (z_from * PLANE + q) * 2 + g]]
        y_copy(g, order, z_from, PLANE - 1).start()

    def each_piece(g, step, act):
        @pl.when(gets(0, step))
        def _():
            act(g, step, z - step, held(g, 0, step))

        if step < 4:
            @pl.when(gets(1, step) & (z + step >= n_z))
            def _():
                act(g, 4 + step, z + step - n_z, held(g, 1, step))

    def set_out(g):
        for part in range(2):
            for way in range(2):
                @pl.when(sends(way, 1))
                def _():
                    z_copy(g, way, 1, part).start()

    set_out(0)
    for part in range(2):
        x_copy(True, 1, part).start()
        x_copy(False, 1, 1 - part).start()
    pick(0, 0, z, m["own0"])
    pick(1, 0, z, m["own1"])

    def relay(g, step):
        for part in range(2):
            for way in range(2):
                if step <= steps(way):
                    @pl.when(gets(way, step))
                    def _():
                        z_copy(g, way, step, part).wait_recv()

                if step + 1 <= steps(way):
                    @pl.when(sends(way, step + 1))
                    def _():
                        z_copy(g, way, step + 1, part).start()

    key_at = lax.broadcasted_iota(jnp.int32, (BLOCK, cols), 0)
    tok_at = lax.broadcasted_iota(jnp.int32, (BLOCK, cols), 1) % BLOCK
    m["bias"][0] = jnp.zeros((BLOCK, cols), F32)
    m["bias"][1] = jnp.where(key_at <= tok_at, 0.0, NEG)
    m["bias"][2] = jnp.full((BLOCK, cols), NEG, F32)
    for p in range(n_b):
        m["terms"][p, n_list] = jnp.zeros((BLOCK, 128), F32)
    loads[4].wait()
    for p in range(n_b):
        for g in range(2):
            row = [
                m["lraw"][g * per_group + r : g * per_group + r + 1, p * BLOCK : (p + 1) * BLOCK]
                for r in range(per_group)
            ]
            m["lse"][p * 2 + g] = jnp.concatenate(row, axis=1)

    for step in range(1, 5):
        relay(0, step)
        if step == 3:
            set_out(1)
        each_piece(0, step, pick)

    def relay_and_pick(g, step):
        relay(g, step)
        each_piece(g, step, pick)

    def relay_x():
        x_copy(True, 1, 0).wait_recv()
        x_copy(True, 2, 0).start()
        x_copy(False, 1, 1).wait_recv()
        x_copy(False, 2, 1).start()

    def landed(g, order, z_from, ref):
        wait_group(m["picked"].at[g, order, others], m["y_recv"].at[g, order])

    def masked_rows(ref, row, g, factor, side):
        parts = []
        for r in range(per_group):
            col = (g * per_group + r) * HD
            part = ref[pl.ds(row, BLOCK), col // 128 * 128 : col // 128 * 128 + 128]
            part = part.astype(F32) * factor
            if r % 2 != side:
                part = pltpu.roll(part, HD, 1)
            parts.append(jnp.where(low != (side == 1), part, 0.0).astype(BF16))
        return parts

    def attention(g, between):
        tab = m[f"tab{g}"]
        sdp, pd, qd, cat, shift = m["sdp"], m["pd"], m["qd"], m["cat"], m["shift"]
        chunks = [slice(n, n + CHUNK) for n in range(0, n_list, CHUNK)]
        nt = (((1,), (1,)), ((), ()))
        nn = (((1,), (0,)), ((), ()))

        def one_position(p, carry):
            row = pl.multiple_of(p * BLOCK, BLOCK)
            unit = (p * 2 + g) * n_list
            for r, part in enumerate(masked_rows(m["qraw"], row, g, HD ** -0.5, 0)):
                qd[r * BLOCK : (r + 1) * BLOCK, :] = part
            for r, part in enumerate(masked_rows(m["graw"], row, g, 1.0, 1)):
                qd[cols + r * BLOCK : cols + (r + 1) * BLOCK, :] = part
            for n in range(n_list):
                cat[n] = tab[idx[at_slots + unit + n]]
            for kind in range(3):
                shift[kind] = m["bias"][kind] - m["lse"][p * 2 + g] * LOG2E

            def products(ch):
                sdp[ch] = lax.dot_general(
                    cat[ch].reshape(CHUNK * BLOCK, 128), qd[...], nt, preferred_element_type=F32
                ).reshape(CHUNK, BLOCK, 2 * cols)

            acc = jnp.zeros((8, cols), F32)
            products(chunks[0])
            for i, ch in enumerate(chunks):
                if i + 1 < len(chunks):
                    products(chunks[i + 1])
                for n in range(ch.start, ch.stop):
                    pr = jnp.exp2(sdp[n, :, :cols] * LOG2E + shift[idx[at_kinds + unit + n]])
                    sdp[n, :, :cols] = pr
                    pd[n, :, cols:] = pr.astype(BF16)
                    pr = pr * sdp[n, :, cols:]
                    acc = acc + pr.reshape(BLOCK // 8, 8, cols).sum(axis=0)
            delta = acc.sum(axis=0, keepdims=True)
            for ch in chunks:
                for n in range(ch.start, ch.stop):
                    ds = sdp[n, :, :cols] * (sdp[n, :, cols:] - delta)
                    pd[n, :, :cols] = ds.astype(BF16)
                m["terms"][p, ch] = lax.dot_general(
                    pd[ch].reshape(CHUNK * BLOCK, 2 * cols), qd[...], nn, preferred_element_type=F32
                ).reshape(CHUNK, BLOCK, 128)
            dq_t = lax.dot_general(
                cat[...].reshape(n_list * BLOCK, 128),
                pd[:, :, :cols].reshape(n_list * BLOCK, cols),
                (((0,), (0,)), ((), ())),
                preferred_element_type=F32,
            )
            dq = dq_t.T * (HD ** -0.5)
            for pair in range(per_group // 2):
                even = dq[(2 * pair) * BLOCK : (2 * pair + 1) * BLOCK]
                odd = dq[(2 * pair + 1) * BLOCK : (2 * pair + 2) * BLOCK]
                col = g * per_group * HD + pair * 128
                m["qg"][pl.ds(row, BLOCK), col : col + 128] = jnp.where(
                    low, even, pltpu.roll(odd, HD, 1)
                )
            for at, act in between.items():
                @pl.when(p == at)
                def _():
                    act()

            return carry

        lax.fori_loop(0, n_b, one_position, 0)

    def summed_terms(g, j):
        at = at_inv + (g * (n_dev + n_b) + j) * n_b
        total = m["terms"][0, idx[at]]
        for p in range(1, n_b):
            total = total + m["terms"][p, idx[at + p]]
        return total

    def b_copy(g, d, r):
        to = (q + r) % PLANE
        return pltpu.make_async_remote_copy(
            src_ref=m["ret"].at[g, (z - d) * PLANE + to],
            dst_ref=m["back"].at[g, d, q],
            send_sem=m["b_send"].at[g, d],
            recv_sem=m["b_recv"].at[g, d],
            device_id={"kv": z * PLANE + to},
            device_id_type=MESH,
        )

    def give_back(g):
        for d in RETURN_ORDER:
            @pl.when(z - d >= 0)
            def _():
                def one(r, carry):
                    j = (z - d) * PLANE + (q + r) % PLANE
                    m["ret"][g, j] = summed_terms(g, j).astype(BF16)

                    @pl.when(r > 1)
                    def _():
                        b_copy(g, d, r - 1).start()

                    return carry

                lax.fori_loop(1, PLANE, one, 0)
                j = (z - d) * PLANE + q
                m["ret"][g, j] = summed_terms(g, j).astype(BF16)
                b_copy(g, d, PLANE - 1).start()

        def own(b, carry):
            m["own_tot"][g, b] = summed_terms(g, n_dev + b)
            return carry

        lax.fori_loop(0, n_b, own, 0)

    def accumulate(g, d, part):
        rows = slice(part * 32, part * 32 + 32)
        accs = [jnp.zeros((32, 128), F32) for _ in range(n_b)]
        for r in range(PLANE):
            frm = (q + r) % PLANE
            if r == 0:
                val = m["ret"][g, (z - d) * PLANE + q, rows, :]
            else:
                val = m["back"][g, d, frm, rows, :]
            val = val.astype(F32)
            block = idx[at_picks + ((z - d) * PLANE + frm) * 2 + g]
            for b in range(n_b):
                accs[b] = accs[b] + jnp.where(block == b, val, 0.0)
        for b in range(n_b):
            m["acc"][g, b, rows, :] = accs[b]

    def dn_copy(g, d, part):
        return pltpu.make_async_remote_copy(
            src_ref=m["zs"].at[g, d, part],
            dst_ref=m["zr_dn"].at[g, d - 1, part],
            send_sem=m["r_send"].at[g, d, part],
            recv_sem=m["r_recv_dn"].at[g, d - 1, part],
            device_id=dn_z,
            device_id_type=MESH,
        )

    def up_copy(g, e, part, passing=False):
        return pltpu.make_async_remote_copy(
            src_ref=m["zr_up"].at[g, e, part] if passing else m["zs"].at[g, n_z - e, part],
            dst_ref=m["zr_up"].at[g, e - 1, part],
            send_sem=m["r_send"].at[g, n_z - e, part],
            recv_sem=m["r_recv_up"].at[g, e - 1, part],
            device_id=up_z,
            device_id_type=MESH,
        )

    def add_arrival(g, copy, ref, part):
        copy.wait_recv()
        rows = slice(part * 32, part * 32 + 32)
        for b in range(n_b):
            m["acc"][g, b, rows, :] += ref[b].astype(F32)

    def dn_arrival(g, d, part):
        add_arrival(g, dn_copy(g, d + 1, part), m["zr_dn"].at[g, d, part], part)

    def up_arrival(g, e, part):
        add_arrival(g, up_copy(g, e + 1, part), m["zr_up"].at[g, e, part], part)

    def store_out(g, d, part):
        rows = slice(part * 32, part * 32 + 32)
        for b in range(n_b):
            m["zs"][g, d, part, b] = m["acc"][g, b, rows, :].astype(BF16)

    def collect(g, d):
        e = n_z - d

        @pl.when(z - d >= 0)
        def _():
            wait_group(m["back"].at[g, d, others], m["b_recv"].at[g, d])
            for part in range(2):
                accumulate(g, d, part)
                if d > 4:
                    if e < 3:
                        up_arrival(g, e, part)
                    store_out(g, d, part)
                    up_copy(g, e, part).start()
                else:
                    if d < 4:
                        @pl.when(z < n_z - 1)
                        def _():
                            dn_arrival(g, d, part)
                    if d > 0:
                        store_out(g, d, part)
                        dn_copy(g, d, part).start()

        if d > 4 and e < 3:
            @pl.when(z < 3 - e)
            def _():
                for part in range(2):
                    up_copy(g, e + 1, part).wait_recv()
                    up_copy(g, e, part, passing=True).start()

        if d == 0:
            @pl.when(z < 3)
            def _():
                for part in range(2):
                    up_arrival(g, 0, part)

    def wait_fetch(g):
        landed(g, 0, z, None)
        for step in range(1, 5):
            each_piece(g, step, landed)

    relay_and_pick(1, 1)
    relay_and_pick(1, 2)
    loads[2].wait()
    loads[3].wait()
    wait_fetch(0)
    attention(
        0,
        {
            0: functools.partial(relay_and_pick, 1, 3),
            1: functools.partial(relay_and_pick, 1, 4),
            2: relay_x,
        },
    )
    give_back(0)
    wait_fetch(1)
    attention(1, {i: functools.partial(collect, 0, RETURN_ORDER[i]) for i in range(6)})
    give_back(1)
    out_q = pltpu.make_async_copy(m["qg"], query_grad, m["out_sem"].at[0])
    out_q.start()
    collect(0, 1)
    collect(1, 4)
    collect(1, 5)
    collect(0, 0)
    for d in RETURN_ORDER[2:]:
        collect(1, d)

    for b in range(n_b):
        rows = slice(b * BLOCK, (b + 1) * BLOCK)
        t0 = m["acc"][0, b] + m["own_tot"][0, b]
        t1 = m["acc"][1, b] + m["own_tot"][1, b]
        kg = jnp.where(low, t0, pltpu.roll(t1, HD, 1))
        m["kgo"][rows, :] = kg
        m["vgo"][rows, :] = jnp.where(low, pltpu.roll(t0, HD, 1), t1)
        m["kg"][rows, :] = kg.astype(BF16)

    def c_copy(i):
        return pltpu.make_async_remote_copy(
            src_ref=m["wpart"].at[i, 1 - c],
            dst_ref=m["crecv"].at[i],
            send_sem=m["c_send"].at[i],
            recv_sem=m["c_recv"].at[i],
            device_id={"kv": z * PLANE + y * N_C + (1 - c)},
            device_id_type=MESH,
        )

    x_copy(True, 1, 1).wait_recv()
    x_copy(False, 1, 0).wait_recv()
    x_copy(True, 2, 0).wait_recv()
    x_copy(False, 2, 1).wait_recv()
    loads[5].wait()
    kg_t = m["kg"][...].T
    half = inputs.shape[1] // 2
    n_i = 2 * n_x

    def wy_copy(part, r):
        to = (y + r) % N_Y
        return pltpu.make_async_remote_copy(
            src_ref=m["wy"].at[part, r],
            dst_ref=m["wyr"].at[part, r],
            send_sem=m["wy_send"].at[part, r],
            recv_sem=m["wy_recv"].at[part, r],
            device_id={"kv": z * PLANE + to * N_C + c},
            device_id_type=MESH,
        )

    def own_terms(i):
        rel, h = i // 2, i % 2
        w_t = lax.dot_general(
            kg_t, m["xraw"][rel, :, h * half : (h + 1) * half], (((1,), (0,)), ((), ())),
            preferred_element_type=F32,
        )
        w = w_t.T.astype(BF16)
        for yy in range(N_Y):
            for cc in range(N_C):
                first = (yy * N_C + cc) * BLOCK
                m["wpart"][i, cc, yy] = w[first : first + BLOCK]

    def core_sum(i):
        c_copy(i).wait_recv()
        for r in range(N_Y):
            yy = (y + r) % N_Y
            both = m["wpart"][i, c, yy].astype(F32) + m["crecv"][i, yy].astype(F32)
            if r:
                m["wy"][i // 4, r, i % 4] = both.astype(BF16)
            else:
                m["wy_own"][i] = both

    out_k = pltpu.make_async_copy(m["kgo"], key_grad, m["out_sem"].at[1])
    out_v = pltpu.make_async_copy(m["vgo"], value_grad, m["out_sem"].at[2])
    for i in range(n_i + 4):
        if i < n_i:
            own_terms(i)
        if 0 < i <= n_i:
            c_copy(i - 1).start()
        if i >= 4:
            core_sum(i - 4)
        if i == n_i - 1:
            for r in (2, 1, 3):
                wy_copy(0, r).start()
    for r in (2, 1, 3):
        wy_copy(1, r).start()
    out_k.start()
    out_v.start()

    def z_of(i):
        return 2 * ((x + n_x - i // 2) % n_x) + i % 2

    def wz_copy(i):
        return pltpu.make_async_remote_copy(
            src_ref=m["wz"].at[i],
            dst_ref=m["wzr"].at[z],
            send_sem=m["wz_send"].at[i],
            recv_sem=m["wz_recv"].at[z],
            device_id={"kv": z_of(i) * PLANE + q},
            device_id_type=MESH,
        )

    def sent(g, order, z_from, ref):
        wait_group(m["picked"].at[g, order, others], m["y_send"].at[g, order])

    for g in range(2):
        for way in range(2):
            for step in range(1, steps(way) + 1):
                @pl.when(sends(way, step))
                def _():
                    for part in range(2):
                        z_copy(g, way, step, part).wait_send()

        sent(g, 0, z, None)
        for step in range(1, 5):
            each_piece(g, step, sent)
        for d in range(8):
            @pl.when(z - d >= 0)
            def _():
                wait_group(m["back"].at[g, d, others], m["b_send"].at[g, d])

            for part in range(2):
                if 0 < d < 5:
                    @pl.when(z - d >= 0)
                    def _():
                        dn_copy(g, d, part).wait_send()
                elif d:
                    e = n_z - d
                    @pl.when((z - d >= 0) | (z < 3 - e))
                    def _():
                        up_copy(g, e, part).wait_send()

    for part in range(2):
        x_copy(True, 1, part).wait_send()
        x_copy(False, 1, part).wait_send()
    x_copy(True, 2, 0).wait_send()
    x_copy(False, 2, 1).wait_send()
    for i in range(n_i):
        c_copy(i).wait_send()
    out_q.wait()

    for part in range(2):
        for r in (1, 3, 2):
            wy_copy(part, r).wait_recv()
        for i in range(part * 4, part * 4 + 4):
            total = m["wy_own"][i]
            for r in range(1, N_Y):
                total = total + m["wyr"][part, r, i % 4].astype(F32)
            m["wz_own"][i] = total
            m["wz"][i] = total.astype(BF16)
        for i in range(part * 4, part * 4 + 4):
            @pl.when(z_of(i) != z)
            def _():
                wz_copy(i).start()
    for part in range(2):
        for r in range(1, N_Y):
            wy_copy(part, r).wait_send()
    out_k.wait()
    out_v.wait()
    mine = 2 * ((x + n_x - z // 2) % n_x) + z % 2
    total = m["wz_own"][mine]
    for r in range(1, n_z):
        frm = (z + r) % n_z
        pltpu.make_async_remote_copy(
            src_ref=m["wz"].at[0],
            dst_ref=m["wzr"].at[frm],
            send_sem=m["wz_send"].at[0],
            recv_sem=m["wz_recv"].at[frm],
            device_id={"kv": frm * PLANE + q},
            device_id_type=MESH,
        ).wait_recv()
        total = total + m["wzr"][frm].astype(F32)
    m["wgo"][...] = total
    for i in range(n_i):
        @pl.when(z_of(i) != z)
        def _():
            wz_copy(i).wait_send()
    out_w = pltpu.make_async_copy(m["wgo"], weight_grad, m["out_sem"].at[3])
    out_w.start()
    out_w.wait()


def index_table(chosen, n_b, n_dev):
    groups, _, n_list = chosen.shape
    me = lax.axis_index("kv")
    z, q = place()
    plane = lax.dynamic_slice_in_dim(chosen, z * PLANE * n_b, PLANE * n_b, 1)
    column = (jnp.arange(n_dev // PLANE) * PLANE + q) * n_b
    offs = plane[..., None] - column
    offs = jnp.where((offs >= 0) & (offs < n_b), offs, 0)
    picks = jnp.max(offs.reshape(groups, PLANE, n_b * n_list, -1), axis=2)
    picks = picks.transpose(2, 1, 0).reshape(-1)
    lists = lax.dynamic_slice_in_dim(chosen, me * n_b, n_b, 1)
    owner = lists // n_b
    slot = jnp.where(owner == me, n_dev + lists % n_b, jnp.maximum(owner, 0))
    at_diag = lists == me * n_b + jnp.arange(n_b)[None, :, None]
    kind = jnp.where(lists < 0, 2, at_diag.astype(jnp.int32))
    listed = (slot[..., None] == jnp.arange(n_dev + n_b)) & (lists >= 0)[..., None]
    inverse = jnp.min(
        jnp.where(listed, jnp.arange(n_list)[:, None], n_list), axis=2
    )
    slots = slot.transpose(1, 0, 2).reshape(-1)
    kinds = kind.transpose(1, 0, 2).reshape(-1)
    inverse = inverse.transpose(0, 2, 1).reshape(-1)
    return jnp.concatenate([picks, slots, kinds, inverse]).astype(jnp.int32)


def local(queries, key_heads, values, log_sums, out_grad, inputs, chosen):
    n_dev = lax.axis_size("kv")
    n_x = lax.axis_size("tp")
    rows, feats = inputs.shape
    n_b = rows // BLOCK
    heads = log_sums.shape[0]
    n_list = chosen.shape[2]
    idx = index_table(chosen, n_b, n_dev)
    scratch = scratch_list(rows, n_dev, n_x, n_list, feats, heads)
    hbm = pl.BlockSpec(memory_space=pl.ANY)
    return pl.pallas_call(
        functools.partial(
            fused_kernel, [name for name, _ in scratch], n_dev // PLANE, n_x, n_list
        ),
        out_shape=(
            jax.ShapeDtypeStruct(queries.shape, F32),
            jax.ShapeDtypeStruct(key_heads.shape, F32),
            jax.ShapeDtypeStruct(values.shape, F32),
            jax.ShapeDtypeStruct((feats * n_x // n_dev, 128), F32),
        ),
        in_specs=[pl.BlockSpec(memory_space=pltpu.SMEM)] + [hbm] * 6,
        out_specs=(hbm,) * 4,
        scratch_shapes=[kind for _, kind in scratch],
        compiler_params=pltpu.CompilerParams(
            collective_id=0, has_side_effects=True, vmem_limit_bytes=60 * 1024 * 1024
        ),
        name="fused",
    )(
        idx,
        key_heads.reshape(n_b, BLOCK, -1),
        values.reshape(n_b, BLOCK, -1),
        queries,
        out_grad,
        log_sums,
        inputs,
    )


def solution(mesh):
    placed = (
        P("kv", "tp"),
        P("kv", "tp"),
        P("kv", "tp"),
        P("tp", "kv"),
        P("kv", "tp"),
        P("kv", "tp"),
        P("tp", None, None),
    )
    return jax.shard_map(
        local,
        mesh=mesh,
        in_specs=placed,
        out_specs=(P("kv", "tp"), P("kv", "tp"), P("kv", "tp"), P("kv", "tp")),
        check_vma=False,
    )
```

time: 122 us -> 103 us (0.84)
  Pallas kernels: 112 us -> 94.1 us
    pallas_call x1, Pallas kernels: 112 us -> 94.1 us  [local(): pl.pallas_call(functools.partial(fused_kernel, [name for name, _ in scrat...]
where the time goes in v4:
time: 103 us; the launch traced here: 102 us
  Pallas kernels  94.1 us (91%)
  local copies, waits for them, and re-layouts  7.01 us (7%)
    pallas_call x1, Pallas kernels, local(): pl.pallas_call(functools.partial(fused_kernel, [name for name, _ in scrat...  94.1 us
    unnamed x13, local copies, waits for them, and re-layouts  5.31 us

profile of v4, /device:TPU:6, one launch (start us, length us, event | category | flops | bytes accessed | tf_op | source)
XLA Modules:
  0.0 102.5 jit_solution(1880956070647449272)
XLA Ops:
  0.6 0.0 copy-start
  0.7 0.7 copy-done
  1.4 0.1 constant_dynamic-slice_fusion
  1.5 0.1 copy.31
  1.6 0.1 select_bitcast_fusion
  1.7 0.1 reshape.45
  1.8 0.1 reshape.44
  1.9 0.1 select_reduce_fusion
  2.0 0.1 constant_dynamic-slice_fusion.1
  2.1 0.1 copy.25
  2.2 0.1 sub.27
  2.3 0.4 fusion.1
  2.7 0.1 copy.26
  2.8 0.1 reshape.43
  3.0 0.1 copy.30
  3.1 0.1 reshape.46
  3.2 0.7 concatenate.3.refs_0_
  3.9 94.1 %fused.1 = (f32[384,512]{1,0:T(8,128)}, f32[384,128]{1,0:T(8,128)}, f32[384,128]{1,0:T(8,128)}, f32[64,128]{1,0:T(8,128)}) custom-call(s32[1352]{0:T(1024)} %concatenate.3.refs_0_, bf16[6,64,128]{2,1,0:T(8,128)(2,1)} %bitcast.7, bf16[6,64,128]{2,1,0:T(8,128)(2,1)} %bitcast.8, bf16[384,512]{1,0:T(8,128)(2,1)} %refs_3_.1, bf16[384,512]{1,0:T(8,128)(2,1)} %refs_4_.1, ...), custom_call_target="tpu_custom_call" | custom-call | tf_op jit(solution)/shard_map/fused/pallas_call | solution.py:749
  98.0 0.0 copy-start.2
  98.0 2.1 %copy.36 = f32[384,512]{1,0:T(8,128)} copy(f32[384,512]{1,0:T(8,128)} %get-tuple-element.10) | data formatting | bytes 1572864
  100.1 0.0 copy-done.2
  100.1 0.0 copy-start.1
  100.1 0.7 copy.37
  100.8 0.3 copy-done.1
  101.1 0.0 copy-start.3
  101.1 0.7 copy.38
  101.8 0.1 copy-done.3
  101.9 0.6 copy.39
  (5 shorter events, 0.0 us)
Async XLA Ops:
  0.6 0.8 copy-start
  98.0 2.1 %copy-start.2 = (f32[384,128]{1,0:T(8,128)S(1)}, f32[384,128]{1,0:T(8,128)}, u32[]{:S(2)}) copy-start(f32[384,128]{1,0:T(8,128)} %get-tuple-element.11) | copy-start | bytes 589828
  100.1 1.0 copy-start.1
  101.1 0.8 copy-start.3

commit v5 on v4

--- a/solution.py
+++ b/solution.py
@@ -41,9 +41,6 @@
         ("bias", pltpu.VMEM((3,) + (BLOCK, cols), F32)),
         ("shift", pltpu.VMEM((3,) + (BLOCK, cols), F32)),
         ("qg", pltpu.VMEM((rows, heads * HD), F32)),
-        ("kgo", pltpu.VMEM((rows, 128), F32)),
-        ("vgo", pltpu.VMEM((rows, 128), F32)),
-        ("wgo", pltpu.VMEM(tile, F32)),
         ("picked", pltpu.VMEM((2, 8, PLANE) + tile, BF16)),
         ("qd", pltpu.VMEM((2 * cols, 128), BF16)),
         ("cat", pltpu.VMEM((n_list,) + tile, BF16)),
@@ -60,14 +57,14 @@
         ("kg", pltpu.VMEM((rows, 128), BF16)),
         ("wpart", pltpu.VMEM((8, N_C, N_Y) + tile, BF16)),
         ("crecv", pltpu.VMEM((8, N_Y) + tile, BF16)),
-        ("wy", pltpu.VMEM((2, N_Y, 4) + tile, BF16)),
+        ("wy", pltpu.VMEM((4, N_Y, 2) + tile, BF16)),
         ("wy_own", pltpu.VMEM((8,) + tile, F32)),
-        ("wyr", pltpu.VMEM((2, N_Y, 4) + tile, BF16)),
+        ("wyr", pltpu.VMEM((4, N_Y, 2) + tile, BF16)),
         ("wz", pltpu.VMEM((8,) + tile, BF16)),
         ("wz_own", pltpu.VMEM((8,) + tile, F32)),
         ("wzr", pltpu.VMEM((8,) + tile, BF16)),
         ("in_sem", dma((6,))),
-        ("out_sem", dma((4,))),
+        ("out_sem", dma((1,))),
         ("z_send", dma((2, 2, 5, 2))),
         ("z_recv", dma((2, 2, 5, 2))),
         ("y_send", dma((2, 8))),
@@ -81,8 +78,8 @@
         ("r_recv_up", dma((2, 3, 2))),
         ("c_send", dma((8,))),
         ("c_recv", dma((8,))),
-        ("wy_send", dma((2, N_Y))),
-        ("wy_recv", dma((2, N_Y))),
+        ("wy_send", dma((4, N_Y))),
+        ("wy_recv", dma((4, N_Y))),
         ("wz_send", dma((8,))),
         ("wz_recv", dma((8,))),
     ]
@@ -97,18 +94,15 @@
 
 
 def fused_kernel(names, n_z, n_x, n_list, *refs):
-    idx, keys, vals, queries, out_grad, log_sums, inputs = refs[:7]
-    query_grad, key_grad, value_grad, weight_grad = refs[7:11]
-    m = dict(zip(names, refs[11:]))
+    idx_picks, idx_slots, idx_kinds, idx_inv = refs[:4]
+    keys, vals, queries, out_grad, log_sums, inputs = refs[4:10]
+    query_grad, key_grad, value_grad, weight_grad = refs[10:14]
+    m = dict(zip(names, refs[14:]))
     n_b = m["kraw"].shape[0]
     n_dev = n_z * PLANE
     heads = m["lraw"].shape[0]
     per_group = heads // 2
     cols = per_group * BLOCK
-    at_picks = 0
-    at_slots = at_picks + n_z * PLANE * 2
-    at_kinds = at_slots + n_b * 2 * n_list
-    at_inv = at_kinds + n_b * 2 * n_list
     z, q = place()
     y, c = q // N_C, q % N_C
     x = lax.axis_index("tp")
@@ -217,7 +211,7 @@
     def pick(g, order, z_from, ref):
         def one(r, carry):
             to = (q + r) % PLANE
-            m["picked"][g, order, r] = ref[idx[at_picks + (z_from * PLANE + to) * 2 + g]]
+            m["picked"][g, order, r] = ref[idx_picks[(z_from * PLANE + to) * 2 + g]]
 
             @pl.when(r > 1)
             def _():
@@ -226,7 +220,7 @@
             return carry
 
         lax.fori_loop(1, PLANE, one, 0)
-        m[f"tab{g}"][z_from * PLANE + q] = ref[idx[at_picks + (z_from * PLANE + q) * 2 + g]]
+        m[f"tab{g}"][z_from * PLANE + q] = ref[idx_picks[(z_from * PLANE + q) * 2 + g]]
         y_copy(g, order, z_from, PLANE - 1).start()
 
     def each_piece(g, step, act):
@@ -327,25 +321,22 @@
             for r, part in enumerate(masked_rows(m["graw"], row, g, 1.0, 1)):
                 qd[cols + r * BLOCK : cols + (r + 1) * BLOCK, :] = part
             for n in range(n_list):
-                cat[n] = tab[idx[at_slots + unit + n]]
+                cat[n] = tab[idx_slots[unit + n]]
             for kind in range(3):
                 shift[kind] = m["bias"][kind] - m["lse"][p * 2 + g] * LOG2E
 
-            def products(ch):
-                sdp[ch] = lax.dot_general(
+            acc = jnp.zeros((8, cols), F32)
+            for ch in chunks:
+                both = lax.dot_general(
                     cat[ch].reshape(CHUNK * BLOCK, 128), qd[...], nt, preferred_element_type=F32
                 ).reshape(CHUNK, BLOCK, 2 * cols)
-
-            acc = jnp.zeros((8, cols), F32)
-            products(chunks[0])
-            for i, ch in enumerate(chunks):
-                if i + 1 < len(chunks):
-                    products(chunks[i + 1])
                 for n in range(ch.start, ch.stop):
-                    pr = jnp.exp2(sdp[n, :, :cols] * LOG2E + shift[idx[at_kinds + unit + n]])
+                    prod = both[n - ch.start]
+                    pr = jnp.exp2(prod[:, :cols] * LOG2E + shift[idx_kinds[unit + n]])
                     sdp[n, :, :cols] = pr
+                    sdp[n, :, cols:] = prod[:, cols:]
                     pd[n, :, cols:] = pr.astype(BF16)
-                    pr = pr * sdp[n, :, cols:]
+                    pr = pr * prod[:, cols:]
                     acc = acc + pr.reshape(BLOCK // 8, 8, cols).sum(axis=0)
             delta = acc.sum(axis=0, keepdims=True)
             for ch in chunks:
@@ -361,7 +352,7 @@
                 (((0,), (0,)), ((), ())),
                 preferred_element_type=F32,
             )
-            dq = dq_t.T * (HD ** -0.5)
+            dq = dq_t.T
             for pair in range(per_group // 2):
                 even = dq[(2 * pair) * BLOCK : (2 * pair + 1) * BLOCK]
                 odd = dq[(2 * pair + 1) * BLOCK : (2 * pair + 2) * BLOCK]
@@ -379,10 +370,10 @@
         lax.fori_loop(0, n_b, one_position, 0)
 
     def summed_terms(g, j):
-        at = at_inv + (g * (n_dev + n_b) + j) * n_b
-        total = m["terms"][0, idx[at]]
+        at = (g * (n_dev + n_b) + j) * n_b
+        total = m["terms"][0, idx_inv[at]]
         for p in range(1, n_b):
-            total = total + m["terms"][p, idx[at + p]]
+            total = total + m["terms"][p, idx_inv[at + p]]
         return total
 
     def b_copy(g, d, r):
@@ -400,20 +391,11 @@
         for d in RETURN_ORDER:
             @pl.when(z - d >= 0)
             def _():
-                def one(r, carry):
+                for r in list(range(1, PLANE)) + [0]:
                     j = (z - d) * PLANE + (q + r) % PLANE
                     m["ret"][g, j] = summed_terms(g, j).astype(BF16)
-
-                    @pl.when(r > 1)
-                    def _():
-                        b_copy(g, d, r - 1).start()
-
-                    return carry
-
-                lax.fori_loop(1, PLANE, one, 0)
-                j = (z - d) * PLANE + q
-                m["ret"][g, j] = summed_terms(g, j).astype(BF16)
-                b_copy(g, d, PLANE - 1).start()
+                for r in range(1, PLANE):
+                    b_copy(g, d, r).start()
 
         def own(b, carry):
             m["own_tot"][g, b] = summed_terms(g, n_dev + b)
@@ -431,7 +413,7 @@
             else:
                 val = m["back"][g, d, frm, rows, :]
             val = val.astype(F32)
-            block = idx[at_picks + ((z - d) * PLANE + frm) * 2 + g]
+            block = idx_picks[((z - d) * PLANE + frm) * 2 + g]
             for b in range(n_b):
                 accs[b] = accs[b] + jnp.where(block == b, val, 0.0)
         for b in range(n_b):
@@ -515,29 +497,32 @@
             each_piece(g, step, landed)
 
     relay_and_pick(1, 1)
-    relay_and_pick(1, 2)
     loads[2].wait()
     loads[3].wait()
     wait_fetch(0)
     attention(
         0,
         {
-            0: functools.partial(relay_and_pick, 1, 3),
-            1: functools.partial(relay_and_pick, 1, 4),
-            2: relay_x,
+            0: functools.partial(relay_and_pick, 1, 2),
+            2: functools.partial(relay_and_pick, 1, 3),
+            3: functools.partial(relay_and_pick, 1, 4),
+            4: relay_x,
         },
     )
     give_back(0)
     wait_fetch(1)
-    attention(1, {i: functools.partial(collect, 0, RETURN_ORDER[i]) for i in range(6)})
+    attention(1, {2 + i: functools.partial(collect, 0, RETURN_ORDER[i]) for i in range(4)})
     give_back(1)
     out_q = pltpu.make_async_copy(m["qg"], query_grad, m["out_sem"].at[0])
     out_q.start()
+    collect(0, 2)
+    collect(0, 7)
+    collect(1, 4)
     collect(0, 1)
-    collect(1, 4)
     collect(1, 5)
+    collect(1, 3)
     collect(0, 0)
-    for d in RETURN_ORDER[2:]:
+    for d in RETURN_ORDER[3:]:
         collect(1, d)
 
     for b in range(n_b):
@@ -545,8 +530,8 @@
         t0 = m["acc"][0, b] + m["own_tot"][0, b]
         t1 = m["acc"][1, b] + m["own_tot"][1, b]
         kg = jnp.where(low, t0, pltpu.roll(t1, HD, 1))
-        m["kgo"][rows, :] = kg
-        m["vgo"][rows, :] = jnp.where(low, pltpu.roll(t0, HD, 1), t1)
+        key_grad[rows, :] = kg
+        value_grad[rows, :] = jnp.where(low, pltpu.roll(t0, HD, 1), t1)
         m["kg"][rows, :] = kg.astype(BF16)
 
     def c_copy(i):
@@ -597,26 +582,21 @@
             yy = (y + r) % N_Y
             both = m["wpart"][i, c, yy].astype(F32) + m["crecv"][i, yy].astype(F32)
             if r:
-                m["wy"][i // 4, r, i % 4] = both.astype(BF16)
+                m["wy"][i // 2, r, i % 2] = both.astype(BF16)
             else:
                 m["wy_own"][i] = both
 
-    out_k = pltpu.make_async_copy(m["kgo"], key_grad, m["out_sem"].at[1])
-    out_v = pltpu.make_async_copy(m["vgo"], value_grad, m["out_sem"].at[2])
-    for i in range(n_i + 4):
+    lag = 3
+    for i in range(n_i + lag):
         if i < n_i:
             own_terms(i)
         if 0 < i <= n_i:
             c_copy(i - 1).start()
-        if i >= 4:
-            core_sum(i - 4)
-        if i == n_i - 1:
-            for r in (2, 1, 3):
-                wy_copy(0, r).start()
-    for r in (2, 1, 3):
-        wy_copy(1, r).start()
-    out_k.start()
-    out_v.start()
+        if i >= lag:
+            core_sum(i - lag)
+            if (i - lag) % 2:
+                for r in (2, 1, 3):
+                    wy_copy((i - lag) // 2, r).start()
 
     def z_of(i):
         return 2 * ((x + n_x - i // 2) % n_x) + i % 2
@@ -670,24 +650,22 @@
         c_copy(i).wait_send()
     out_q.wait()
 
-    for part in range(2):
+    for part in range(n_x):
         for r in (1, 3, 2):
             wy_copy(part, r).wait_recv()
-        for i in range(part * 4, part * 4 + 4):
+        for i in (2 * part, 2 * part + 1):
             total = m["wy_own"][i]
             for r in range(1, N_Y):
-                total = total + m["wyr"][part, r, i % 4].astype(F32)
+                total = total + m["wyr"][part, r, i % 2].astype(F32)
             m["wz_own"][i] = total
             m["wz"][i] = total.astype(BF16)
-        for i in range(part * 4, part * 4 + 4):
+        for i in (2 * part, 2 * part + 1):
             @pl.when(z_of(i) != z)
             def _():
                 wz_copy(i).start()
-    for part in range(2):
+    for part in range(n_x):
         for r in range(1, N_Y):
             wy_copy(part, r).wait_send()
-    out_k.wait()
-    out_v.wait()
     mine = 2 * ((x + n_x - z // 2) % n_x) + z % 2
     total = m["wz_own"][mine]
     for r in range(1, n_z):
@@ -701,14 +679,11 @@
             device_id_type=MESH,
         ).wait_recv()
         total = total + m["wzr"][frm].astype(F32)
-    m["wgo"][...] = total
+    weight_grad[...] = total
     for i in range(n_i):
         @pl.when(z_of(i) != z)
         def _():
             wz_copy(i).wait_send()
-    out_w = pltpu.make_async_copy(m["wgo"], weight_grad, m["out_sem"].at[3])
-    out_w.start()
-    out_w.wait()
 
 
 def index_table(chosen, n_b, n_dev):
@@ -733,7 +708,7 @@
     slots = slot.transpose(1, 0, 2).reshape(-1)
     kinds = kind.transpose(1, 0, 2).reshape(-1)
     inverse = inverse.transpose(0, 2, 1).reshape(-1)
-    return jnp.concatenate([picks, slots, kinds, inverse]).astype(jnp.int32)
+    return picks, slots, kinds, inverse
 
 
 def local(queries, key_heads, values, log_sums, out_grad, inputs, chosen):
@@ -745,8 +720,9 @@
     n_list = chosen.shape[2]
     idx = index_table(chosen, n_b, n_dev)
     scratch = scratch_list(rows, n_dev, n_x, n_list, feats, heads)
-    hbm = pl.BlockSpec(memory_space=pl.ANY)
-    return pl.pallas_call(
+    hbm = pl.BlockSpec(memory_space=pltpu.HBM)
+    vm = pl.BlockSpec(memory_space=pltpu.VMEM)
+    query_sums, key_grad, value_grad, weight_grad = pl.pallas_call(
         functools.partial(
             fused_kernel, [name for name, _ in scratch], n_dev // PLANE, n_x, n_list
         ),
@@ -756,15 +732,15 @@
             jax.ShapeDtypeStruct(values.shape, F32),
             jax.ShapeDtypeStruct((feats * n_x // n_dev, 128), F32),
         ),
-        in_specs=[pl.BlockSpec(memory_space=pltpu.SMEM)] + [hbm] * 6,
-        out_specs=(hbm,) * 4,
+        in_specs=[pl.BlockSpec(memory_space=pltpu.SMEM)] * 4 + [hbm] * 6,
+        out_specs=(hbm, vm, vm, vm),
         scratch_shapes=[kind for _, kind in scratch],
         compiler_params=pltpu.CompilerParams(
-            collective_id=0, has_side_effects=True, vmem_limit_bytes=60 * 1024 * 1024
+            collective_id=0, has_side_effects=True, vmem_limit_bytes=53 * 1024 * 1024
         ),
         name="fused",
     )(
-        idx,
+        *idx,
         key_heads.reshape(n_b, BLOCK, -1),
         values.reshape(n_b, BLOCK, -1),
         queries,
@@ -772,6 +748,7 @@
         log_sums,
         inputs,
     )
+    return query_sums * (HD ** -0.5), key_grad, value_grad, weight_grad
 
 
 def solution(mesh):

time: 103 us -> 95.9 us (0.931)
  Pallas kernels: 94.1 us -> 87.8 us
  local copies, waits for them, and re-layouts: 7.01 us -> 4.41 us
  other arithmetic: 0.66 us -> 2.74 us
    pallas_call x1, Pallas kernels: 94.1 us -> 87.8 us  [local(): pl.pallas_call(functools.partial(fused_kernel, [name for name, _ in scrat...]
    mul x0 -> x1, other arithmetic: none -> 2.08 us  [local(): return (query_sums * HD ** (-0.5), key_grad, value_grad, weight_grad)]
    unnamed x13 -> x12, local copies, waits for them, and re-layouts: 5.31 us -> 3.4 us
where the time goes in v5:
time: 95.9 us; the launch traced here: 95.7 us
  Pallas kernels  87.8 us (92%)
  local copies, waits for them, and re-layouts  4.41 us (5%)
  other arithmetic  2.74 us (3%)
    pallas_call x1, Pallas kernels, local(): pl.pallas_call(functools.partial(fused_kernel, [name for name, _ in scrat...  87.8 us
    unnamed x12, local copies, waits for them, and re-layouts  3.4 us
    mul x1, other arithmetic, local(): return (query_sums * HD ** (-0.5), key_grad, value_grad, weight_grad)  2.08 us

profile of v5, /device:TPU:6, one launch (start us, length us, event | category | flops | bytes accessed | tf_op | source)
XLA Modules:
  0.0 95.7 jit_solution(12965312231051813436)
XLA Ops:
  0.6 0.0 copy-start
  0.7 0.7 copy-done
  1.4 0.1 constant_dynamic-slice_fusion
  1.5 0.1 copy.31
  1.6 0.1 select_bitcast_fusion
  1.7 0.1 reshape.45.refs_2_
  1.8 0.1 reshape.44.refs_1_
  1.9 0.1 select_reduce_fusion
  2.0 0.1 constant_dynamic-slice_fusion.1
  2.1 0.1 copy.25
  2.2 0.1 sub.27
  2.3 0.4 fusion.1
  2.7 0.0 copy-start.2
  2.7 0.1 copy.26
  2.8 0.0 copy-start.1
  2.8 0.1 reshape.43.refs_0_
  3.0 0.1 copy.30
  3.1 0.0 copy-start.3
  3.1 0.1 reshape.46.refs_3_
  3.2 0.3 copy-done.2
  3.6 0.2 copy-done.1
  3.7 0.1 copy-done.3
  3.8 87.8 %fused.1 = (f32[384,512]{1,0:T(8,128)}, f32[384,128]{1,0:T(8,128)S(1)}, f32[384,128]{1,0:T(8,128)S(1)}, f32[64,128]{1,0:T(8,128)S(1)}) custom-call(s32[128]{0:T(128)S(1)} %reshape.43.refs_0_, s32[192]{0:T(256)S(1)} %reshape.44.refs_1_, s32[192]{0:T(256)S(1)} %reshape.45.refs_2_, s32[840]{0:T(1024)S(1)} %reshape.46.refs_3_, bf16[6,64,128]{2,1,0:T(8,128)(2,1)S(1)} %bitcast.7, ...), custom_call_target="tpu_custom_call" | custom-call | tf_op jit(solution)/shard_map/fused/pallas_call | solution.py:725
  91.7 2.1 %broadcast_multiply_fusion = f32[384,512]{1,0:T(8,128)} fusion(f32[384,512]{1,0:T(8,128)} %get-tuple-element.8), kind=kLoop, calls=%fused_computation | loop fusion | flops 196608 | bytes 1572864 | tf_op jit(solution)/shard_map/mul | solution.py:751
  93.7 0.7 copy.35
  94.4 0.7 copy.36
  95.1 0.6 copy.37
  (5 shorter events, 0.0 us)
Async XLA Ops:
  0.6 0.8 copy-start
  2.7 0.9 copy-start.2
  2.8 0.9 copy-start.1
  3.1 0.7 copy-start.3

commit v6 on v5

--- a/solution.py
+++ b/solution.py
@@ -12,6 +12,7 @@
 NEG = -1e30
 LOG2E = 1.4426950408889634
 CHUNK = 4
+PARTS = 3
 N_Y = 4
 N_C = 2
 PLANE = N_Y * N_C
@@ -65,8 +66,8 @@
         ("wzr", pltpu.VMEM((8,) + tile, BF16)),
         ("in_sem", dma((6,))),
         ("out_sem", dma((1,))),
-        ("z_send", dma((2, 2, 5, 2))),
-        ("z_recv", dma((2, 2, 5, 2))),
+        ("z_send", dma((2, 2, 5, PARTS))),
+        ("z_recv", dma((2, 2, 5, PARTS))),
         ("y_send", dma((2, 8))),
         ("y_recv", dma((2, 8))),
         ("x_send", dma((2, 3, 2))),
@@ -151,7 +152,7 @@
         return m[f"own{g}"] if step == 0 else m[f"held{g}{way}{step}"]
 
     def z_copy(g, way, step, part):
-        blocks = pl.ds(part * (n_b // 2), n_b // 2)
+        blocks = pl.ds(part * (n_b // PARTS), n_b // PARTS)
         return pltpu.make_async_remote_copy(
             src_ref=held(g, way, step - 1).at[blocks],
             dst_ref=held(g, way, step).at[blocks],
@@ -234,7 +235,7 @@
                 act(g, 4 + step, z + step - n_z, held(g, 1, step))
 
     def set_out(g):
-        for part in range(2):
+        for part in range(PARTS):
             for way in range(2):
                 @pl.when(sends(way, 1))
                 def _():
@@ -248,7 +249,7 @@
     pick(1, 0, z, m["own1"])
 
     def relay(g, step):
-        for part in range(2):
+        for part in range(PARTS):
             for way in range(2):
                 if step <= steps(way):
                     @pl.when(gets(way, step))
@@ -278,7 +279,7 @@
 
     for step in range(1, 5):
         relay(0, step)
-        if step == 3:
+        if step == 2:
             set_out(1)
         each_piece(0, step, pick)
 
@@ -352,7 +353,7 @@
                 (((0,), (0,)), ((), ())),
                 preferred_element_type=F32,
             )
-            dq = dq_t.T
+            dq = dq_t.T * (HD ** -0.5)
             for pair in range(per_group // 2):
                 even = dq[(2 * pair) * BLOCK : (2 * pair + 1) * BLOCK]
                 odd = dq[(2 * pair + 1) * BLOCK : (2 * pair + 2) * BLOCK]
@@ -504,7 +505,7 @@
         0,
         {
             0: functools.partial(relay_and_pick, 1, 2),
-            2: functools.partial(relay_and_pick, 1, 3),
+            1: functools.partial(relay_and_pick, 1, 3),
             3: functools.partial(relay_and_pick, 1, 4),
             4: relay_x,
         },
@@ -516,10 +517,10 @@
     out_q = pltpu.make_async_copy(m["qg"], query_grad, m["out_sem"].at[0])
     out_q.start()
     collect(0, 2)
+    collect(1, 4)
     collect(0, 7)
-    collect(1, 4)
+    collect(1, 5)
     collect(0, 1)
-    collect(1, 5)
     collect(1, 3)
     collect(0, 0)
     for d in RETURN_ORDER[3:]:
@@ -619,7 +620,7 @@
             for step in range(1, steps(way) + 1):
                 @pl.when(sends(way, step))
                 def _():
-                    for part in range(2):
+                    for part in range(PARTS):
                         z_copy(g, way, step, part).wait_send()
 
         sent(g, 0, z, None)
@@ -686,6 +687,43 @@
             wz_copy(i).wait_send()
 
 
+def put_kernel(q_src, k_src, v_src, w_src, q_dst, k_dst, v_dst, w_dst, q_mid, sem):
+    rows = q_mid.shape[0] // 3
+    part = [pl.ds(i * rows, rows) for i in range(3)]
+    into = [
+        pltpu.make_async_copy(q_src.at[part[i]], q_mid.at[part[i]], sem.at[i]) for i in range(3)
+    ]
+    rest = [
+        pltpu.make_async_copy(src, dst, sem.at[3 + i])
+        for i, (src, dst) in enumerate([(k_src, k_dst), (v_src, v_dst), (w_src, w_dst)])
+    ]
+    out = [
+        pltpu.make_async_copy(q_mid.at[part[i]], q_dst.at[part[i]], sem.at[6 + i]) for i in range(3)
+    ]
+    for copy in into + rest:
+        copy.start()
+    for i in range(3):
+        into[i].wait()
+        out[i].start()
+    for copy in rest + out:
+        copy.wait()
+
+
+def put_out(query_grad, key_grad, value_grad, weight_grad):
+    hbm = pl.BlockSpec(memory_space=pltpu.HBM)
+    vm = pl.BlockSpec(memory_space=pltpu.VMEM)
+    arrays = (query_grad, key_grad, value_grad, weight_grad)
+    return pl.pallas_call(
+        put_kernel,
+        out_shape=tuple(jax.ShapeDtypeStruct(a.shape, a.dtype) for a in arrays),
+        in_specs=[hbm, vm, vm, vm],
+        out_specs=(hbm,) * 4,
+        scratch_shapes=[pltpu.VMEM(query_grad.shape, F32), pltpu.SemaphoreType.DMA((9,))],
+        compiler_params=pltpu.CompilerParams(vmem_limit_bytes=int(53.4 * 1024 * 1024)),
+        name="put_out",
+    )(*arrays)
+
+
 def index_table(chosen, n_b, n_dev):
     groups, _, n_list = chosen.shape
     me = lax.axis_index("kv")
@@ -722,7 +760,7 @@
     scratch = scratch_list(rows, n_dev, n_x, n_list, feats, heads)
     hbm = pl.BlockSpec(memory_space=pltpu.HBM)
     vm = pl.BlockSpec(memory_space=pltpu.VMEM)
-    query_sums, key_grad, value_grad, weight_grad = pl.pallas_call(
+    results = pl.pallas_call(
         functools.partial(
             fused_kernel, [name for name, _ in scratch], n_dev // PLANE, n_x, n_list
         ),
@@ -748,7 +786,7 @@
         log_sums,
         inputs,
     )
-    return query_sums * (HD ** -0.5), key_grad, value_grad, weight_grad
+    return put_out(*results)
 
 
 def solution(mesh):

time: 95.9 us -> 94.1 us (0.981)
  Pallas kernels: 87.8 us -> 90 us
  other arithmetic: 2.74 us -> 0.66 us
  local copies, waits for them, and re-layouts: 4.41 us -> 2.45 us
    mul x1 -> x0, other arithmetic: 2.08 us -> none  [local(): return (query_sums * HD ** (-0.5), key_grad, value_grad, weight_grad)]
    pallas_call x0 -> x1, Pallas kernels: none -> 2.05 us  [put_out(): pl.pallas_call(put_kernel, out_shape=tuple((jax.ShapeDtypeStruct(a.shape,...]
    unnamed x12 -> x9, local copies, waits for them, and re-layouts: 3.4 us -> 1.43 us
where the time goes in v6:
time: 94.1 us; the launch traced here: 93.9 us
  Pallas kernels  90 us (96%)
  local copies, waits for them, and re-layouts  2.45 us (3%)
    pallas_call x1, Pallas kernels, local(): pl.pallas_call(functools.partial(fused_kernel, [name for name, _ in scrat...  88 us
    pallas_call x1, Pallas kernels, put_out(): pl.pallas_call(put_kernel, out_shape=tuple((jax.ShapeDtypeStruct(a.shape,...  2.05 us

profile of v6, /device:TPU:6, one launch (start us, length us, event | category | flops | bytes accessed | tf_op | source)
XLA Modules:
  0.0 93.9 jit_solution(4152248038727416526)
XLA Ops:
  0.6 0.0 copy-start
  0.7 0.7 copy-done
  1.4 0.1 constant_dynamic-slice_fusion
  1.5 0.1 copy.31
  1.6 0.1 select_bitcast_fusion
  1.7 0.1 reshape.45.refs_2_
  1.8 0.1 reshape.44.refs_1_
  1.9 0.1 select_reduce_fusion
  2.0 0.1 constant_dynamic-slice_fusion.1
  2.1 0.1 copy.25
  2.2 0.1 sub.27
  2.3 0.4 fusion.1
  2.7 0.0 copy-start.2
  2.7 0.1 copy.26
  2.8 0.0 copy-start.1
  2.8 0.1 reshape.43.refs_0_
  3.0 0.1 copy.30
  3.1 0.0 copy-start.3
  3.1 0.1 reshape.46.refs_3_
  3.2 0.3 copy-done.2
  3.6 0.2 copy-done.1
  3.7 0.1 copy-done.3
  3.8 88.0 %fused.1 = (f32[384,512]{1,0:T(8,128)}, f32[384,128]{1,0:T(8,128)S(1)}, f32[384,128]{1,0:T(8,128)S(1)}, f32[64,128]{1,0:T(8,128)S(1)}) custom-call(s32[128]{0:T(128)S(1)} %reshape.43.refs_0_, s32[192]{0:T(256)S(1)} %reshape.44.refs_1_, s32[192]{0:T(256)S(1)} %reshape.45.refs_2_, s32[840]{0:T(1024)S(1)} %reshape.46.refs_3_, bf16[6,64,128]{2,1,0:T(8,128)(2,1)S(1)} %bitcast.7, ...), custom_call_target="tpu_custom_call" | custom-call | tf_op jit(solution)/shard_map/fused/pallas_call | solution.py:763
  91.8 2.1 %put_out.1 = (f32[384,512]{1,0:T(8,128)}, f32[384,128]{1,0:T(8,128)}, f32[384,128]{1,0:T(8,128)}, f32[64,128]{1,0:T(8,128)}) custom-call(f32[384,512]{1,0:T(8,128)} %get-tuple-element.8.q_src, f32[384,128]{1,0:T(8,128)S(1)} %get-tuple-element.9.k_src, f32[384,128]{1,0:T(8,128)S(1)} %get-tuple-element.10.v_src, f32[64,128]{1,0:T(8,128)S(1)} %get-tuple-element.11.w_src), custom_call_target="tpu_custom_call" | custom-call | tf_op jit(solution)/shard_map/put_out/pallas_call | solution.py:716
  (5 shorter events, 0.0 us)
Async XLA Ops:
  0.6 0.8 copy-start
  2.7 0.9 copy-start.2
  2.8 0.9 copy-start.1
  3.1 0.7 copy-start.3

commit v7 on v6

--- a/solution.py
+++ b/solution.py
@@ -164,13 +164,29 @@
 
     def sends(way, step):
         if way:
-            return (z + step - 1) % n_z < 3
+            return gets(1, step - 1) & (z > n_z - 3)
         return (z < n_z - 1) & (z - step + 1 >= 0)
 
     def gets(way, step):
         if way:
-            return (z + step) % n_z < 3
+            return (z + step >= n_z) & (z + step < n_z + 3)
         return z - step >= 0
+
+    def top_copy(g, part):
+        blocks = pl.ds(part * (n_b // PARTS), n_b // PARTS)
+        out = []
+        for step in range(1, 4):
+            out.append(
+                pltpu.make_async_remote_copy(
+                    src_ref=m[f"own{g}"].at[blocks],
+                    dst_ref=held(g, 1, step).at[blocks],
+                    send_sem=m["z_send"].at[g, 1, 0, part],
+                    recv_sem=m["z_recv"].at[g, 1, step, part],
+                    device_id={"kv": (n_z - 1) * PLANE + q},
+                    device_id_type=MESH,
+                )
+            )
+        return out
 
     def steps(way):
         return 3 if way else 4
@@ -230,16 +246,20 @@
             act(g, step, z - step, held(g, 0, step))
 
         if step < 4:
-            @pl.when(gets(1, step) & (z + step >= n_z))
+            @pl.when(gets(1, step))
             def _():
                 act(g, 4 + step, z + step - n_z, held(g, 1, step))
 
     def set_out(g):
         for part in range(PARTS):
-            for way in range(2):
-                @pl.when(sends(way, 1))
+            @pl.when(sends(0, 1))
+            def _():
+                z_copy(g, 0, 1, part).start()
+
+            for step, copy in enumerate(top_copy(g, part), 1):
+                @pl.when(z == step - 1)
                 def _():
-                    z_copy(g, way, 1, part).start()
+                    copy.start()
 
     set_out(0)
     for part in range(2):
@@ -430,13 +450,15 @@
             device_id_type=MESH,
         )
 
-    def up_copy(g, e, part, passing=False):
+    def up_copy(g, e, part, last=False):
+        d = n_z - e
+        at = 0 if last else e - 1
         return pltpu.make_async_remote_copy(
-            src_ref=m["zr_up"].at[g, e, part] if passing else m["zs"].at[g, n_z - e, part],
-            dst_ref=m["zr_up"].at[g, e - 1, part],
-            send_sem=m["r_send"].at[g, n_z - e, part],
-            recv_sem=m["r_recv_up"].at[g, e - 1, part],
-            device_id=up_z,
+            src_ref=m["zs"].at[g, d, part],
+            dst_ref=m["zr_up"].at[g, at, part],
+            send_sem=m["r_send"].at[g, d, part],
+            recv_sem=m["r_recv_up"].at[g, at, part],
+            device_id={"kv": (n_z - 1 - d) * PLANE + q} if last else up_z,
             device_id_type=MESH,
         )
 
@@ -469,7 +491,15 @@
                     if e < 3:
                         up_arrival(g, e, part)
                     store_out(g, d, part)
-                    up_copy(g, e, part).start()
+
+                    @pl.when(z == n_z - 1)
+                    def _():
+                        up_copy(g, e, part, last=True).start()
+
+                    if e > 1:
+                        @pl.when(z < n_z - 1)
+                        def _():
+                            up_copy(g, e, part).start()
                 else:
                     if d < 4:
                         @pl.when(z < n_z - 1)
@@ -479,13 +509,6 @@
                         store_out(g, d, part)
                         dn_copy(g, d, part).start()
 
-        if d > 4 and e < 3:
-            @pl.when(z < 3 - e)
-            def _():
-                for part in range(2):
-                    up_copy(g, e + 1, part).wait_recv()
-                    up_copy(g, e, part, passing=True).start()
-
         if d == 0:
             @pl.when(z < 3)
             def _():
@@ -498,15 +521,15 @@
             each_piece(g, step, landed)
 
     relay_and_pick(1, 1)
+    relay_and_pick(1, 2)
     loads[2].wait()
     loads[3].wait()
     wait_fetch(0)
     attention(
         0,
         {
-            0: functools.partial(relay_and_pick, 1, 2),
-            1: functools.partial(relay_and_pick, 1, 3),
-            3: functools.partial(relay_and_pick, 1, 4),
+            0: functools.partial(relay_and_pick, 1, 3),
+            2: functools.partial(relay_and_pick, 1, 4),
             4: relay_x,
         },
     )
@@ -616,8 +639,13 @@
         wait_group(m["picked"].at[g, order, others], m["y_send"].at[g, order])
 
     for g in range(2):
+        for part in range(PARTS):
+            @pl.when(z < 3)
+            def _():
+                top_copy(g, part)[0].wait_send()
+
         for way in range(2):
-            for step in range(1, steps(way) + 1):
+            for step in range(1 + way, steps(way) + 1):
                 @pl.when(sends(way, step))
                 def _():
                     for part in range(PARTS):
@@ -638,9 +666,9 @@
                         dn_copy(g, d, part).wait_send()
                 elif d:
                     e = n_z - d
-                    @pl.when((z - d >= 0) | (z < 3 - e))
+                    @pl.when(z - d >= 0)
                     def _():
-                        up_copy(g, e, part).wait_send()
+                        up_copy(g, e, part, last=True).wait_send()
 
     for part in range(2):
         x_copy(True, 1, part).wait_send()

time: 94.1 us -> 99.8 us (1.061)
  Pallas kernels: 90 us -> 95.8 us
    pallas_call x1, Pallas kernels: 88 us -> 93.7 us  [local(): pl.pallas_call(functools.partial(fused_kernel, [name for name, _ in scrat...]
where the time goes in v7:
time: 99.8 us; the launch traced here: 99.6 us
  Pallas kernels  95.8 us (96%)
  local copies, waits for them, and re-layouts  2.45 us (2%)
    pallas_call x1, Pallas kernels, local(): pl.pallas_call(functools.partial(fused_kernel, [name for name, _ in scrat...  93.7 us
    pallas_call x1, Pallas kernels, put_out(): pl.pallas_call(put_kernel, out_shape=tuple((jax.ShapeDtypeStruct(a.shape,...  2.05 us

profile of v7, /device:TPU:6, one launch (start us, length us, event | category | flops | bytes accessed | tf_op | source)
XLA Modules:
  0.0 99.6 jit_solution(2325718849916409817)
XLA Ops:
  0.6 0.0 copy-start
  0.7 0.7 copy-done
  1.4 0.1 constant_dynamic-slice_fusion
  1.5 0.1 copy.31
  1.6 0.1 select_bitcast_fusion
  1.7 0.1 reshape.45.refs_2_
  1.8 0.1 reshape.44.refs_1_
  1.9 0.1 select_reduce_fusion
  2.0 0.1 constant_dynamic-slice_fusion.1
  2.1 0.1 copy.25
  2.2 0.1 sub.27
  2.3 0.4 fusion.1
  2.7 0.0 copy-start.2
  2.7 0.1 copy.26
  2.8 0.0 copy-start.1
  2.8 0.1 reshape.43.refs_0_
  3.0 0.1 copy.30
  3.1 0.0 copy-start.3
  3.1 0.1 reshape.46.refs_3_
  3.2 0.3 copy-done.2
  3.6 0.2 copy-done.1
  3.7 0.1 copy-done.3
  3.8 93.7 %fused.1 = (f32[384,512]{1,0:T(8,128)}, f32[384,128]{1,0:T(8,128)S(1)}, f32[384,128]{1,0:T(8,128)S(1)}, f32[64,128]{1,0:T(8,128)S(1)}) custom-call(s32[128]{0:T(128)S(1)} %reshape.43.refs_0_, s32[192]{0:T(256)S(1)} %reshape.44.refs_1_, s32[192]{0:T(256)S(1)} %reshape.45.refs_2_, s32[840]{0:T(1024)S(1)} %reshape.46.refs_3_, bf16[6,64,128]{2,1,0:T(8,128)(2,1)S(1)} %bitcast.7, ...), custom_call_target="tpu_custom_call" | custom-call | tf_op jit(solution)/shard_map/fused/pallas_call | solution.py:791
  97.6 2.1 %put_out.1 = (f32[384,512]{1,0:T(8,128)}, f32[384,128]{1,0:T(8,128)}, f32[384,128]{1,0:T(8,128)}, f32[64,128]{1,0:T(8,128)}) custom-call(f32[384,512]{1,0:T(8,128)} %get-tuple-element.8.q_src, f32[384,128]{1,0:T(8,128)S(1)} %get-tuple-element.9.k_src, f32[384,128]{1,0:T(8,128)S(1)} %get-tuple-element.10.v_src, f32[64,128]{1,0:T(8,128)S(1)} %get-tuple-element.11.w_src), custom_call_target="tpu_custom_call" | custom-call | tf_op jit(solution)/shard_map/put_out/pallas_call | solution.py:744
  (5 shorter events, 0.0 us)
Async XLA Ops:
  0.6 0.8 copy-start
  2.7 0.9 copy-start.2
  2.8 0.9 copy-start.1
  3.1 0.7 copy-start.3

commit v8 on v6

--- a/solution.py
+++ b/solution.py
@@ -17,7 +17,7 @@
 N_C = 2
 PLANE = N_Y * N_C
 MESH = pl.DeviceIdType.MESH
-RETURN_ORDER = (4, 5, 3, 6, 2, 7, 1, 0)
+RETURN_ORDER = (4, 3, 5, 6, 2, 1, 7, 0)
 F32, BF16 = jnp.float32, jnp.bfloat16
 
 
@@ -54,7 +54,7 @@
         ("acc", pltpu.VMEM((2, n_b) + tile, F32)),
         ("zs", pltpu.VMEM((2, 8, 2, n_b, BLOCK // 2, 128), BF16)),
         ("zr_dn", pltpu.VMEM((2, 4, 2, n_b, BLOCK // 2, 128), BF16)),
-        ("zr_up", pltpu.VMEM((2, 3, 2, n_b, BLOCK // 2, 128), BF16)),
+        ("zr_up", pltpu.VMEM((2, 4, 2, n_b, BLOCK // 2, 128), BF16)),
         ("kg", pltpu.VMEM((rows, 128), BF16)),
         ("wpart", pltpu.VMEM((8, N_C, N_Y) + tile, BF16)),
         ("crecv", pltpu.VMEM((8, N_Y) + tile, BF16)),
@@ -76,7 +76,7 @@
         ("b_recv", dma((2, 8))),
         ("r_send", dma((2, 8, 2))),
         ("r_recv_dn", dma((2, 4, 2))),
-        ("r_recv_up", dma((2, 3, 2))),
+        ("r_recv_up", dma((2, 4, 2))),
         ("c_send", dma((8,))),
         ("c_recv", dma((8,))),
         ("wy_send", dma((4, N_Y))),
@@ -426,17 +426,18 @@
             dst_ref=m["zr_dn"].at[g, d - 1, part],
             send_sem=m["r_send"].at[g, d, part],
             recv_sem=m["r_recv_dn"].at[g, d - 1, part],
-            device_id=dn_z,
-            device_id_type=MESH,
-        )
-
-    def up_copy(g, e, part, passing=False):
+            device_id={"kv": (z + n_z - (2 - d % 2)) % n_z * PLANE + q},
+            device_id_type=MESH,
+        )
+
+    def up_copy(g, d, at, part):
+        to = n_z - 1 if at else n_z - 1 - d
         return pltpu.make_async_remote_copy(
-            src_ref=m["zr_up"].at[g, e, part] if passing else m["zs"].at[g, n_z - e, part],
-            dst_ref=m["zr_up"].at[g, e - 1, part],
-            send_sem=m["r_send"].at[g, n_z - e, part],
-            recv_sem=m["r_recv_up"].at[g, e - 1, part],
-            device_id=up_z,
+            src_ref=m["zs"].at[g, d, part],
+            dst_ref=m["zr_up"].at[g, at, part],
+            send_sem=m["r_send"].at[g, d, part],
+            recv_sem=m["r_recv_up"].at[g, at, part],
+            device_id={"kv": to * PLANE + q},
             device_id_type=MESH,
         )
 
@@ -447,10 +448,12 @@
             m["acc"][g, b, rows, :] += ref[b].astype(F32)
 
     def dn_arrival(g, d, part):
-        add_arrival(g, dn_copy(g, d + 1, part), m["zr_dn"].at[g, d, part], part)
-
-    def up_arrival(g, e, part):
-        add_arrival(g, up_copy(g, e + 1, part), m["zr_up"].at[g, e, part], part)
+        @pl.when(z < n_z - (2 - d % 2))
+        def _():
+            add_arrival(g, dn_copy(g, d, part), m["zr_dn"].at[g, d - 1, part], part)
+
+    def up_arrival(g, at, part):
+        add_arrival(g, up_copy(g, 5, at, part), m["zr_up"].at[g, at, part], part)
 
     def store_out(g, d, part):
         rows = slice(part * 32, part * 32 + 32)
@@ -458,39 +461,37 @@
             m["zs"][g, d, part, b] = m["acc"][g, b, rows, :].astype(BF16)
 
     def collect(g, d):
-        e = n_z - d
-
         @pl.when(z - d >= 0)
         def _():
             wait_group(m["back"].at[g, d, others], m["b_recv"].at[g, d])
             for part in range(2):
                 accumulate(g, d, part)
-                if d > 4:
-                    if e < 3:
-                        up_arrival(g, e, part)
-                    store_out(g, d, part)
-                    up_copy(g, e, part).start()
+                if d in (0, 2):
+                    dn_arrival(g, d + 1, part)
+                    dn_arrival(g, d + 2, part)
+                if d in (6, 7):
+                    @pl.when(z == n_z - 1)
+                    def _():
+                        for at in {6: (2,), 7: (1, 3)}[d]:
+                            up_arrival(g, at, part)
+
+                if d == 0:
+                    @pl.when(z < 3)
+                    def _():
+                        up_arrival(g, 0, part)
+                    continue
+                store_out(g, d, part)
+                if d < 5:
+                    dn_copy(g, d, part).start()
                 else:
-                    if d < 4:
-                        @pl.when(z < n_z - 1)
+                    @pl.when(z == n_z - 1)
+                    def _():
+                        up_copy(g, d, 0, part).start()
+
+                    for plane, at in {5: ((5, 1), (6, 2)), 6: ((6, 3),), 7: ()}[d]:
+                        @pl.when(z == plane)
                         def _():
-                            dn_arrival(g, d, part)
-                    if d > 0:
-                        store_out(g, d, part)
-                        dn_copy(g, d, part).start()
-
-        if d > 4 and e < 3:
-            @pl.when(z < 3 - e)
-            def _():
-                for part in range(2):
-                    up_copy(g, e + 1, part).wait_recv()
-                    up_copy(g, e, part, passing=True).start()
-
-        if d == 0:
-            @pl.when(z < 3)
-            def _():
-                for part in range(2):
-                    up_arrival(g, 0, part)
+                            up_copy(g, d, at, part).start()
 
     def wait_fetch(g):
         landed(g, 0, z, None)
@@ -498,15 +499,15 @@
             each_piece(g, step, landed)
 
     relay_and_pick(1, 1)
+    relay_and_pick(1, 2)
     loads[2].wait()
     loads[3].wait()
     wait_fetch(0)
     attention(
         0,
         {
-            0: functools.partial(relay_and_pick, 1, 2),
-            1: functools.partial(relay_and_pick, 1, 3),
-            3: functools.partial(relay_and_pick, 1, 4),
+            0: functools.partial(relay_and_pick, 1, 3),
+            2: functools.partial(relay_and_pick, 1, 4),
             4: relay_x,
         },
     )
@@ -516,15 +517,10 @@
     give_back(1)
     out_q = pltpu.make_async_copy(m["qg"], query_grad, m["out_sem"].at[0])
     out_q.start()
-    collect(0, 2)
-    collect(1, 4)
-    collect(0, 7)
-    collect(1, 5)
-    collect(0, 1)
-    collect(1, 3)
-    collect(0, 0)
-    for d in RETURN_ORDER[3:]:
-        collect(1, d)
+    for g, d in [
+        (0, 2), (1, 4), (0, 1), (1, 3), (0, 7), (1, 5), (1, 6), (1, 2), (1, 1), (1, 7), (1, 0), (0, 0)
+    ]:
+        collect(g, d)
 
     for b in range(n_b):
         rows = slice(b * BLOCK, (b + 1) * BLOCK)
@@ -637,10 +633,9 @@
                     def _():
                         dn_copy(g, d, part).wait_send()
                 elif d:
-                    e = n_z - d
-                    @pl.when((z - d >= 0) | (z < 3 - e))
+                    @pl.when(z - d >= 0)
                     def _():
-                        up_copy(g, e, part).wait_send()
+                        up_copy(g, d, 0, part).wait_send()
 
     for part in range(2):
         x_copy(True, 1, part).wait_send()

time: 94.1 us -> 99.3 us (1.055)
  Pallas kernels: 90 us -> 95.3 us
    pallas_call x1, Pallas kernels: 88 us -> 93.2 us  [local(): pl.pallas_call(functools.partial(fused_kernel, [name for name, _ in scrat...]
where the time goes in v8:
time: 99.3 us; the launch traced here: 99.1 us
  Pallas kernels  95.3 us (96%)
  local copies, waits for them, and re-layouts  2.45 us (2%)
    pallas_call x1, Pallas kernels, local(): pl.pallas_call(functools.partial(fused_kernel, [name for name, _ in scrat...  93.2 us
    pallas_call x1, Pallas kernels, put_out(): pl.pallas_call(put_kernel, out_shape=tuple((jax.ShapeDtypeStruct(a.shape,...  2.05 us

profile of v8, /device:TPU:6, one launch (start us, length us, event | category | flops | bytes accessed | tf_op | source)
XLA Modules:
  0.0 99.1 jit_solution(8157122756273538312)
XLA Ops:
  0.6 0.0 copy-start
  0.7 0.7 copy-done
  1.4 0.1 constant_dynamic-slice_fusion
  1.5 0.1 copy.31
  1.6 0.1 select_bitcast_fusion
  1.7 0.1 reshape.45.refs_2_
  1.8 0.1 reshape.44.refs_1_
  1.9 0.1 select_reduce_fusion
  2.0 0.1 constant_dynamic-slice_fusion.1
  2.1 0.1 copy.25
  2.2 0.1 sub.27
  2.3 0.4 fusion.1
  2.7 0.0 copy-start.2
  2.7 0.1 copy.26
  2.8 0.0 copy-start.1
  2.8 0.1 reshape.43.refs_0_
  3.0 0.1 copy.30
  3.1 0.0 copy-start.3
  3.1 0.1 reshape.46.refs_3_
  3.2 0.3 copy-done.2
  3.6 0.2 copy-done.1
  3.7 0.1 copy-done.3
  3.8 93.2 %fused.1 = (f32[384,512]{1,0:T(8,128)}, f32[384,128]{1,0:T(8,128)S(1)}, f32[384,128]{1,0:T(8,128)S(1)}, f32[64,128]{1,0:T(8,128)S(1)}) custom-call(s32[128]{0:T(128)S(1)} %reshape.43.refs_0_, s32[192]{0:T(256)S(1)} %reshape.44.refs_1_, s32[192]{0:T(256)S(1)} %reshape.45.refs_2_, s32[840]{0:T(1024)S(1)} %reshape.46.refs_3_, bf16[6,64,128]{2,1,0:T(8,128)(2,1)S(1)} %bitcast.7, ...), custom_call_target="tpu_custom_call" | custom-call | tf_op jit(solution)/shard_map/fused/pallas_call | solution.py:758
  97.1 2.1 %put_out.1 = (f32[384,512]{1,0:T(8,128)}, f32[384,128]{1,0:T(8,128)}, f32[384,128]{1,0:T(8,128)}, f32[64,128]{1,0:T(8,128)}) custom-call(f32[384,512]{1,0:T(8,128)} %get-tuple-element.8.q_src, f32[384,128]{1,0:T(8,128)S(1)} %get-tuple-element.9.k_src, f32[384,128]{1,0:T(8,128)S(1)} %get-tuple-element.10.v_src, f32[64,128]{1,0:T(8,128)S(1)} %get-tuple-element.11.w_src), custom_call_target="tpu_custom_call" | custom-call | tf_op jit(solution)/shard_map/put_out/pallas_call | solution.py:711
  (5 shorter events, 0.0 us)
Async XLA Ops:
  0.6 0.8 copy-start
  2.7 0.9 copy-start.2
  2.8 0.9 copy-start.1
  3.1 0.7 copy-start.3

commit v9 on v8

--- a/solution.py
+++ b/solution.py
@@ -13,11 +13,13 @@
 LOG2E = 1.4426950408889634
 CHUNK = 4
 PARTS = 3
+ROW_PARTS = 4
+PART_ROWS = BLOCK // ROW_PARTS
 N_Y = 4
 N_C = 2
 PLANE = N_Y * N_C
 MESH = pl.DeviceIdType.MESH
-RETURN_ORDER = (4, 3, 5, 6, 2, 1, 7, 0)
+RETURN_ORDER = (4, 5, 3, 6, 2, 7, 1, 0)
 F32, BF16 = jnp.float32, jnp.bfloat16
 
 
@@ -52,36 +54,30 @@
         ("own_tot", pltpu.VMEM((2, n_b) + tile, F32)),
         ("back", pltpu.VMEM((2, 8, PLANE) + tile, BF16)),
         ("acc", pltpu.VMEM((2, n_b) + tile, F32)),
-        ("zs", pltpu.VMEM((2, 8, 2, n_b, BLOCK // 2, 128), BF16)),
-        ("zr_dn", pltpu.VMEM((2, 4, 2, n_b, BLOCK // 2, 128), BF16)),
-        ("zr_up", pltpu.VMEM((2, 4, 2, n_b, BLOCK // 2, 128), BF16)),
+        ("zs", pltpu.VMEM((2, 8, ROW_PARTS, n_b, PART_ROWS, 128), BF16)),
+        ("zr_dn", pltpu.VMEM((2, 4, ROW_PARTS, n_b, PART_ROWS, 128), BF16)),
+        ("zr_up", pltpu.VMEM((2, 4, ROW_PARTS, n_b, PART_ROWS, 128), BF16)),
         ("kg", pltpu.VMEM((rows, 128), BF16)),
-        ("wpart", pltpu.VMEM((8, N_C, N_Y) + tile, BF16)),
-        ("crecv", pltpu.VMEM((8, N_Y) + tile, BF16)),
-        ("wy", pltpu.VMEM((4, N_Y, 2) + tile, BF16)),
-        ("wy_own", pltpu.VMEM((8,) + tile, F32)),
-        ("wyr", pltpu.VMEM((4, N_Y, 2) + tile, BF16)),
+        ("kg_t", pltpu.VMEM((128, rows), BF16)),
+        ("wpart", pltpu.VMEM((2, n_x, N_C, N_Y) + tile, BF16)),
+        ("crecv", pltpu.VMEM((2, n_x, N_Y) + tile, BF16)),
+        ("wy", pltpu.VMEM((2, 2, N_Y, n_x // 2) + tile, BF16)),
+        ("wy_own", pltpu.VMEM((2, n_x) + tile, F32)),
+        ("wyr", pltpu.VMEM((2, 2, N_Y, n_x // 2) + tile, BF16)),
         ("wz", pltpu.VMEM((8,) + tile, BF16)),
         ("wz_own", pltpu.VMEM((8,) + tile, F32)),
         ("wzr", pltpu.VMEM((8,) + tile, BF16)),
         ("in_sem", dma((6,))),
         ("out_sem", dma((1,))),
-        ("z_send", dma((2, 2, 5, PARTS))),
-        ("z_recv", dma((2, 2, 5, PARTS))),
-        ("y_send", dma((2, 8))),
+        ("sent", dma((8,))),
+        ("z_recv", dma((2, 7, PARTS))),
         ("y_recv", dma((2, 8))),
-        ("x_send", dma((2, 3, 2))),
-        ("x_recv", dma((2, 3, 2))),
-        ("b_send", dma((2, 8))),
+        ("x_recv", dma((2, 3))),
         ("b_recv", dma((2, 8))),
-        ("r_send", dma((2, 8, 2))),
-        ("r_recv_dn", dma((2, 4, 2))),
-        ("r_recv_up", dma((2, 4, 2))),
-        ("c_send", dma((8,))),
-        ("c_recv", dma((8,))),
-        ("wy_send", dma((4, N_Y))),
-        ("wy_recv", dma((4, N_Y))),
-        ("wz_send", dma((8,))),
+        ("r_recv_dn", dma((2, 4, ROW_PARTS))),
+        ("r_recv_up", dma((2, 4, ROW_PARTS))),
+        ("c_recv", dma((2, n_x))),
+        ("wy_recv", dma((2, 2, N_Y - 1))),
         ("wz_recv", dma((8,))),
     ]
     for g in range(2):
@@ -156,8 +152,8 @@
         return pltpu.make_async_remote_copy(
             src_ref=held(g, way, step - 1).at[blocks],
             dst_ref=held(g, way, step).at[blocks],
-            send_sem=m["z_send"].at[g, way, step, part],
-            recv_sem=m["z_recv"].at[g, way, step, part],
+            send_sem=m["sent"].at[0],
+            recv_sem=m["z_recv"].at[g, way * 4 + step - 1, part],
             device_id=dn_z if way else up_z,
             device_id_type=MESH,
         )
@@ -187,8 +183,8 @@
         return pltpu.make_async_remote_copy(
             src_ref=src,
             dst_ref=m["xraw"].at[slot, rows],
-            send_sem=m["x_send"].at[side, rel, part],
-            recv_sem=m["x_recv"].at[side, rel, part],
+            send_sem=m["sent"].at[1],
+            recv_sem=m["x_recv"].at[side, 2 if rel == 2 else part],
             device_id=right if to_right else left,
             device_id_type=MESH,
         )
@@ -198,7 +194,7 @@
         return pltpu.make_async_remote_copy(
             src_ref=m["picked"].at[g, order, r],
             dst_ref=m[f"tab{g}"].at[z_from * PLANE + q],
-            send_sem=m["y_send"].at[g, order],
+            send_sem=m["sent"].at[2],
             recv_sem=m["y_recv"].at[g, order],
             device_id={"kv": z * PLANE + to},
             device_id_type=MESH,
@@ -382,7 +378,7 @@
         return pltpu.make_async_remote_copy(
             src_ref=m["ret"].at[g, (z - d) * PLANE + to],
             dst_ref=m["back"].at[g, d, q],
-            send_sem=m["b_send"].at[g, d],
+            send_sem=m["sent"].at[3],
             recv_sem=m["b_recv"].at[g, d],
             device_id={"kv": z * PLANE + to},
             device_id_type=MESH,
@@ -405,8 +401,8 @@
         lax.fori_loop(0, n_b, own, 0)
 
     def accumulate(g, d, part):
-        rows = slice(part * 32, part * 32 + 32)
-        accs = [jnp.zeros((32, 128), F32) for _ in range(n_b)]
+        rows = slice(part * PART_ROWS, (part + 1) * PART_ROWS)
+        accs = [jnp.zeros((PART_ROWS, 128), F32) for _ in range(n_b)]
         for r in range(PLANE):
             frm = (q + r) % PLANE
             if r == 0:
@@ -424,9 +420,9 @@
         return pltpu.make_async_remote_copy(
             src_ref=m["zs"].at[g, d, part],
             dst_ref=m["zr_dn"].at[g, d - 1, part],
-            send_sem=m["r_send"].at[g, d, part],
+            send_sem=m["sent"].at[4],
             recv_sem=m["r_recv_dn"].at[g, d - 1, part],
-            device_id={"kv": (z + n_z - (2 - d % 2)) % n_z * PLANE + q},
+            device_id=dn_z,
             device_id_type=MESH,
         )
 
@@ -435,7 +431,7 @@
         return pltpu.make_async_remote_copy(
             src_ref=m["zs"].at[g, d, part],
             dst_ref=m["zr_up"].at[g, at, part],
-            send_sem=m["r_send"].at[g, d, part],
+            send_sem=m["sent"].at[4],
             recv_sem=m["r_recv_up"].at[g, at, part],
             device_id={"kv": to * PLANE + q},
             device_id_type=MESH,
@@ -443,12 +439,12 @@
 
     def add_arrival(g, copy, ref, part):
         copy.wait_recv()
-        rows = slice(part * 32, part * 32 + 32)
+        rows = slice(part * PART_ROWS, (part + 1) * PART_ROWS)
         for b in range(n_b):
             m["acc"][g, b, rows, :] += ref[b].astype(F32)
 
     def dn_arrival(g, d, part):
-        @pl.when(z < n_z - (2 - d % 2))
+        @pl.when(z < n_z - 1)
         def _():
             add_arrival(g, dn_copy(g, d, part), m["zr_dn"].at[g, d - 1, part], part)
 
@@ -456,7 +452,7 @@
         add_arrival(g, up_copy(g, 5, at, part), m["zr_up"].at[g, at, part], part)
 
     def store_out(g, d, part):
-        rows = slice(part * 32, part * 32 + 32)
+        rows = slice(part * PART_ROWS, (part + 1) * PART_ROWS)
         for b in range(n_b):
             m["zs"][g, d, part, b] = m["acc"][g, b, rows, :].astype(BF16)
 
@@ -464,11 +460,10 @@
         @pl.when(z - d >= 0)
         def _():
             wait_group(m["back"].at[g, d, others], m["b_recv"].at[g, d])
-            for part in range(2):
+            for part in range(ROW_PARTS):
                 accumulate(g, d, part)
-                if d in (0, 2):
+                if d < 4:
                     dn_arrival(g, d + 1, part)
-                    dn_arrival(g, d + 2, part)
                 if d in (6, 7):
                     @pl.when(z == n_z - 1)
                     def _():
@@ -513,87 +508,104 @@
     )
     give_back(0)
     wait_fetch(1)
-    attention(1, {2 + i: functools.partial(collect, 0, RETURN_ORDER[i]) for i in range(4)})
+    attention(1, {2 + i: functools.partial(collect, 0, RETURN_ORDER[i]) for i in range(3)})
     give_back(1)
     out_q = pltpu.make_async_copy(m["qg"], query_grad, m["out_sem"].at[0])
     out_q.start()
+    def c_copy(g, i):
+        return pltpu.make_async_remote_copy(
+            src_ref=m["wpart"].at[g, i, 1 - c],
+            dst_ref=m["crecv"].at[g, i],
+            send_sem=m["sent"].at[5],
+            recv_sem=m["c_recv"].at[g, i],
+            device_id={"kv": z * PLANE + y * N_C + (1 - c)},
+            device_id_type=MESH,
+        )
+
+    def wy_copy(g, part, r):
+        to = (y + r) % N_Y
+        return pltpu.make_async_remote_copy(
+            src_ref=m["wy"].at[g, part, r],
+            dst_ref=m["wyr"].at[g, part, r],
+            send_sem=m["sent"].at[6],
+            recv_sem=m["wy_recv"].at[g, part, r - 1],
+            device_id={"kv": z * PLANE + to * N_C + c},
+            device_id_type=MESH,
+        )
+
+    half = inputs.shape[1] // 2
+
+    def combine(g):
+        for b in range(n_b):
+            total = m["acc"][g, b] + m["own_tot"][g, b]
+            m["acc"][g, b] = total
+            m["kg"][b * BLOCK : (b + 1) * BLOCK, :] = total.astype(BF16)
+        m["kg_t"][...] = m["kg"][...].T
+
+    def own_terms(g, i):
+        w_t = [
+            lax.dot_general(
+                m["kg_t"][:HD, :], m["xraw"][i, :, h * half : (h + 1) * half],
+                (((1,), (0,)), ((), ())), preferred_element_type=F32,
+            )
+            for h in range(2)
+        ]
+        w = jnp.concatenate(w_t, axis=0).T.astype(BF16)
+        for yy in range(N_Y):
+            for cc in range(N_C):
+                first = (yy * N_C + cc) * BLOCK
+                m["wpart"][g, i, cc, yy] = w[first : first + BLOCK]
+
+    def core_sum(g, i):
+        c_copy(g, i).wait_recv()
+        for r in range(N_Y):
+            yy = (y + r) % N_Y
+            both = m["wpart"][g, i, c, yy].astype(F32) + m["crecv"][g, i, yy].astype(F32)
+            if r:
+                m["wy"][g, i // 2, r, i % 2] = both.astype(BF16)
+            else:
+                m["wy_own"][g, i] = both
+        if i % 2:
+            for r in (2, 1, 3):
+                wy_copy(g, i // 2, r).start()
+
+    def terms_out(g):
+        combine(g)
+        for i in range(n_x):
+            own_terms(g, i)
+            if i:
+                c_copy(g, i - 1).start()
+        c_copy(g, n_x - 1).start()
+
     for g, d in [
-        (0, 2), (1, 4), (0, 1), (1, 3), (0, 7), (1, 5), (1, 6), (1, 2), (1, 1), (1, 7), (1, 0), (0, 0)
+        (0, 2), (1, 4), (0, 6), (1, 5), (0, 1), (1, 3), (0, 7), (1, 6), (1, 2), (0, 0)
     ]:
         collect(g, d)
-
-    for b in range(n_b):
-        rows = slice(b * BLOCK, (b + 1) * BLOCK)
-        t0 = m["acc"][0, b] + m["own_tot"][0, b]
-        t1 = m["acc"][1, b] + m["own_tot"][1, b]
-        kg = jnp.where(low, t0, pltpu.roll(t1, HD, 1))
-        key_grad[rows, :] = kg
-        value_grad[rows, :] = jnp.where(low, pltpu.roll(t0, HD, 1), t1)
-        m["kg"][rows, :] = kg.astype(BF16)
-
-    def c_copy(i):
-        return pltpu.make_async_remote_copy(
-            src_ref=m["wpart"].at[i, 1 - c],
-            dst_ref=m["crecv"].at[i],
-            send_sem=m["c_send"].at[i],
-            recv_sem=m["c_recv"].at[i],
-            device_id={"kv": z * PLANE + y * N_C + (1 - c)},
-            device_id_type=MESH,
-        )
-
     x_copy(True, 1, 1).wait_recv()
     x_copy(False, 1, 0).wait_recv()
     x_copy(True, 2, 0).wait_recv()
     x_copy(False, 2, 1).wait_recv()
     loads[5].wait()
-    kg_t = m["kg"][...].T
-    half = inputs.shape[1] // 2
-    n_i = 2 * n_x
-
-    def wy_copy(part, r):
-        to = (y + r) % N_Y
-        return pltpu.make_async_remote_copy(
-            src_ref=m["wy"].at[part, r],
-            dst_ref=m["wyr"].at[part, r],
-            send_sem=m["wy_send"].at[part, r],
-            recv_sem=m["wy_recv"].at[part, r],
-            device_id={"kv": z * PLANE + to * N_C + c},
-            device_id_type=MESH,
-        )
-
-    def own_terms(i):
-        rel, h = i // 2, i % 2
-        w_t = lax.dot_general(
-            kg_t, m["xraw"][rel, :, h * half : (h + 1) * half], (((1,), (0,)), ((), ())),
-            preferred_element_type=F32,
-        )
-        w = w_t.T.astype(BF16)
-        for yy in range(N_Y):
-            for cc in range(N_C):
-                first = (yy * N_C + cc) * BLOCK
-                m["wpart"][i, cc, yy] = w[first : first + BLOCK]
-
-    def core_sum(i):
-        c_copy(i).wait_recv()
-        for r in range(N_Y):
-            yy = (y + r) % N_Y
-            both = m["wpart"][i, c, yy].astype(F32) + m["crecv"][i, yy].astype(F32)
-            if r:
-                m["wy"][i // 2, r, i % 2] = both.astype(BF16)
-            else:
-                m["wy_own"][i] = both
-
-    lag = 3
-    for i in range(n_i + lag):
-        if i < n_i:
-            own_terms(i)
-        if 0 < i <= n_i:
-            c_copy(i - 1).start()
+    terms_out(0)
+    collect(1, 7)
+    for i in range(n_x):
+        core_sum(0, i)
+    collect(1, 1)
+    collect(1, 0)
+    combine(1)
+    lag = 2
+    for i in range(n_x + lag):
+        if i < n_x:
+            own_terms(1, i)
+        if 0 < i <= n_x:
+            c_copy(1, i - 1).start()
         if i >= lag:
-            core_sum(i - lag)
-            if (i - lag) % 2:
-                for r in (2, 1, 3):
-                    wy_copy((i - lag) // 2, r).start()
+            core_sum(1, i - lag)
+    for b in range(n_b):
+        rows = slice(b * BLOCK, (b + 1) * BLOCK)
+        t0, t1 = m["acc"][0, b], m["acc"][1, b]
+        key_grad[rows, :] = jnp.where(low, t0, pltpu.roll(t1, HD, 1))
+        value_grad[rows, :] = jnp.where(low, pltpu.roll(t0, HD, 1), t1)
 
     def z_of(i):
         return 2 * ((x + n_x - i // 2) % n_x) + i % 2
@@ -602,14 +614,14 @@
         return pltpu.make_async_remote_copy(
             src_ref=m["wz"].at[i],
             dst_ref=m["wzr"].at[z],
-            send_sem=m["wz_send"].at[i],
+            send_sem=m["sent"].at[7],
             recv_sem=m["wz_recv"].at[z],
             device_id={"kv": z_of(i) * PLANE + q},
             device_id_type=MESH,
         )
 
     def sent(g, order, z_from, ref):
-        wait_group(m["picked"].at[g, order, others], m["y_send"].at[g, order])
+        wait_group(m["picked"].at[g, order, others], m["sent"].at[2])
 
     for g in range(2):
         for way in range(2):
@@ -625,9 +637,9 @@
         for d in range(8):
             @pl.when(z - d >= 0)
             def _():
-                wait_group(m["back"].at[g, d, others], m["b_send"].at[g, d])
-
-            for part in range(2):
+                wait_group(m["back"].at[g, d, others], m["sent"].at[3])
+
+            for part in range(ROW_PARTS):
                 if 0 < d < 5:
                     @pl.when(z - d >= 0)
                     def _():
@@ -642,26 +654,37 @@
         x_copy(False, 1, part).wait_send()
     x_copy(True, 2, 0).wait_send()
     x_copy(False, 2, 1).wait_send()
-    for i in range(n_i):
-        c_copy(i).wait_send()
+    for g in range(2):
+        for i in range(n_x):
+            c_copy(g, i).wait_send()
     out_q.wait()
 
-    for part in range(n_x):
+    for g, part in ((0, 0), (0, 1), (1, 0), (1, 1)):
         for r in (1, 3, 2):
-            wy_copy(part, r).wait_recv()
+            wy_copy(g, part, r).wait_recv()
+        if g == 0:
+            continue
         for i in (2 * part, 2 * part + 1):
-            total = m["wy_own"][i]
-            for r in range(1, N_Y):
-                total = total + m["wyr"][part, r, i % 2].astype(F32)
-            m["wz_own"][i] = total
-            m["wz"][i] = total.astype(BF16)
-        for i in (2 * part, 2 * part + 1):
+            total = []
+            for h in range(2):
+                total.append(m["wy_own"][h, i])
+                for r in range(1, N_Y):
+                    total[h] = total[h] + m["wyr"][h, part, r, i % 2].astype(F32)
+            tiles = [
+                jnp.where(low, total[0], pltpu.roll(total[1], HD, 1)),
+                jnp.where(low, pltpu.roll(total[0], HD, 1), total[1]),
+            ]
+            for h in range(2):
+                m["wz_own"][2 * i + h] = tiles[h]
+                m["wz"][2 * i + h] = tiles[h].astype(BF16)
+        for i in range(4 * part, 4 * part + 4):
             @pl.when(z_of(i) != z)
             def _():
                 wz_copy(i).start()
-    for part in range(n_x):
-        for r in range(1, N_Y):
-            wy_copy(part, r).wait_send()
+    for g in range(2):
+        for part in range(2):
+            for r in range(1, N_Y):
+                wy_copy(g, part, r).wait_send()
     mine = 2 * ((x + n_x - z // 2) % n_x) + z % 2
     total = m["wz_own"][mine]
     for r in range(1, n_z):
@@ -669,14 +692,14 @@
         pltpu.make_async_remote_copy(
             src_ref=m["wz"].at[0],
             dst_ref=m["wzr"].at[frm],
-            send_sem=m["wz_send"].at[0],
+            send_sem=m["sent"].at[7],
             recv_sem=m["wz_recv"].at[frm],
             device_id={"kv": frm * PLANE + q},
             device_id_type=MESH,
         ).wait_recv()
         total = total + m["wzr"][frm].astype(F32)
     weight_grad[...] = total
-    for i in range(n_i):
+    for i in range(n_z):
         @pl.when(z_of(i) != z)
         def _():
             wz_copy(i).wait_send()

time: 99.3 us -> 90.4 us (0.910)
  Pallas kernels: 95.3 us -> 86.3 us
    pallas_call x1, Pallas kernels: 93.2 us -> 84.3 us  [local(): pl.pallas_call(functools.partial(fused_kernel, [name for name, _ in scrat...]
where the time goes in v9:
time: 90.4 us; the launch traced here: 90.2 us
  Pallas kernels  86.3 us (95%)
  local copies, waits for them, and re-layouts  2.45 us (3%)
    pallas_call x1, Pallas kernels, local(): pl.pallas_call(functools.partial(fused_kernel, [name for name, _ in scrat...  84.3 us
    pallas_call x1, Pallas kernels, put_out(): pl.pallas_call(put_kernel, out_shape=tuple((jax.ShapeDtypeStruct(a.shape,...  2.05 us

profile of v9, /device:TPU:6, one launch (start us, length us, event | category | flops | bytes accessed | tf_op | source)
XLA Modules:
  0.0 90.2 jit_solution(4748888839189123558)
XLA Ops:
  0.6 0.0 copy-start
  0.7 0.7 copy-done
  1.4 0.1 constant_dynamic-slice_fusion
  1.5 0.1 copy.31
  1.6 0.1 select_bitcast_fusion
  1.7 0.1 reshape.45.refs_2_
  1.8 0.1 reshape.44.refs_1_
  1.9 0.1 select_reduce_fusion
  2.0 0.1 constant_dynamic-slice_fusion.1
  2.1 0.1 copy.25
  2.2 0.1 sub.27
  2.3 0.4 fusion.1
  2.7 0.0 copy-start.2
  2.7 0.1 copy.26
  2.8 0.0 copy-start.1
  2.8 0.1 reshape.43.refs_0_
  3.0 0.1 copy.30
  3.1 0.0 copy-start.3
  3.1 0.1 reshape.46.refs_3_
  3.2 0.3 copy-done.2
  3.6 0.2 copy-done.1
  3.7 0.1 copy-done.3
  3.8 84.3 %fused.1 = (f32[384,512]{1,0:T(8,128)}, f32[384,128]{1,0:T(8,128)S(1)}, f32[384,128]{1,0:T(8,128)S(1)}, f32[64,128]{1,0:T(8,128)S(1)}) custom-call(s32[128]{0:T(128)S(1)} %reshape.43.refs_0_, s32[192]{0:T(256)S(1)} %reshape.44.refs_1_, s32[192]{0:T(256)S(1)} %reshape.45.refs_2_, s32[840]{0:T(1024)S(1)} %reshape.46.refs_3_, bf16[6,64,128]{2,1,0:T(8,128)(2,1)S(1)} %bitcast.7, ...), custom_call_target="tpu_custom_call" | custom-call | tf_op jit(solution)/shard_map/fused/pallas_call | solution.py:781
  88.1 2.1 %put_out.1 = (f32[384,512]{1,0:T(8,128)}, f32[384,128]{1,0:T(8,128)}, f32[384,128]{1,0:T(8,128)}, f32[64,128]{1,0:T(8,128)}) custom-call(f32[384,512]{1,0:T(8,128)} %get-tuple-element.8.q_src, f32[384,128]{1,0:T(8,128)S(1)} %get-tuple-element.9.k_src, f32[384,128]{1,0:T(8,128)S(1)} %get-tuple-element.10.v_src, f32[64,128]{1,0:T(8,128)S(1)} %get-tuple-element.11.w_src), custom_call_target="tpu_custom_call" | custom-call | tf_op jit(solution)/shard_map/put_out/pallas_call | solution.py:734
  (5 shorter events, 0.0 us)
Async XLA Ops:
  0.6 0.8 copy-start
  2.7 0.9 copy-start.2
  2.8 0.9 %copy-start.1 = (bf16[384,128]{1,0:T(8,128)(2,1)S(1)}, bf16[384,128]{1,0:T(8,128)(2,1)}, u32[]{:S(2)}) copy-start(bf16[384,128]{1,0:T(8,128)(2,1)} %param.8) | copy-start | bytes 294916
  3.1 0.7 copy-start.3

commit v10 on v9

--- a/solution.py
+++ b/solution.py
@@ -11,7 +11,7 @@
 BLOCK = 64
 NEG = -1e30
 LOG2E = 1.4426950408889634
-CHUNK = 4
+CHUNK = 8
 PARTS = 3
 ROW_PARTS = 4
 PART_ROWS = BLOCK // ROW_PARTS
@@ -91,10 +91,9 @@
 
 
 def fused_kernel(names, n_z, n_x, n_list, *refs):
-    idx_picks, idx_slots, idx_kinds, idx_inv = refs[:4]
-    keys, vals, queries, out_grad, log_sums, inputs = refs[4:10]
-    query_grad, key_grad, value_grad, weight_grad = refs[10:14]
-    m = dict(zip(names, refs[14:]))
+    idx, keys, vals, queries, out_grad, log_sums, inputs = refs[:7]
+    query_grad, key_grad, value_grad, weight_grad = refs[7:11]
+    m = dict(zip(names, refs[11:]))
     n_b = m["kraw"].shape[0]
     n_dev = n_z * PLANE
     heads = m["lraw"].shape[0]
@@ -208,7 +207,7 @@
     def pick(g, order, z_from, ref):
         def one(r, carry):
             to = (q + r) % PLANE
-            m["picked"][g, order, r] = ref[idx_picks[(z_from * PLANE + to) * 2 + g]]
+            m["picked"][g, order, r] = ref[idx[24 + g * n_z + z_from, to * n_b]]
 
             @pl.when(r > 1)
             def _():
@@ -217,7 +216,7 @@
             return carry
 
         lax.fori_loop(1, PLANE, one, 0)
-        m[f"tab{g}"][z_from * PLANE + q] = ref[idx_picks[(z_from * PLANE + q) * 2 + g]]
+        m[f"tab{g}"][z_from * PLANE + q] = ref[idx[24 + g * n_z + z_from, q * n_b]]
         y_copy(g, order, z_from, PLANE - 1).start()
 
     def each_piece(g, step, act):
@@ -312,13 +311,12 @@
 
         def one_position(p, carry):
             row = pl.multiple_of(p * BLOCK, BLOCK)
-            unit = (p * 2 + g) * n_list
             for r, part in enumerate(masked_rows(m["qraw"], row, g, HD ** -0.5, 0)):
                 qd[r * BLOCK : (r + 1) * BLOCK, :] = part
             for r, part in enumerate(masked_rows(m["graw"], row, g, 1.0, 1)):
                 qd[cols + r * BLOCK : cols + (r + 1) * BLOCK, :] = part
             for n in range(n_list):
-                cat[n] = tab[idx_slots[unit + n]]
+                cat[n] = tab[idx[p, g * n_list + n]]
             for kind in range(3):
                 shift[kind] = m["bias"][kind] - m["lse"][p * 2 + g] * LOG2E
 
@@ -329,7 +327,7 @@
                 ).reshape(CHUNK, BLOCK, 2 * cols)
                 for n in range(ch.start, ch.stop):
                     prod = both[n - ch.start]
-                    pr = jnp.exp2(prod[:, :cols] * LOG2E + shift[idx_kinds[unit + n]])
+                    pr = jnp.exp2(prod[:, :cols] * LOG2E + shift[idx[p, (2 + g) * n_list + n]])
                     sdp[n, :, :cols] = pr
                     sdp[n, :, cols:] = prod[:, cols:]
                     pd[n, :, cols:] = pr.astype(BF16)
@@ -367,10 +365,9 @@
         lax.fori_loop(0, n_b, one_position, 0)
 
     def summed_terms(g, j):
-        at = (g * (n_dev + n_b) + j) * n_b
-        total = m["terms"][0, idx_inv[at]]
+        total = m["terms"][0, idx[8 + 8 * g, j]]
         for p in range(1, n_b):
-            total = total + m["terms"][p, idx_inv[at + p]]
+            total = total + m["terms"][p, idx[8 + 8 * g + p, j]]
         return total
 
     def b_copy(g, d, r):
@@ -410,7 +407,7 @@
             else:
                 val = m["back"][g, d, frm, rows, :]
             val = val.astype(F32)
-            block = idx_picks[((z - d) * PLANE + frm) * 2 + g]
+            block = idx[24 + g * n_z + z - d, frm * n_b]
             for b in range(n_b):
                 accs[b] = accs[b] + jnp.where(block == b, val, 0.0)
         for b in range(n_b):
@@ -742,29 +739,56 @@
     )(*arrays)
 
 
-def index_table(chosen, n_b, n_dev):
-    groups, _, n_list = chosen.shape
-    me = lax.axis_index("kv")
-    z, q = place()
-    plane = lax.dynamic_slice_in_dim(chosen, z * PLANE * n_b, PLANE * n_b, 1)
-    column = (jnp.arange(n_dev // PLANE) * PLANE + q) * n_b
-    offs = plane[..., None] - column
-    offs = jnp.where((offs >= 0) & (offs < n_b), offs, 0)
-    picks = jnp.max(offs.reshape(groups, PLANE, n_b * n_list, -1), axis=2)
-    picks = picks.transpose(2, 1, 0).reshape(-1)
-    lists = lax.dynamic_slice_in_dim(chosen, me * n_b, n_b, 1)
-    owner = lists // n_b
-    slot = jnp.where(owner == me, n_dev + lists % n_b, jnp.maximum(owner, 0))
-    at_diag = lists == me * n_b + jnp.arange(n_b)[None, :, None]
-    kind = jnp.where(lists < 0, 2, at_diag.astype(jnp.int32))
-    listed = (slot[..., None] == jnp.arange(n_dev + n_b)) & (lists >= 0)[..., None]
-    inverse = jnp.min(
-        jnp.where(listed, jnp.arange(n_list)[:, None], n_list), axis=2
-    )
-    slots = slot.transpose(1, 0, 2).reshape(-1)
-    kinds = kind.transpose(1, 0, 2).reshape(-1)
-    inverse = inverse.transpose(0, 2, 1).reshape(-1)
-    return picks, slots, kinds, inverse
+def index_kernel(n_dev, n_b, place_of, lists, out, flat):
+    z, q = place_of()
+    me = z * PLANE + q
+    n_list = lists.shape[1]
+    n_z = n_dev // PLANE
+    width = lists.shape[2]
+    heads = []
+    for g in range(2):
+        near = pltpu.roll(lists[g], (width - z * PLANE * n_b) % width, 1)[:, :128]
+        heads.append(near)
+        for plane in range(n_z):
+            offs = near - (plane * PLANE + q) * n_b
+            offs = jnp.where((offs >= 0) & (offs < n_b), offs, 0)
+            out[24 + g * n_z + plane : 25 + g * n_z + plane, :] = offs.max(axis=0, keepdims=True)
+    best = out[24 : 24 + 2 * n_z, :]
+    widest = best
+    for k in range(1, n_b):
+        widest = jnp.maximum(widest, pltpu.roll(best, 128 - k, 1))
+    out[24 : 24 + 2 * n_z, :] = widest
+    both = pltpu.roll(jnp.concatenate(heads, axis=0), (128 - q * n_b) % 128, 1)
+    flat[...] = jnp.zeros((128, 128), jnp.int32)
+    flat[: 2 * n_list, :] = both
+    entry = flat[...].T[:8, :]
+    block = lax.broadcasted_iota(jnp.int32, (8, 128), 0)
+    lane = lax.broadcasted_iota(jnp.int32, (8, 128), 1)
+    owner = jnp.floor((entry.astype(F32) + 0.5) * (1.0 / n_b)).astype(jnp.int32)
+    slot = jnp.where(owner == me, n_dev + entry - owner * n_b, jnp.maximum(owner, 0))
+    kind = jnp.where(entry < 0, 2, jnp.where(entry == me * n_b + block, 1, 0))
+    out[:8, :] = jnp.where(lane < 2 * n_list, slot, pltpu.roll(kind, 2 * n_list, 1))
+    used = jnp.where(entry < 0, -1, slot)
+    for g in range(2):
+        found = jnp.full((8, 128), n_list, jnp.int32)
+        for n in range(n_list):
+            at = g * n_list + n
+            found = jnp.where(used[:, at : at + 1] == lane, n, found)
+        out[8 + 8 * g : 16 + 8 * g, :] = found
+
+
+def index_table(chosen, n_b, n_dev, place_of=place, interpret=False):
+    vm = pl.BlockSpec(memory_space=pltpu.VMEM)
+    return pl.pallas_call(
+        functools.partial(index_kernel, n_dev, n_b, place_of),
+        out_shape=jax.ShapeDtypeStruct((24 + 2 * n_dev // PLANE, 128), jnp.int32),
+        in_specs=[vm],
+        out_specs=vm,
+        scratch_shapes=[pltpu.VMEM((128, 128), jnp.int32)],
+        compiler_params=pltpu.CompilerParams(vmem_limit_bytes=4 * 1024 * 1024),
+        name="index",
+        interpret=interpret,
+    )(chosen.transpose(0, 2, 1))
 
 
 def local(queries, key_heads, values, log_sums, out_grad, inputs, chosen):
@@ -788,7 +812,7 @@
             jax.ShapeDtypeStruct(values.shape, F32),
             jax.ShapeDtypeStruct((feats * n_x // n_dev, 128), F32),
         ),
-        in_specs=[pl.BlockSpec(memory_space=pltpu.SMEM)] * 4 + [hbm] * 6,
+        in_specs=[pl.BlockSpec(memory_space=pltpu.SMEM)] + [hbm] * 6,
         out_specs=(hbm, vm, vm, vm),
         scratch_shapes=[kind for _, kind in scratch],
         compiler_params=pltpu.CompilerParams(
@@ -796,7 +820,7 @@
         ),
         name="fused",
     )(
-        *idx,
+        idx,
         key_heads.reshape(n_b, BLOCK, -1),
         values.reshape(n_b, BLOCK, -1),
         queries,

time: 90.4 us -> 90.6 us (level)
    unnamed x9 -> x8, local copies, waits for them, and re-layouts: 1.43 us -> 2.9 us
where the time goes in v10:
time: 90.6 us; the launch traced here: 90.3 us
  Pallas kernels  86.8 us (96%)
  local copies, waits for them, and re-layouts  2.9 us (3%)
    pallas_call x1, Pallas kernels, local(): pl.pallas_call(functools.partial(fused_kernel, [name for name, _ in scrat...  84.3 us
    unnamed x8, local copies, waits for them, and re-layouts  2.9 us
    pallas_call x1, Pallas kernels, put_out(): pl.pallas_call(put_kernel, out_shape=tuple((jax.ShapeDtypeStruct(a.shape,...  2.05 us

profile of v10, /device:TPU:6, one launch (start us, length us, event | category | flops | bytes accessed | tf_op | source)
XLA Modules:
  0.0 90.3 jit_solution(795345133532176393)
XLA Ops:
  0.6 0.0 copy-start.2
  0.6 0.8 copy-done.2
  1.4 0.0 copy-start.3
  1.4 0.4 index.1.refs_0_
  1.8 0.3 copy-done.3
  2.1 0.0 copy-start
  2.1 0.9 copy-done
  3.0 0.0 copy-start.1
  3.0 0.9 copy-done.1
  3.9 84.3 %fused.1 = (f32[384,512]{1,0:T(8,128)}, f32[384,128]{1,0:T(8,128)S(1)}, f32[384,128]{1,0:T(8,128)S(1)}, f32[64,128]{1,0:T(8,128)S(1)}) custom-call(s32[40,128]{1,0:T(8,128)S(1)} %index.1.refs_0_, bf16[6,64,128]{2,1,0:T(8,128)(2,1)S(1)} %bitcast.3, bf16[6,64,128]{2,1,0:T(8,128)(2,1)S(1)} %bitcast.4, bf16[384,512]{1,0:T(8,128)(2,1)} %refs_3_.1, ...), custom_call_target="tpu_custom_call" | custom-call | tf_op jit(solution)/shard_map/fused/pallas_call | solution.py:805
  88.3 2.1 %put_out.1 = (f32[384,512]{1,0:T(8,128)}, f32[384,128]{1,0:T(8,128)}, f32[384,128]{1,0:T(8,128)}, f32[64,128]{1,0:T(8,128)}) custom-call(f32[384,512]{1,0:T(8,128)} %get-tuple-element.8.q_src, f32[384,128]{1,0:T(8,128)S(1)} %get-tuple-element.9.k_src, f32[384,128]{1,0:T(8,128)S(1)} %get-tuple-element.10.v_src, f32[64,128]{1,0:T(8,128)S(1)} %get-tuple-element.11.w_src), custom_call_target="tpu_custom_call" | custom-call | tf_op jit(solution)/shard_map/put_out/pallas_call | solution.py:731
Async XLA Ops:
  0.6 0.8 copy-start.2
  1.4 0.7 copy-start.3
  2.1 0.9 copy-start
  3.0 0.9 copy-start.1

commit v11 on v10

--- a/solution.py
+++ b/solution.py
@@ -786,6 +786,7 @@
         out_specs=vm,
         scratch_shapes=[pltpu.VMEM((128, 128), jnp.int32)],
         compiler_params=pltpu.CompilerParams(vmem_limit_bytes=4 * 1024 * 1024),
+        cost_estimate=pl.CostEstimate(flops=10**9, bytes_accessed=8 * 1024 * 1024, transcendentals=0),
         name="index",
         interpret=interpret,
     )(chosen.transpose(0, 2, 1))

time: 90.6 us -> 89 us (0.982)
  local copies, waits for them, and re-layouts: 2.9 us -> 1.33 us
    unnamed x8, local copies, waits for them, and re-layouts: 2.9 us -> 1.33 us
where the time goes in v11:
time: 89 us; the launch traced here: 88.8 us
  Pallas kernels  86.8 us (98%)
  local copies, waits for them, and re-layouts  1.33 us (1%)
    pallas_call x1, Pallas kernels, local(): pl.pallas_call(functools.partial(fused_kernel, [name for name, _ in scrat...  84.4 us
    pallas_call x1, Pallas kernels, put_out(): pl.pallas_call(put_kernel, out_shape=tuple((jax.ShapeDtypeStruct(a.shape,...  2.05 us

profile of v11, /device:TPU:6, one launch (start us, length us, event | category | flops | bytes accessed | tf_op | source)
XLA Modules:
  0.0 88.8 jit_solution(1237551179416172322)
XLA Ops:
  0.6 0.0 copy-start.3
  0.6 0.8 copy-done.3
  1.4 0.0 copy-start
  1.4 0.0 copy-start.1
  1.4 0.0 copy-start.2
  1.4 0.4 index.1.refs_0_
  1.8 0.5 copy-done
  2.3 0.0 copy-done.1
  2.4 0.0 copy-done.2
  2.4 84.4 %fused.1 = (f32[384,512]{1,0:T(8,128)}, f32[384,128]{1,0:T(8,128)S(1)}, f32[384,128]{1,0:T(8,128)S(1)}, f32[64,128]{1,0:T(8,128)S(1)}) custom-call(s32[40,128]{1,0:T(8,128)S(1)} %index.1.refs_0_, bf16[6,64,128]{2,1,0:T(8,128)(2,1)S(1)} %bitcast.3, bf16[6,64,128]{2,1,0:T(8,128)(2,1)S(1)} %bitcast.4, bf16[384,512]{1,0:T(8,128)(2,1)} %refs_3_.1, ...), custom_call_target="tpu_custom_call" | custom-call | tf_op jit(solution)/shard_map/fused/pallas_call | solution.py:806
  86.8 2.1 %put_out.1 = (f32[384,512]{1,0:T(8,128)}, f32[384,128]{1,0:T(8,128)}, f32[384,128]{1,0:T(8,128)}, f32[64,128]{1,0:T(8,128)}) custom-call(f32[384,512]{1,0:T(8,128)} %get-tuple-element.8.q_src, f32[384,128]{1,0:T(8,128)S(1)} %get-tuple-element.9.k_src, f32[384,128]{1,0:T(8,128)S(1)} %get-tuple-element.10.v_src, f32[64,128]{1,0:T(8,128)S(1)} %get-tuple-element.11.w_src), custom_call_target="tpu_custom_call" | custom-call | tf_op jit(solution)/shard_map/put_out/pallas_call | solution.py:731
Async XLA Ops:
  0.6 0.8 copy-start.3
  1.4 0.9 %copy-start = (bf16[384,128]{1,0:T(8,128)(2,1)S(1)}, bf16[384,128]{1,0:T(8,128)(2,1)}, u32[]{:S(2)}) copy-start(bf16[384,128]{1,0:T(8,128)(2,1)} %param.8) | copy-start | bytes 294916
  1.4 0.9 %copy-start.1 = (bf16[384,128]{1,0:T(8,128)(2,1)S(1)}, bf16[384,128]{1,0:T(8,128)(2,1)}, u32[]{:S(2)}) copy-start(bf16[384,128]{1,0:T(8,128)(2,1)} %param.9) | copy-start | bytes 294916
  1.4 0.9 %copy-start.2 = (f32[8,384]{1,0:T(8,128)S(1)}, f32[8,384]{1,0:T(8,128)}, u32[]{:S(2)}) copy-start(f32[8,384]{1,0:T(8,128)} %refs_5_.1) | copy-start | bytes 36868

commit v12 on v11

--- a/solution.py
+++ b/solution.py
@@ -498,8 +498,8 @@
     attention(
         0,
         {
-            0: functools.partial(relay_and_pick, 1, 3),
-            2: functools.partial(relay_and_pick, 1, 4),
+            1: functools.partial(relay_and_pick, 1, 3),
+            3: functools.partial(relay_and_pick, 1, 4),
             4: relay_x,
         },
     )

time: 89 us -> 87.6 us (0.984)
  Pallas kernels: 86.8 us -> 85.4 us
    pallas_call x1, Pallas kernels: 84.4 us -> 83 us  [local(): pl.pallas_call(functools.partial(fused_kernel, [name for name, _ in scrat...]
where the time goes in v12:
time: 87.6 us; the launch traced here: 87.4 us
  Pallas kernels  85.4 us (97%)
  local copies, waits for them, and re-layouts  1.33 us (2%)
    pallas_call x1, Pallas kernels, local(): pl.pallas_call(functools.partial(fused_kernel, [name for name, _ in scrat...  83 us
    pallas_call x1, Pallas kernels, put_out(): pl.pallas_call(put_kernel, out_shape=tuple((jax.ShapeDtypeStruct(a.shape,...  2.05 us

profile of v12, /device:TPU:6, one launch (start us, length us, event | category | flops | bytes accessed | tf_op | source)
XLA Modules:
  0.0 87.4 jit_solution(6562658520206503099)
XLA Ops:
  0.6 0.0 copy-start.3
  0.6 0.8 copy-done.3
  1.4 0.0 copy-start
  1.4 0.0 copy-start.1
  1.4 0.0 copy-start.2
  1.4 0.4 index.1.refs_0_
  1.8 0.5 copy-done
  2.3 0.0 copy-done.1
  2.4 0.0 copy-done.2
  2.4 83.0 %fused.1 = (f32[384,512]{1,0:T(8,128)}, f32[384,128]{1,0:T(8,128)S(1)}, f32[384,128]{1,0:T(8,128)S(1)}, f32[64,128]{1,0:T(8,128)S(1)}) custom-call(s32[40,128]{1,0:T(8,128)S(1)} %index.1.refs_0_, bf16[6,64,128]{2,1,0:T(8,128)(2,1)S(1)} %bitcast.3, bf16[6,64,128]{2,1,0:T(8,128)(2,1)S(1)} %bitcast.4, bf16[384,512]{1,0:T(8,128)(2,1)} %refs_3_.1, ...), custom_call_target="tpu_custom_call" | custom-call | tf_op jit(solution)/shard_map/fused/pallas_call | solution.py:806
  85.3 2.1 %put_out.1 = (f32[384,512]{1,0:T(8,128)}, f32[384,128]{1,0:T(8,128)}, f32[384,128]{1,0:T(8,128)}, f32[64,128]{1,0:T(8,128)}) custom-call(f32[384,512]{1,0:T(8,128)} %get-tuple-element.8.q_src, f32[384,128]{1,0:T(8,128)S(1)} %get-tuple-element.9.k_src, f32[384,128]{1,0:T(8,128)S(1)} %get-tuple-element.10.v_src, f32[64,128]{1,0:T(8,128)S(1)} %get-tuple-element.11.w_src), custom_call_target="tpu_custom_call" | custom-call | tf_op jit(solution)/shard_map/put_out/pallas_call | solution.py:731
Async XLA Ops:
  0.6 0.8 copy-start.3
  1.4 0.9 %copy-start = (bf16[384,128]{1,0:T(8,128)(2,1)S(1)}, bf16[384,128]{1,0:T(8,128)(2,1)}, u32[]{:S(2)}) copy-start(bf16[384,128]{1,0:T(8,128)(2,1)} %param.8) | copy-start | bytes 294916
  1.4 0.9 %copy-start.1 = (bf16[384,128]{1,0:T(8,128)(2,1)S(1)}, bf16[384,128]{1,0:T(8,128)(2,1)}, u32[]{:S(2)}) copy-start(bf16[384,128]{1,0:T(8,128)(2,1)} %param.9) | copy-start | bytes 294916
  1.4 0.9 %copy-start.2 = (f32[8,384]{1,0:T(8,128)S(1)}, f32[8,384]{1,0:T(8,128)}, u32[]{:S(2)}) copy-start(f32[8,384]{1,0:T(8,128)} %refs_5_.1) | copy-start | bytes 36868

commit v13 on v12

--- a/solution.py
+++ b/solution.py
@@ -702,25 +702,12 @@
             wz_copy(i).wait_send()
 
 
-def put_kernel(q_src, k_src, v_src, w_src, q_dst, k_dst, v_dst, w_dst, q_mid, sem):
-    rows = q_mid.shape[0] // 3
-    part = [pl.ds(i * rows, rows) for i in range(3)]
-    into = [
-        pltpu.make_async_copy(q_src.at[part[i]], q_mid.at[part[i]], sem.at[i]) for i in range(3)
-    ]
-    rest = [
-        pltpu.make_async_copy(src, dst, sem.at[3 + i])
-        for i, (src, dst) in enumerate([(k_src, k_dst), (v_src, v_dst), (w_src, w_dst)])
-    ]
-    out = [
-        pltpu.make_async_copy(q_mid.at[part[i]], q_dst.at[part[i]], sem.at[6 + i]) for i in range(3)
-    ]
-    for copy in into + rest:
+def put_kernel(q_src, k_src, v_src, w_src, q_dst, k_dst, v_dst, w_dst, sem):
+    pairs = [(q_src, q_dst), (k_src, k_dst), (v_src, v_dst), (w_src, w_dst)]
+    copies = [pltpu.make_async_copy(src, dst, sem.at[i]) for i, (src, dst) in enumerate(pairs)]
+    for copy in copies:
         copy.start()
-    for i in range(3):
-        into[i].wait()
-        out[i].start()
-    for copy in rest + out:
+    for copy in copies:
         copy.wait()
 
 
@@ -731,10 +718,10 @@
     return pl.pallas_call(
         put_kernel,
         out_shape=tuple(jax.ShapeDtypeStruct(a.shape, a.dtype) for a in arrays),
-        in_specs=[hbm, vm, vm, vm],
+        in_specs=[vm] * 4,
         out_specs=(hbm,) * 4,
-        scratch_shapes=[pltpu.VMEM(query_grad.shape, F32), pltpu.SemaphoreType.DMA((9,))],
-        compiler_params=pltpu.CompilerParams(vmem_limit_bytes=int(53.4 * 1024 * 1024)),
+        scratch_shapes=[pltpu.SemaphoreType.DMA((4,))],
+        compiler_params=pltpu.CompilerParams(vmem_limit_bytes=50 * 1024 * 1024),
         name="put_out",
     )(*arrays)
 
@@ -817,7 +804,7 @@
         out_specs=(hbm, vm, vm, vm),
         scratch_shapes=[kind for _, kind in scratch],
         compiler_params=pltpu.CompilerParams(
-            collective_id=0, has_side_effects=True, vmem_limit_bytes=53 * 1024 * 1024
+            collective_id=0, has_side_effects=True, vmem_limit_bytes=50 * 1024 * 1024
         ),
         name="fused",
     )(

time: 87.6 us -> 87.1 us (level)
  Pallas kernels: 85.4 us -> 84.5 us
    pallas_call x1, Pallas kernels: 2.05 us -> 1.04 us  [put_out(): pl.pallas_call(put_kernel, out_shape=tuple((jax.ShapeDtypeStruct(a.shape,...]
    unnamed x8 -> x14, local copies, waits for them, and re-layouts: 1.33 us -> 1.76 us
where the time goes in v13:
time: 87.1 us; the launch traced here: 87 us
  Pallas kernels  84.5 us (97%)
  local copies, waits for them, and re-layouts  1.76 us (2%)
    pallas_call x1, Pallas kernels, local(): pl.pallas_call(functools.partial(fused_kernel, [name for name, _ in scrat...  83.1 us
    unnamed x14, local copies, waits for them, and re-layouts  1.76 us

profile of v13, /device:TPU:6, one launch (start us, length us, event | category | flops | bytes accessed | tf_op | source)
XLA Modules:
  0.0 87.0 jit_solution(6155962185316464913)
XLA Ops:
  0.6 0.0 copy-start.6
  0.6 0.8 copy-done.6
  1.4 0.0 copy-start
  1.4 0.0 copy-start.1
  1.4 0.0 copy-start.2
  1.4 0.0 copy-start.3
  1.4 0.0 copy-start.4
  1.5 0.0 copy-start.5
  1.5 0.4 index.1.refs_0_
  1.9 0.7 copy-done
  2.6 0.1 copy-done.1
  2.7 0.1 copy-done.2
  2.8 0.0 copy-done.3
  2.8 0.0 copy-done.4
  2.8 0.0 copy-done.5
  2.8 83.1 %fused.1 = (f32[384,512]{1,0:T(8,128)S(1)}, f32[384,128]{1,0:T(8,128)S(1)}, f32[384,128]{1,0:T(8,128)S(1)}, f32[64,128]{1,0:T(8,128)S(1)}) custom-call(s32[40,128]{1,0:T(8,128)S(1)} %index.1.refs_0_, bf16[6,64,128]{2,1,0:T(8,128)(2,1)S(1)} %bitcast.3, bf16[6,64,128]{2,1,0:T(8,128)(2,1)S(1)} %bitcast.4, bf16[384,512]{1,0:T(8,128)(2,1)S(1)} %copy-done.1, ...), custom_call_target="tpu_custom_call" | custom-call | tf_op jit(solution)/shard_map/fused/pallas_call | solution.py:793
  85.9 1.0 %put_out.1 = (f32[384,512]{1,0:T(8,128)}, f32[384,128]{1,0:T(8,128)}, f32[384,128]{1,0:T(8,128)}, f32[64,128]{1,0:T(8,128)}) custom-call(f32[384,512]{1,0:T(8,128)S(1)} %get-tuple-element.8.q_src, f32[384,128]{1,0:T(8,128)S(1)} %get-tuple-element.9.k_src, f32[384,128]{1,0:T(8,128)S(1)} %get-tuple-element.10.v_src, f32[64,128]{1,0:T(8,128)S(1)} %get-tuple-element.11.w_src), custom_call_target="tpu_custom_call" | custom-call | tf_op jit(solution)/shard_map/put_out/pallas_call | solution.py:718
Async XLA Ops:
  0.6 0.8 copy-start.6
  1.4 1.1 %copy-start = (bf16[384,1024]{1,0:T(8,128)(2,1)S(1)}, bf16[384,1024]{1,0:T(8,128)(2,1)}, u32[]{:S(2)}) copy-start(bf16[384,1024]{1,0:T(8,128)(2,1)} %refs_6_.1) | copy-start | bytes 2359300
  1.4 1.2 %copy-start.1 = (bf16[384,512]{1,0:T(8,128)(2,1)S(1)}, bf16[384,512]{1,0:T(8,128)(2,1)}, u32[]{:S(2)}) copy-start(bf16[384,512]{1,0:T(8,128)(2,1)} %refs_3_.1) | copy-start | bytes 1179652
  1.4 1.3 %copy-start.2 = (bf16[384,512]{1,0:T(8,128)(2,1)S(1)}, bf16[384,512]{1,0:T(8,128)(2,1)}, u32[]{:S(2)}) copy-start(bf16[384,512]{1,0:T(8,128)(2,1)} %refs_4_.1) | copy-start | bytes 1179652
  1.4 1.4 %copy-start.3 = (bf16[384,128]{1,0:T(8,128)(2,1)S(1)}, bf16[384,128]{1,0:T(8,128)(2,1)}, u32[]{:S(2)}) copy-start(bf16[384,128]{1,0:T(8,128)(2,1)} %param.8) | copy-start | bytes 294916
  1.4 1.4 %copy-start.4 = (bf16[384,128]{1,0:T(8,128)(2,1)S(1)}, bf16[384,128]{1,0:T(8,128)(2,1)}, u32[]{:S(2)}) copy-start(bf16[384,128]{1,0:T(8,128)(2,1)} %param.9) | copy-start | bytes 294916
  1.5 1.4 %copy-start.5 = (f32[8,384]{1,0:T(8,128)S(1)}, f32[8,384]{1,0:T(8,128)}, u32[]{:S(2)}) copy-start(f32[8,384]{1,0:T(8,128)} %refs_5_.1) | copy-start | bytes 36868
